TPU v7x, 512 devices: a whole 4x8x8 slice. The times are simulated.
512 devices in a mesh: sp: 64 (over z, y), fs: 4 (over x), tp: 2 (over core).
Axes of the slice: x: 4, y: 8, z: 8, core: 2. Of those that a mesh axis runs over, the one named last changes fastest.
Arguments:
- tokens: bfloat16 [16384, 2048], P('sp', ('fs', 'tp')), may hold values from -500 to 500
- norm_gain: float32 [2048], replicated, may hold values from 0.1 to 1.9
- query_w: bfloat16 [2048, 1024], P('sp', ('fs', 'tp')), may hold values from -1 to 1
- key_w: bfloat16 [2048, 512], P('sp', ('fs', 'tp')), may hold values from -1 to 1
- value_w: bfloat16 [2048, 512], P('sp', ('fs', 'tp')), may hold values from -0.125 to 0.125
- recept_w: bfloat16 [2048, 1024], P('sp', ('fs', 'tp')), may hold values from -0.125 to 0.125
- rec_key_w: bfloat16 [2048, 1024], P('sp', ('fs', 'tp')), may hold values from -0.125 to 0.125
- rec_value_w: bfloat16 [2048, 1024], P('sp', ('fs', 'tp')), may hold values from -0.125 to 0.125
- decay_down: bfloat16 [2048, 64], replicated, may hold values from -0.125 to 0.125
- decay_up: bfloat16 [64, 1024], replicated, may hold values from -1 to 1
- decay_base: float32 [16, 16384], P(('fs', 'tp'), 'sp'), may hold values from -14 to 0
- learn_rate: float32 [1024], P(('fs', 'tp')), may hold values from 0.1 to 1
- query_gain: float32 [64], replicated, may hold values from 0 to 7
- key_gain: float32 [64], replicated, may hold values from 0 to 7
- sink_logit: float32 [16], P(('fs', 'tp')), may hold values from 1 to 5
- group_gain: float32 [1024], P(('fs', 'tp')), may hold values from 0.1 to 1.9
- out_att_w: bfloat16 [1024, 2048], P(('fs', 'tp'), 'sp'), may hold values from -0.75 to 0.75
- out_rec_w: bfloat16 [1024, 2048], P(('fs', 'tp'), 'sp'), may hold values from -0.1875 to 0.1875
Outputs:
- mixed: bfloat16 [16384, 2048], P(('sp', 'fs', 'tp'))
- row_lse: float32 [16, 16384], P(('fs', 'tp'), 'sp')
All inputs are finite; a program needn't handle non-finite values.
Results may differ from a plain program's by a relative error of at most 0.015.
Values may be sent and summed in bfloat16 or wider, within the bound.
No kernel may reach another device: no remote copies, remote signals or barrier semaphores. Data moves between devices by JAX's collectives and lax.ppermute only.
A program may use at most 64 MiB of HBM per device.

v0:
```python
import math

import jax
import jax.numpy as jnp
from jax import lax
from jax.sharding import Mesh
from jax.sharding import PartitionSpec as P

HEAD = 64
WINDOW = 128
BLOCK = 32
SP = ("sp_0", "sp_1")
SP_FS_TP = ("sp_0", "sp_1", "fs", "tp")


NORM_EPS = 1e-06
KEY_EPS = 1e-06
GROUP_EPS = 0.00064


def passed_along(array, axis, by):
    devices = lax.axis_size(axis)
    pairs = [(i, i + by) for i in range(devices) if 0 <= i + by < devices]
    return lax.ppermute(array, axis, pairs)


def filled_with(array, identity):
    return jnp.broadcast_to(jnp.asarray(identity, array.dtype), array.shape)


def prefix_by_axis(array, axes, combine, identity):
    before = start = filled_with(array, identity)
    total = array
    for axis in reversed(axes):
        devices, place = (lax.axis_size(axis), lax.axis_index(axis))
        pieces = lax.all_gather(total.astype(jnp.bfloat16), axis)
        inside, total = (start, start)
        for k in range(devices):
            passed = k < place
            total = combine(total, pieces[k].astype(array.dtype))
            inside = jnp.where(passed, total, inside)
        before = combine(inside, before)
    return before


def from_everyone(array, axis):
    copies = jnp.broadcast_to(array, (lax.axis_size(axis), *array.shape))
    return lax.all_to_all(copies, axis, split_axis=0, concat_axis=0, tiled=True)


def joined_along(tiles, dim):
    tiles = jnp.moveaxis(tiles, 0, dim)
    dims = tiles.shape
    return tiles.reshape(*dims[:dim], dims[dim] * dims[dim + 1], *dims[dim + 2 :])


def collect(array, axis, dim):
    tiles = from_everyone(array, axis)
    return joined_along(tiles, dim)


def sent_together(arrays, axis, dim, along):
    ends, at = ([], 0)
    for a in arrays[:-1]:
        at += a.shape[along]
        ends.append(at)
    both = jnp.concatenate(arrays, axis=along)
    return tuple(jnp.split(lax.all_gather(both, axis, axis=dim, tiled=True), ends, axis=along))


def turned_gather(arrays, axis, dims):
    turned = [jnp.moveaxis(a, dim, 0) for a, dim in zip(arrays, dims)]
    widths = [t[0].size for t in turned]
    both = jnp.concatenate([t.reshape(-1, w) for t, w in zip(turned, widths)], axis=1)
    filled = lax.all_gather(both, axis, axis=0, tiled=True)
    tiles = jnp.split(filled, [sum(widths[:k]) for k in range(1, len(widths))], axis=1)
    return tuple(
        (
            jnp.moveaxis(b.reshape(-1, *t.shape[1:]), 0, dim)
            for b, t, dim in zip(tiles, turned, dims)
        )
    )


def in_blocks(array, dim, devices):
    dims = array.shape
    tiles = array.reshape(*dims[:dim], devices, dims[dim] // devices, *dims[dim + 1 :])
    return jnp.moveaxis(tiles, dim, 0)


def summed_on_arrival(array, axis, dim):
    devices = lax.axis_size(axis)
    tiles = lax.all_to_all(in_blocks(array, dim, devices), axis, 0, 0, tiled=True)
    return jnp.sum(tiles.astype(jnp.float32), axis=0)


def head_rms(values, gain_vec, num_heads):
    shaped = values.astype(jnp.float32).reshape(values.shape[0], num_heads, HEAD)
    mean_sq = jnp.mean(shaped * shaped, axis=-1, keepdims=True)
    return (shaped * lax.rsqrt(mean_sq + NORM_EPS) * gain_vec).astype(jnp.bfloat16)


def attend(query_rows, key_rows, value_rows, query_gain, key_gain, sink_logit):
    num_rows = query_rows.shape[0]
    num_heads = query_rows.shape[1] // HEAD
    kv_heads = key_rows.shape[1] // HEAD
    group_size = num_heads // kv_heads
    blocks = num_rows // WINDOW
    query_n = head_rms(query_rows, query_gain, num_heads).reshape(
        blocks, WINDOW, kv_heads, group_size, HEAD
    )
    key_n = head_rms(key_rows, key_gain, kv_heads).reshape(num_rows, kv_heads * HEAD)
    paired = jnp.concatenate([key_n, value_rows], axis=1)
    before = passed_along(paired[num_rows - WINDOW :], SP, 1)
    current = paired.reshape(blocks, WINDOW, 2 * kv_heads * HEAD)
    previous = jnp.concatenate([before[None], current[:-1]], axis=0)
    key_band = jnp.concatenate([previous, current], axis=1).reshape(
        blocks, 2 * WINDOW, 2, kv_heads, HEAD
    )
    scores = jnp.einsum(
        "nqkgd,nskd->nkgqs", query_n, key_band[:, :, 0], preferred_element_type=jnp.float32
    ) * (1.0 / math.sqrt(HEAD))
    offset = lax.axis_index(SP) * num_rows
    lag_table = (
        lax.broadcasted_iota(jnp.int32, (WINDOW, 2 * WINDOW), 0)
        + WINDOW
        - lax.broadcasted_iota(jnp.int32, (WINDOW, 2 * WINDOW), 1)
    )
    key_place = (
        offset
        + (lax.broadcasted_iota(jnp.int32, (blocks, 2 * WINDOW), 0) - 1) * WINDOW
        + lax.broadcasted_iota(jnp.int32, (blocks, 2 * WINDOW), 1)
    )
    allowed = ((lag_table >= 0) & (lag_table < WINDOW))[None, :, :] & (key_place >= 0)[:, None, :]
    allowed = allowed[:, None, None]
    sink_cols = sink_logit.reshape(kv_heads, group_size)[None, :, :, None, None]
    masked = jnp.where(allowed, scores, -jnp.inf)
    row_top = jnp.maximum(jnp.max(masked, axis=-1, keepdims=True), sink_cols)
    weight = jnp.where(allowed, jnp.exp(masked - row_top), 0.0)
    row_total = jnp.sum(weight, axis=-1, keepdims=True) + jnp.exp(sink_cols - row_top)
    row_lse = (
        (row_top + jnp.log(row_total))[..., 0].transpose(1, 2, 0, 3).reshape(num_heads, num_rows)
    )
    att_probs = (weight / row_total).astype(jnp.bfloat16)
    mixed_heads = jnp.einsum(
        "nkgqs,nskd->nqkgd", att_probs, key_band[:, :, 1], preferred_element_type=jnp.float32
    )
    return (mixed_heads.reshape(num_rows, num_heads * HEAD).astype(jnp.bfloat16), row_lse)


def unit_inverse(lower_mat):
    mat_size = lower_mat.shape[-1]
    result = jnp.eye(mat_size, dtype=jnp.float32) + lower_mat
    power_mat = lower_mat
    for section_index in range(mat_size.bit_length() - 2):
        power_mat = jnp.einsum("hij,hjk->hik", power_mat, power_mat)
        result = result + jnp.einsum("hij,hjk->hik", result, power_mat)
    return result


def pair_table(left_vals, right_vals, allowed):
    return jnp.where(allowed, jnp.einsum("hid,hjd->hij", left_vals, right_vals), 0.0)


def recur(reads, rec_keys, rec_values, log_decay, learn_rate, group_gain):
    num_rows = reads.shape[0]
    num_heads = reads.shape[1] // HEAD
    blocks = num_rows // BLOCK

    def by_block(values):
        return (
            values.astype(jnp.float32).reshape(blocks, BLOCK, num_heads, HEAD).transpose(0, 2, 1, 3)
        )

    read_vals = by_block(reads)
    key_vals = by_block(rec_keys)
    value_vals = by_block(rec_values)
    decay_vals = by_block(log_decay)
    unit_key = key_vals * lax.rsqrt(jnp.sum(key_vals * key_vals, axis=-1, keepdims=True) + KEY_EPS)
    removal = -unit_key
    writing = unit_key * learn_rate.reshape(num_heads, HEAD)[None, :, None, :]
    stacked = jnp.concatenate([jnp.zeros_like(value_vals), value_vals], axis=-1)
    unit_matrix = jnp.broadcast_to(jnp.eye(HEAD, dtype=jnp.float32), (num_heads, HEAD, HEAD))
    start_pair = jnp.concatenate(
        [unit_matrix, jnp.zeros((num_heads, HEAD, HEAD), jnp.float32)], axis=1
    )
    row_iota = lax.broadcasted_iota(jnp.int32, (BLOCK, BLOCK), 0)
    col_iota = lax.broadcasted_iota(jnp.int32, (BLOCK, BLOCK), 1)
    strict = (row_iota > col_iota)[None]
    inclusive = (row_iota >= col_iota)[None]

    def block_step(state_per_block, inputs):
        read_now, key_now, removal_now, writing_now, decay_now, current_value = inputs
        cum_decay = jnp.cumsum(decay_now, axis=1)
        decay_matrix_a = removal_now * jnp.exp(cum_decay - decay_now)
        decay_matrix_b = writing_now * jnp.exp(-cum_decay)
        stacked_key_matrix = key_now * jnp.exp(-cum_decay)
        stacked_receptance = read_now * jnp.exp(cum_decay)
        m_ab = pair_table(decay_matrix_a, decay_matrix_b, strict)
        m_ak = pair_table(decay_matrix_a, stacked_key_matrix, strict)
        m_rb = pair_table(stacked_receptance, decay_matrix_b, inclusive)
        m_rk = pair_table(stacked_receptance, stacked_key_matrix, inclusive)
        right_operand = jnp.einsum("bvq,bzq->bvz", decay_matrix_a, state_per_block) + jnp.einsum(
            "hij,hjm->him", m_ak, current_value
        )
        delta_updates = jnp.einsum("hij,hjm->him", unit_inverse(m_ab), right_operand)
        block_out = (
            jnp.einsum("bvq,bzq->bvz", stacked_receptance, state_per_block)
            + jnp.einsum("hij,hjm->him", m_rb, delta_updates)
            + jnp.einsum("hij,hjm->him", m_rk, current_value)
        )
        grown_state = (
            state_per_block
            + jnp.einsum("sao,sac->soc", delta_updates, decay_matrix_b)
            + jnp.einsum("sao,sac->soc", current_value, stacked_key_matrix)
        )
        return (grown_state * jnp.exp(cum_decay[:, -1])[:, None, :], block_out)

    final_state, block_outs = lax.scan(
        block_step, start_pair, (read_vals, key_vals, removal, writing, decay_vals, stacked)
    )

    def chain(earlier, later_pair):
        moved_state = jnp.einsum("hmk,hkj->hmj", earlier, later_pair[:, :HEAD])
        return moved_state + jnp.concatenate(
            [jnp.zeros_like(later_pair[:, HEAD:]), later_pair[:, HEAD:]], axis=1
        )

    carried = prefix_by_axis(final_state, SP, chain, start_pair)
    incoming = carried[:, HEAD:]
    result = block_outs[..., HEAD:] + jnp.einsum("nhlm,hvm->nhlv", block_outs[..., :HEAD], incoming)
    mean_val = jnp.mean(result, axis=-1, keepdims=True)
    centered = result - mean_val
    variance = jnp.mean(centered * centered, axis=-1, keepdims=True)
    normed = (
        (centered * lax.rsqrt(variance + GROUP_EPS))
        .transpose(0, 2, 1, 3)
        .reshape(num_rows, num_heads * HEAD)
    )
    return (normed * group_gain).astype(jnp.bfloat16)


def per_device(
    tokens,
    norm_gain,
    query_w,
    key_w,
    value_w,
    recept_w,
    rec_key_w,
    rec_value_w,
    decay_down,
    decay_up,
    decay_base,
    learn_rate,
    query_gain,
    key_gain,
    sink_logit,
    group_gain,
    out_att_w,
    out_rec_w,
):
    gathered = collect(tokens, ("fs", "tp"), 1)
    full_rows = gathered.astype(jnp.float32)
    mean_sq = jnp.mean(full_rows * full_rows, axis=1, keepdims=True)
    hidden = (full_rows * lax.rsqrt(mean_sq + NORM_EPS) * norm_gain).astype(jnp.bfloat16)

    def rounded(sums):
        return lax.optimization_barrier(
            tuple((acc_total.astype(jnp.bfloat16) for acc_total in sums))
        )

    rec_span = recept_w.shape[1]
    decay_cols = lax.dynamic_slice_in_dim(
        decay_up, lax.axis_index(("fs", "tp")) * rec_span, rec_span, 1
    )
    decay_low = jnp.tanh(jnp.dot(hidden, decay_down, preferred_element_type=jnp.float32)).astype(
        jnp.bfloat16
    )
    decay_rate = jnp.dot(decay_low, decay_cols, preferred_element_type=jnp.float32) + jnp.repeat(
        decay_base.T, HEAD, axis=1
    )
    log_decay = -jnp.exp(decay_rate)
    pieces = sent_together((query_w, key_w, value_w, recept_w, rec_key_w, rec_value_w), SP, 0, 1)
    all_sums = tuple(
        (
            jnp.dot(hidden, weight_piece, preferred_element_type=jnp.float32)
            for weight_piece in pieces
        )
    )
    att_inputs = rounded(all_sums[:3])
    att_mix, row_lse = attend(
        att_inputs[0], att_inputs[1], att_inputs[2], query_gain, key_gain, sink_logit
    )
    rec_sums = all_sums[3:]
    rec_inputs = rounded(rec_sums)
    rec_mix = recur(rec_inputs[0], rec_inputs[1], rec_inputs[2], log_decay, learn_rate, group_gain)
    att_full, rec_full = turned_gather((out_att_w, out_rec_w), SP, (1, 1))
    mixed_out = summed_on_arrival(
        (
            jnp.dot(att_mix, att_full, preferred_element_type=jnp.float32)
            + jnp.dot(rec_mix, rec_full, preferred_element_type=jnp.float32)
        ).astype(jnp.bfloat16),
        ("fs", "tp"),
        0,
    )
    return (mixed_out.astype(jnp.bfloat16), row_lse)


def solution(mesh):
    split = Mesh(
        mesh.devices.reshape(8, 8, mesh.shape["fs"], mesh.shape["tp"]), ("sp_0", "sp_1", "fs", "tp")
    )
    in_specs = (
        P(SP, ("fs", "tp")),
        P(),
        P(SP, ("fs", "tp")),
        P(SP, ("fs", "tp")),
        P(SP, ("fs", "tp")),
        P(SP, ("fs", "tp")),
        P(SP, ("fs", "tp")),
        P(SP, ("fs", "tp")),
        P(),
        P(),
        P(("fs", "tp"), SP),
        P(("fs", "tp")),
        P(),
        P(),
        P(("fs", "tp")),
        P(("fs", "tp")),
        P(("fs", "tp"), SP),
        P(("fs", "tp"), SP),
    )
    out_specs = (P(SP_FS_TP, None), P(("fs", "tp"), SP))
    return jax.shard_map(
        per_device, mesh=split, in_specs=in_specs, out_specs=out_specs, check_vma=False
    )
```

profile of v0, /device:TPU:1, one launch (start us, length us, event | category | flops | bytes accessed | tf_op | source)
XLA Modules:
  0.0 228.8 jit_solution(15124077085833047071)
XLA Ops:
  7.3 1.5 concatenate.113
  8.8 1.0 copy.55
  9.8 1.0 broadcast_in_dim.97
  10.9 10.3 %all-to-all-start = ((bf16[8,256,256]{1,2,0:T(8,128)(2,1)}), bf16[8,256,256]{1,2,0:T(8,128)(2,1)S(1)}, u32[]{:S(2)}, u32[]{:S(2)}) async-start(bf16[8,256,256]{1,2,0:T(8,128)(2,1)} %broadcast_in_dim.97), calls=%async_computation | async-start | bytes 2097152 | tf_op jit(solution)/shard_map/all_to_all | solution.py:48
  21.2 0.6 pad_maximum_fusion.1
  22.5 13.7 %all-to-all-done = bf16[8,256,256]{1,2,0:T(8,128)(2,1)S(1)} async-done(((bf16[8,256,256]{1,2,0:T(8,128)(2,1)}), bf16[8,256,256]{1,2,0:T(8,128)(2,1)S(1)}, u32[]{:S(2)}, u32[]{:S(2)}) %all-to-all-start) | async-done | bytes 1048608 | tf_op jit(solution)/shard_map/all_to_all | solution.py:48
  36.2 0.3 multiply_reduce_fusion
  36.5 0.3 fusion.33
  36.8 1.3 fusion.38
  38.3 59.2 %all-gather.5.cloned.1.call-done = bf16[2048,640]{1,0:T(8,128)(2,1)} async-done(((bf16[32,640]{1,0:T(8,128)(2,1)}), bf16[2048,640]{1,0:T(8,128)(2,1)}) %all-gather.5.cloned.1.call-update) | async-done | bytes 2621456 | tf_op jit(solution)/shard_map/all_gather | solution.py:68
  97.5 1.5 convolution_convert_fusion
  99.0 1.5 convolution_convert_fusion.1
  100.6 1.5 convolution_convert_fusion.2
  103.2 27.6 %while.14 = (s32[]{:T(128)}, f32[2,128,64]{1,2,0:T(8,128)S(1)}, f32[8,2,32,128]{3,2,0,1:T(8,128)}, f32[8,2,32,64]{3,2,1,0:T(8,128)S(1)}, f32[8,2,32,64]{3,2,1,0:...) while((s32[]{:T(128)}, f32[2,128,64]{1,2,0:T(8,128)S(1)}, ...), condition=%wide.region_8.9_spmd.clone.clone, body=%wide.region_6.8_spmd.clone.clone.sunk | while | flops 8679426 | bytes 1357433 | solution.py:219
  104.4 0.3 convolution_add_fusion.33
  104.7 0.2 fusion.287
  105.0 0.2 convolution_add_fusion.38
  105.3 0.9 fusion.291
  107.9 0.3 convolution_add_fusion.33
  108.1 0.2 fusion.287
  108.5 0.2 convolution_add_fusion.38
  108.7 0.9 fusion.291
  111.3 0.3 convolution_add_fusion.33
  111.5 0.2 fusion.287
  111.9 0.2 convolution_add_fusion.38
  112.2 0.9 fusion.291
  114.7 0.3 convolution_add_fusion.33
  115.0 0.2 fusion.287
  115.4 0.2 convolution_add_fusion.38
  115.6 0.9 fusion.291
  118.2 0.3 convolution_add_fusion.33
  118.4 0.2 fusion.287
  118.8 0.2 convolution_add_fusion.38
  119.1 0.9 fusion.291
  121.6 0.3 convolution_add_fusion.33
  121.9 0.2 fusion.287
  122.3 0.2 convolution_add_fusion.38
  122.5 0.9 fusion.291
  125.1 0.3 convolution_add_fusion.33
  125.3 0.2 fusion.287
  125.7 0.2 convolution_add_fusion.38
  126.0 0.9 fusion.291
  128.5 0.3 convolution_add_fusion.33
  128.8 0.2 fusion.287
  129.2 0.2 convolution_add_fusion.38
  129.4 0.9 fusion.291
  130.5 0.2 fusion.288
  130.7 19.7 %all-gather = bf16[16,128,64]{1,2,0:T(8,128)(2,1)S(1)} all-gather(bf16[2,128,64]{1,2,0:T(8,128)(2,1)S(1)} %convert_element_type.134), channel_id=2, replica_groups=mesh['sp_0'=8,'sp_1'=8,'fs'=4,'tp'=2] {'sp_1'}, dimensions={0}, use_global_device_ids=true | all-gather | bytes 294912 | tf_op jit(solution)/shard_map/all_gather | solution.py:36
  151.7 19.2 %all-gather.1 = bf16[16,128,64]{1,2,0:T(8,128)(2,1)S(1)} all-gather(bf16[2,128,64]{1,2,0:T(8,128)(2,1)S(1)} %convolution_add_fusion.19), channel_id=3, replica_groups=mesh['sp_0'=8,'sp_1'=8,'fs'=4,'tp'=2] {'sp_0'}, dimensions={0}, use_global_device_ids=true | all-gather | bytes 294912 | tf_op jit(solution)/shard_map/all_gather | solution.py:36
  172.2 0.3 fusion.41
  172.5 0.4 fusion.140
  172.9 1.5 convolution_convert_fusion.3
  174.4 1.6 convolution_convert_fusion.5
  176.1 1.4 convolution_convert_fusion.6
  177.6 2.4 %collective-permute-start = (bf16[128,128]{0,1:T(8,128)(2,1)S(1)}, bf16[128,128]{0,1:T(8,128)(2,1)S(1)}, u32[]{:S(2)}, u32[]{:S(2)}) collective-permute-start(bf16[128,128]{0,1:T(8,128)(2,1)S(1)} %get-tuple-element.169), channel_id=1, source_target_pairs={{0,8},{8,16},{16,24},{24,32},{32,40},{40,48},{48,56},{56,64},{64,7... | collective-permute-start | bytes 98312 | tf_op jit(solution)/shard_map/ppermute | solution.py:24
  180.2 0.3 multiply_reduce_fusion.1
  181.5 0.3 fusion.139
  182.1 0.3 fusion.39
  182.4 1.6 fusion.47
  184.1 1.4 fusion.31
  185.5 20.7 %all-to-all-start.1 = ((bf16[8,32,2048]{2,1,0:T(8,128)(2,1)}), bf16[8,32,2048]{2,1,0:T(8,128)(2,1)S(1)}, u32[]{:S(2)}, u32[]{:S(2)}) async-start(bf16[8,32,2048]{2,1,0:T(8,128)(2,1)} %bitcast.29), calls=%async_computation.1 | async-start | bytes 2097152 | tf_op jit(solution)/shard_map/all_to_all | solution.py:93
  206.2 0.7 fusion.128
  206.8 14.3 %all-to-all-done.1 = bf16[8,32,2048]{2,1,0:T(8,128)(2,1)S(1)} async-done(((bf16[8,32,2048]{2,1,0:T(8,128)(2,1)}), bf16[8,32,2048]{2,1,0:T(8,128)(2,1)S(1)}, u32[]{:S(2)}, u32[]{:S(2)}) %all-to-all-start.1) | async-done | bytes 1048608 | tf_op jit(solution)/shard_map/all_to_all | solution.py:93
  221.1 0.8 reduce_sum.84
  (248 shorter events, 20.0 us)
Async XLA Ops:
  7.2 29.7 %copy-start = (bf16[2048,64]{0,1:T(8,128)(2,1)S(1)}, bf16[2048,64]{0,1:T(8,128)(2,1)}, u32[]{:S(2)}) copy-start(bf16[2048,64]{0,1:T(8,128)(2,1)} %param.28) | copy-start | bytes 786436
  7.2 14.0 %copy-start.5 = (bf16[128,32]{0,1:T(8,128)(2,1)S(1)}, bf16[128,32]{0,1:T(8,128)(2,1)}, u32[]{:S(2)}) copy-start(bf16[128,32]{0,1:T(8,128)(2,1)} %param.36) | copy-start | bytes 24580
  7.2 14.0 %copy-start.4 = (bf16[128,32]{0,1:T(8,128)(2,1)S(1)}, bf16[128,32]{0,1:T(8,128)(2,1)}, u32[]{:S(2)}) copy-start(bf16[128,32]{0,1:T(8,128)(2,1)} %param.37) | copy-start | bytes 24580
  7.2 14.8 %copy-start.11 = (f32[128]{0:T(128)S(1)}, f32[128]{0:T(128)}, u32[]{:S(2)}) copy-start(f32[128]{0:T(128)} %param.31) | copy-start | bytes 1540
  7.2 14.9 %copy-start.7 = (f32[2,256]{1,0:T(2,128)S(1)}, f32[2,256]{1,0:T(2,128)}, u32[]{:S(2)}) copy-start(f32[2,256]{1,0:T(2,128)} %param.30) | copy-start | bytes 6148
  7.2 90.3 %all-gather.5.cloned.1.call-start = ((), (), s32[]{:S(2)}) async-start(), calls=%async_computation.2 | async-start | bytes 2662400 | tf_op jit(solution)/shard_map/all_gather | solution.py:68
  9.8 26.7 %copy-start.3 = (f32[2048]{0:T(1024)S(1)}, f32[2048]{0:T(1024)}, u32[]{:S(2)}) copy-start(f32[2048]{0:T(1024)} %param.21) | copy-start | bytes 24580
  10.9 25.3 %all-to-all-start = ((bf16[8,256,256]{1,2,0:T(8,128)(2,1)}), bf16[8,256,256]{1,2,0:T(8,128)(2,1)S(1)}, u32[]{:S(2)}, u32[]{:S(2)}) async-start(bf16[8,256,256]{1,2,0:T(8,128)(2,1)} %broadcast_in_dim.97), calls=%async_computation | async-start | bytes 2097152 | tf_op jit(solution)/shard_map/all_to_all | solution.py:48
  21.2 161.3 %all-gather.7.cloned.1.call-start = ((), (), s32[]{:S(2)}) async-start(), calls=%async_computation.3 | async-start | bytes 1064960 | tf_op jit(solution)/shard_map/all_gather | solution.py:75
  130.7 41.8 %copy-start.2 = (f32[8,2,32,128]{3,2,0,1:T(8,128)S(1)}, f32[8,2,32,128]{3,2,0,1:T(8,128)}, u32[]{:S(2)}) copy-start(f32[8,2,32,128]{3,2,0,1:T(8,128)} %get-tuple-element.78) | copy-start | bytes 786436
  172.9 4.7 %copy-start.8 = (f32[64]{0:T(128)S(1)}, f32[64]{0:T(128)}, u32[]{:S(2)}) copy-start(f32[64]{0:T(128)} %param.33) | copy-start | bytes 772
  174.4 6.2 %copy-start.9 = (f32[64]{0:T(128)S(1)}, f32[64]{0:T(128)}, u32[]{:S(2)}) copy-start(f32[64]{0:T(128)} %param.32) | copy-start | bytes 772
  176.1 5.7 %copy-start.6 = (f32[2]{0:T(128)S(1)}, f32[2]{0:T(128)}, u32[]{:S(2)}) copy-start(f32[2]{0:T(128)} %param.34) | copy-start | bytes 28
  177.6 3.8 %collective-permute-start = (bf16[128,128]{0,1:T(8,128)(2,1)S(1)}, bf16[128,128]{0,1:T(8,128)(2,1)S(1)}, u32[]{:S(2)}, u32[]{:S(2)}) collective-permute-start(bf16[128,128]{0,1:T(8,128)(2,1)S(1)} %get-tuple-element.169), channel_id=1, source_target_pairs={{0,8},{8,16},{16,24},{24,32},{32,40},{40,48},{48,56},{56,64},{64,7... | collective-permute-start | bytes 98312 | tf_op jit(solution)/shard_map/ppermute | solution.py:24
  182.1 2.0 copy-start.10
  182.4 1.6 copy-start.1
  185.5 35.7 %all-to-all-start.1 = ((bf16[8,32,2048]{2,1,0:T(8,128)(2,1)}), bf16[8,32,2048]{2,1,0:T(8,128)(2,1)S(1)}, u32[]{:S(2)}, u32[]{:S(2)}) async-start(bf16[8,32,2048]{2,1,0:T(8,128)(2,1)} %bitcast.29), calls=%async_computation.1 | async-start | bytes 2097152 | tf_op jit(solution)/shard_map/all_to_all | solution.py:93
Sparse Core Ops, SparseCore 0:
  11.6 85.8 all-gather.4
  100.6 78.9 all-gather.6
where the time goes:
time: 230 us; the launch traced here: 229 us
  waiting for transfers between devices  87.3 us (38%)
  matrix products  42.8 us (19%)
  blocking collectives  38.9 us (17%)
  starting transfers between devices  33.4 us (15%)
  between operations  14.7 us (6%)
  local copies, waits for them, and re-layouts  5.91 us (3%)
  other arithmetic  5.28 us (2%)
    all_gather x1, waiting for transfers between devices, sent_together(): lax.all_gather(both, axis, axis=dim, tiled=True)  59.2 us
    all_gather x2, blocking collectives, prefix_by_axis(): pieces = lax.all_gather(total.astype(jnp.bfloat16), axis)  38.9 us
    all_to_all x1, starting transfers between devices, summed_on_arrival(): lax.all_to_all(in_blocks(array, dim, devices), axis, 0, 0, tiled=True)  20.7 us
    all_to_all x1, waiting for transfers between devices, summed_on_arrival(): lax.all_to_all(in_blocks(array, dim, devices), axis, 0, 0, tiled=True)  14.3 us
    all_to_all x1, waiting for transfers between devices, from_everyone(): return lax.all_to_all(copies, axis, split_axis=0, concat_axis=0, tiled=True)  13.7 us
    all_to_all x1, starting transfers between devices, from_everyone(): return lax.all_to_all(copies, axis, split_axis=0, concat_axis=0, tiled=True)  10.3 us
    dot_general x6, matrix products, per_device(): jnp.dot(hidden, weight_piece, preferred_element_type=jnp.float32)  9.11 us
    dot_general x8, matrix products, block_step(): jnp.einsum('hij,hjm->him', m_rk, current_value)  7.01 us
  transfers between devices with their start and end apart: 5, of which 3 were waited for; matrix products, arithmetic and copies ran while one was open for 21% of the time, Pallas kernels for 0%

commit v1 on v0

v1 whole, which is shorter than its diff:
```python
import functools
import math

import jax
import jax.numpy as jnp
from jax import lax
from jax.experimental import pallas as pl
from jax.experimental.pallas import tpu as pltpu
from jax.sharding import Mesh
from jax.sharding import PartitionSpec as P

HEAD = 64
WINDOW = 128
CHUNK = 32
SP = ("sp_0", "sp_1")
SP_FS_TP = ("sp_0", "sp_1", "fs", "tp")
F32 = jnp.float32
BF16 = jnp.bfloat16

NORM_EPS = 1e-06
KEY_EPS = 1e-06
GROUP_EPS = 0.00064
DECAY_FLOOR = -104.0

NT = (((1,), (1,)), ((), ()))
TN = (((0,), (0,)), ((), ()))


def ring_shift(array, axis, by):
    devices = lax.axis_size(axis)
    return lax.ppermute(array, axis, [(i, (i + by) % devices) for i in range(devices)])


def passed_along(array, axis, by):
    devices = lax.axis_size(axis)
    pairs = [(i, i + by) for i in range(devices) if 0 <= i + by < devices]
    return lax.ppermute(array, axis, pairs)


def from_everyone(array, axis):
    copies = jnp.broadcast_to(array, (lax.axis_size(axis), *array.shape))
    return lax.all_to_all(copies, axis, split_axis=0, concat_axis=0, tiled=True)


def call(kernel, outs, scratch=(), flops=0, smem=0, name=None):
    def run(*args):
        specs = [
            pl.BlockSpec(memory_space=pltpu.SMEM if i < smem else pltpu.VMEM)
            for i in range(len(args))
        ]
        return pl.pallas_call(
            kernel,
            out_shape=[jax.ShapeDtypeStruct(s, d) for s, d in outs],
            in_specs=specs,
            out_specs=[pl.BlockSpec(memory_space=pltpu.VMEM)] * len(outs),
            scratch_shapes=list(scratch),
            cost_estimate=pl.CostEstimate(flops=flops, bytes_accessed=1 << 21, transcendentals=0),
            compiler_params=pltpu.CompilerParams(vmem_limit_bytes=40 << 20),
            name=name,
        )(*args)

    return run


def dot(a, b, dims=(((1,), (0,)), ((), ()))):
    return lax.dot_general(a.astype(BF16), b.astype(BF16), dims, preferred_element_type=F32)


def hidden_kernel(place, own, next_, before, across, other, gain, down, up, base, hid, ld, cum, rest):
    x = place[0]
    core = place[1]
    rows = own.shape[0]
    blocks = [own, before, across, next_]
    sums = jnp.zeros((rows, 1), F32)
    for k in range(4):
        mine = blocks[k][...].astype(F32)
        theirs = other[k].astype(F32)
        sums += jnp.sum(mine * mine + theirs * theirs, axis=1, keepdims=True)
    width = own.shape[1]
    scale = lax.rsqrt(sums / (8 * width) + NORM_EPS)
    low = jnp.zeros((rows, down.shape[1]), F32)
    for k in range(4):
        chip = lax.rem(x + k, 4)
        for c, block in ((core, blocks[k][...]), (1 - core, other[k])):
            at = pl.multiple_of((chip * 2 + c) * width, width)
            h = (block.astype(F32) * scale * gain[:, pl.ds(at, width)]).astype(BF16)
            hid[:, pl.ds(at, width)] = h
            low += jnp.dot(h, down[pl.ds(at, width), :], preferred_element_type=F32)
    low = jnp.tanh(low).astype(BF16)
    rate = lax.dot_general(up[...], low, (((0,), (1,)), ((), ())), preferred_element_type=F32)
    heads = base.shape[0]
    base_rows = jnp.concatenate(
        [jnp.broadcast_to(base[h : h + 1, :], (HEAD, rows)) for h in range(heads)], axis=0
    )
    log_decay = jnp.maximum(-jnp.exp(rate + base_rows), DECAY_FLOOR)
    ld[...] = log_decay
    lane = lax.broadcasted_iota(jnp.int32, log_decay.shape, 1) % CHUNK
    total, after = log_decay, log_decay
    step = 1
    while step < CHUNK:
        total = total + jnp.where(lane >= step, pltpu.roll(total, step, 1), 0.0)
        after = after + jnp.where(lane < CHUNK - step, pltpu.roll(after, rows - step, 1), 0.0)
        step *= 2
    cum[...] = total
    rest[...] = after - log_decay


def head_rows(h):
    return slice(h * HEAD, (h + 1) * HEAD)


def band_tables(left, right, start, end, rate, first, heads):
    rows = left.shape[1]
    dist = (
        lax.broadcasted_iota(jnp.int32, (CHUNK, rows), 1) % CHUNK
        - lax.broadcasted_iota(jnp.int32, (CHUNK, rows), 0)
    )
    plain, rated = [], []
    for h in range(heads):
        sl = head_rows(h)
        l, r, s, e = left[sl, :], right[sl, :], start[sl, :], end[sl, :]
        speed = jnp.broadcast_to(rate[sl, :], l.shape)
        t_plain = jnp.zeros((CHUNK, rows), F32)
        t_rated = jnp.zeros((CHUNK, rows), F32)
        for d in range(first, CHUNK):
            rd = r if d == 0 else pltpu.roll(r, d, 1)
            ed = e if d == 0 else pltpu.roll(e, d, 1)
            x = l * rd * jnp.exp(s - ed)
            here = dist == d
            t_plain = jnp.where(here, jnp.sum(x, axis=0, keepdims=True), t_plain)
            t_rated = jnp.where(here, jnp.sum(x * speed, axis=0, keepdims=True), t_rated)
        plain.append(t_plain)
        rated.append(t_rated)
    return plain, rated


def in_chunks(table):
    rows = table.shape[1]
    tall = jnp.concatenate([table] * (rows // CHUNK), axis=0)
    same = (
        lax.broadcasted_iota(jnp.int32, (rows, rows), 0) // CHUNK
        == lax.broadcasted_iota(jnp.int32, (rows, rows), 1) // CHUNK
    )
    return jnp.where(same, tall, 0.0).astype(BF16)


def by_chunk(array):
    rows = array.shape[1]
    chunk = lax.broadcasted_iota(jnp.int32, array.shape, 1) // CHUNK
    return jnp.concatenate(
        [jnp.where(chunk == c, array, 0.0).astype(BF16) for c in range(rows // CHUNK)], axis=0
    )


def state_kernel(hid, w, lr, ld, cum, rest, ends, unit, value, solved, starts, dec):
    rows = hid.shape[0]
    heads = lr.shape[0] // HEAD
    span = heads * HEAD
    kv = jnp.dot(hid[...], w[...], preferred_element_type=F32).astype(BF16).astype(F32)
    kv_t = kv.T
    for h in range(heads):
        k = kv_t[head_rows(h), :]
        square = jnp.sum(k * k, axis=0, keepdims=True) + KEY_EPS
        inv = lax.rsqrt(square)
        unit[head_rows(h), :] = k * inv
        value[head_rows(h), :] = kv_t[span + h * HEAD : span + (h + 1) * HEAD, :] * (square * inv)
    cum_all = cum[...]
    prev = cum_all - ld[...]
    dec[...] = jnp.exp(cum_all).T
    u = unit[...]
    v = value[...]
    plain, rated = band_tables(u, u, prev, cum_all, lr, 1, heads)
    reach = jnp.exp(prev)
    x, q = [], []
    for h in range(heads):
        sl = head_rows(h)
        x.append(jnp.concatenate([-u[sl, :] * reach[sl, :], -dot(v[sl, :], in_chunks(plain[h]))], axis=0))
        q.append(in_chunks(-rated[h]))
    power = 1
    while power < CHUNK:
        for h in range(heads):
            x[h] = x[h] + dot(x[h], q[h])
        power *= 2
        if power < CHUNK:
            for h in range(heads):
                q[h] = dot(q[h], q[h]).astype(BF16)
    left = jnp.exp(rest[...])
    chunks = rows // CHUNK
    grow = []
    for h in range(heads):
        sl = head_rows(h)
        solved[h] = x[h].astype(BF16)
        out_u = u[sl, :] * left[sl, :]
        out_b = out_u * lr[sl, :]
        g = dot(x[h], by_chunk(out_b), NT)
        g_low = g[HEAD:, :] + dot(v[sl, :], by_chunk(out_u), NT)
        grow.append((g[:HEAD, :].astype(BF16), g_low))
    eye = (
        lax.broadcasted_iota(jnp.int32, (2 * HEAD, HEAD), 0)
        == lax.broadcasted_iota(jnp.int32, (2 * HEAD, HEAD), 1)
    ).astype(F32)
    state = [eye] * heads
    zero = jnp.zeros((HEAD, HEAD), F32)
    for c in range(chunks):
        at = slice(c * HEAD, (c + 1) * HEAD)
        last = c * CHUNK + CHUNK - 1
        for h in range(heads):
            low = state[h].astype(BF16)
            starts[h, :, at] = low
            kept = state[h] * dec[last : last + 1, head_rows(h)]
            added = jnp.concatenate([zero, grow[h][1][:, at]], axis=0)
            state[h] = kept + added + jnp.dot(low, grow[h][0][:, at], preferred_element_type=F32)
    for h in range(heads):
        ends[h] = state[h].astype(BF16)


def read_kernel(hid, w, lr, cum, unit, value, solved, starts, out):
    rows = hid.shape[0]
    heads = lr.shape[0] // HEAD
    reads = jnp.dot(hid[...], w[...], preferred_element_type=F32).astype(BF16).astype(F32)
    r = reads.T
    cum_all = cum[...]
    plain, rated = band_tables(r, unit[...], cum_all, cum_all, lr, 0, heads)
    reach = r * jnp.exp(cum_all)
    for h in range(heads):
        sl = head_rows(h)
        mixed = dot(solved[h], in_chunks(rated[h]))
        query = mixed[:HEAD, :] + reach[sl, :]
        local = mixed[HEAD:, :] + dot(value[sl, :], in_chunks(plain[h]))
        both = dot(starts[h], by_chunk(query))
        out[h, :HEAD, :] = both[:HEAD, :]
        out[h, HEAD:, :] = both[HEAD:, :] + local


def chain(earlier, later):
    moved = jnp.dot(earlier.astype(BF16), later[:HEAD, :], preferred_element_type=F32)
    return moved + jnp.concatenate([jnp.zeros((HEAD, HEAD), F32), later[HEAD:, :].astype(F32)], axis=0)


def row_kernel(place, pieces, total_out, inside_out):
    devices, heads = pieces.shape[0], pieces.shape[1]
    eye = (
        lax.broadcasted_iota(jnp.int32, (2 * HEAD, HEAD), 0)
        == lax.broadcasted_iota(jnp.int32, (2 * HEAD, HEAD), 1)
    ).astype(F32)
    total = [eye] * heads
    inside = [eye] * heads
    for k in range(devices):
        passed = k < place[0]
        for h in range(heads):
            later = pieces[k, h]
            total[h] = later.astype(F32) if k == 0 else chain(total[h], later)
            inside[h] = jnp.where(passed, total[h], inside[h])
    for h in range(heads):
        total_out[h] = total[h].astype(BF16)
        inside_out[h] = inside[h].astype(BF16)


def final_kernel(place, pieces, inside, local, gain, att, w, out):
    devices, heads = pieces.shape[0], pieces.shape[1]
    state = [jnp.zeros((HEAD, HEAD), F32)] * heads
    for k in range(devices - 1):
        passed = k < place[0]
        for h in range(heads):
            new = jnp.dot(state[h].astype(BF16), pieces[k, h, :HEAD, :], preferred_element_type=F32)
            new = new + pieces[k, h, HEAD:, :].astype(F32)
            state[h] = jnp.where(passed, new, state[h])
    rows = []
    for h in range(heads):
        start = jnp.dot(state[h].astype(BF16), inside[h, :HEAD, :], preferred_element_type=F32)
        start = start + inside[h, HEAD:, :].astype(F32)
        y = dot(start, local[h, :HEAD, :]) + local[h, HEAD:, :]
        centered = y - jnp.mean(y, axis=0, keepdims=True)
        variance = jnp.mean(centered * centered, axis=0, keepdims=True)
        rows.append(centered * lax.rsqrt(variance + GROUP_EPS) * gain[head_rows(h), :])
    rec = jnp.concatenate(rows, axis=0).T.astype(BF16)
    mix = jnp.concatenate([att[...], rec], axis=1)
    groups, width = out.shape[0], 512
    size = out.shape[1]
    for n in range(w.shape[0] // width):
        at = slice(n * width, (n + 1) * width)
        part = lax.dot_general(mix, w[at, :], NT, preferred_element_type=F32).astype(BF16)
        for g in range(groups):
            out[g, :, at] = part[g * size : (g + 1) * size, :]


def head_rms(values, gain_vec, num_heads):
    shaped = values.astype(jnp.float32).reshape(values.shape[0], num_heads, HEAD)
    mean_sq = jnp.mean(shaped * shaped, axis=-1, keepdims=True)
    return (shaped * lax.rsqrt(mean_sq + NORM_EPS) * gain_vec).astype(jnp.bfloat16)


def attend(query_rows, key_rows, value_rows, query_gain, key_gain, sink_logit):
    num_rows = query_rows.shape[0]
    num_heads = query_rows.shape[1] // HEAD
    kv_heads = key_rows.shape[1] // HEAD
    group_size = num_heads // kv_heads
    blocks = num_rows // WINDOW
    query_n = head_rms(query_rows, query_gain, num_heads).reshape(
        blocks, WINDOW, kv_heads, group_size, HEAD
    )
    key_n = head_rms(key_rows, key_gain, kv_heads).reshape(num_rows, kv_heads * HEAD)
    paired = jnp.concatenate([key_n, value_rows], axis=1)
    before = passed_along(paired[num_rows - WINDOW :], SP, 1)
    current = paired.reshape(blocks, WINDOW, 2 * kv_heads * HEAD)
    previous = jnp.concatenate([before[None], current[:-1]], axis=0)
    key_band = jnp.concatenate([previous, current], axis=1).reshape(
        blocks, 2 * WINDOW, 2, kv_heads, HEAD
    )
    scores = jnp.einsum(
        "nqkgd,nskd->nkgqs", query_n, key_band[:, :, 0], preferred_element_type=jnp.float32
    ) * (1.0 / math.sqrt(HEAD))
    offset = lax.axis_index(SP) * num_rows
    lag_table = (
        lax.broadcasted_iota(jnp.int32, (WINDOW, 2 * WINDOW), 0)
        + WINDOW
        - lax.broadcasted_iota(jnp.int32, (WINDOW, 2 * WINDOW), 1)
    )
    key_place = (
        offset
        + (lax.broadcasted_iota(jnp.int32, (blocks, 2 * WINDOW), 0) - 1) * WINDOW
        + lax.broadcasted_iota(jnp.int32, (blocks, 2 * WINDOW), 1)
    )
    allowed = ((lag_table >= 0) & (lag_table < WINDOW))[None, :, :] & (key_place >= 0)[:, None, :]
    allowed = allowed[:, None, None]
    sink_cols = sink_logit.reshape(kv_heads, group_size)[None, :, :, None, None]
    masked = jnp.where(allowed, scores, -jnp.inf)
    row_top = jnp.maximum(jnp.max(masked, axis=-1, keepdims=True), sink_cols)
    weight = jnp.where(allowed, jnp.exp(masked - row_top), 0.0)
    row_total = jnp.sum(weight, axis=-1, keepdims=True) + jnp.exp(sink_cols - row_top)
    row_lse = (
        (row_top + jnp.log(row_total))[..., 0].transpose(1, 2, 0, 3).reshape(num_heads, num_rows)
    )
    att_probs = (weight / row_total).astype(jnp.bfloat16)
    mixed_heads = jnp.einsum(
        "nkgqs,nskd->nqkgd", att_probs, key_band[:, :, 1], preferred_element_type=jnp.float32
    )
    return (mixed_heads.reshape(num_rows, num_heads * HEAD).astype(jnp.bfloat16), row_lse)


def per_device(
    tokens,
    norm_gain,
    query_w,
    key_w,
    value_w,
    recept_w,
    rec_key_w,
    rec_value_w,
    decay_down,
    decay_up,
    decay_base,
    learn_rate,
    query_gain,
    key_gain,
    sink_logit,
    group_gain,
    out_att_w,
    out_rec_w,
):
    rows = tokens.shape[0]
    span = recept_w.shape[1]
    heads = span // HEAD
    features = norm_gain.shape[0]
    groups = lax.axis_size(("fs", "tp"))
    place_zy = [lax.axis_index(a).astype(jnp.int32).reshape(1) for a in SP]

    own = jnp.concatenate(
        [rec_key_w, rec_value_w, recept_w, query_w, key_w, value_w, out_att_w.T, out_rec_w.T], axis=1
    )
    column = from_everyone(own, "sp_1").reshape(-1, own.shape[1])
    state_w = from_everyone(column[:, : 2 * span], "sp_0").reshape(features, 2 * span)
    other_w = lax.all_gather(column[:, 2 * span :], "sp_0", axis=0, tiled=True)

    before = ring_shift(tokens, "fs", -1)
    across = ring_shift(tokens, "fs", 2)
    next_ = ring_shift(tokens, "fs", 1)
    other = ring_shift(jnp.stack([tokens, before, across, next_]), "tp", 1)

    place_xc = jnp.stack([lax.axis_index("fs"), lax.axis_index("tp")]).astype(jnp.int32)
    decay_cols = lax.dynamic_slice_in_dim(
        decay_up, lax.axis_index(("fs", "tp")) * span, span, 1
    )
    flat = (span, rows)
    hid, ld, cum, rest = call(
        hidden_kernel,
        [((rows, features), BF16), (flat, F32), (flat, F32), (flat, F32)],
        smem=1,
        flops=1 << 27,
        name="hidden",
    )(
        place_xc, tokens, next_, before, across, other, norm_gain.reshape(1, -1), decay_down, decay_cols, decay_base
    )

    lr = learn_rate.reshape(span, 1)
    chunks = rows // CHUNK
    ends, unit, value, solved, starts = call(
        state_kernel,
        [
            ((heads, 2 * HEAD, HEAD), BF16),
            (flat, F32),
            (flat, F32),
            ((heads, 2 * HEAD, rows), BF16),
            ((heads, 2 * HEAD, chunks * HEAD), BF16),
        ],
        scratch=[pltpu.VMEM((rows, span), F32)],
        flops=1 << 31,
        name="state",
    )(hid, state_w, lr, ld, cum, rest)

    row_pieces = from_everyone(ends, "sp_1")
    row_total, inside = call(
        row_kernel,
        [((heads, 2 * HEAD, HEAD), BF16)] * 2,
        smem=1,
        flops=1 << 27,
        name="rowchain",
    )(place_zy[1], row_pieces)
    all_pieces = from_everyone(row_total, "sp_0")

    (local,) = call(
        read_kernel, [((heads, 2 * HEAD, rows), F32)], flops=1 << 31, name="reads"
    )(hid, other_w[:, :span], lr, cum, unit, value, solved, starts)
    q_w, kv_w = query_w.shape[1], key_w.shape[1]
    att_w = other_w[:, span : span + q_w + 2 * kv_w]
    att_in = lax.optimization_barrier(
        jnp.dot(hid, att_w, preferred_element_type=F32).astype(BF16)
    )
    att_mix, row_lse = attend(
        att_in[:, :q_w], att_in[:, q_w : q_w + kv_w], att_in[:, q_w + kv_w :], query_gain, key_gain, sink_logit
    )
    out_w = other_w[:, span + q_w + 2 * kv_w :]

    (partial,) = call(
        final_kernel,
        [((groups, rows // groups, features), BF16)],
        smem=1,
        flops=1 << 30,
        name="final",
    )(place_zy[0], all_pieces, inside, local, group_gain.reshape(span, 1), att_mix, out_w)
    tiles = lax.all_to_all(partial, ("fs", "tp"), 0, 0, tiled=True)
    mixed = jnp.sum(tiles.astype(F32), axis=0).astype(BF16)
    return (mixed, row_lse)


def solution(mesh):
    split = Mesh(
        mesh.devices.reshape(8, 8, mesh.shape["fs"], mesh.shape["tp"]), ("sp_0", "sp_1", "fs", "tp")
    )
    in_specs = (
        P(SP, ("fs", "tp")),
        P(),
        P(SP, ("fs", "tp")),
        P(SP, ("fs", "tp")),
        P(SP, ("fs", "tp")),
        P(SP, ("fs", "tp")),
        P(SP, ("fs", "tp")),
        P(SP, ("fs", "tp")),
        P(),
        P(),
        P(("fs", "tp"), SP),
        P(("fs", "tp")),
        P(),
        P(),
        P(("fs", "tp")),
        P(("fs", "tp")),
        P(("fs", "tp"), SP),
        P(("fs", "tp"), SP),
    )
    out_specs = (P(SP_FS_TP, None), P(("fs", "tp"), SP))
    return jax.shard_map(
        per_device, mesh=split, in_specs=in_specs, out_specs=out_specs, check_vma=False
    )
```

time: 230 us -> 163 us (0.71)
  matrix products: 42.8 us -> 2.21 us
  waiting for transfers between devices: 87.3 us -> 50.8 us
  blocking collectives: 38.9 us -> 21.7 us
  Pallas kernels: 0 us -> 13.6 us
  starting transfers between devices: 33.4 us -> 44.7 us
  local copies, waits for them, and re-layouts: 5.91 us -> 10.9 us
    all_gather x2 -> x1, waiting for transfers between devices: 59.2 us -> 0.02 us  [per_device(): other_w = lax.all_gather(column[:, 2 * span:], 'sp_0', axis=0, tiled=True)]
    dot_general x155 -> x1, matrix products: 42.2 us -> 1.66 us  [per_device(): jnp.dot(hid, att_w, preferred_element_type=F32).astype(BF16)]
    all_gather x2 -> x0, blocking collectives: 38.9 us -> none  [prefix_by_axis(): pieces = lax.all_gather(total.astype(jnp.bfloat16), axis)]
    all_to_all x0 -> x1, blocking collectives: none -> 21.7 us  [from_everyone(): return lax.all_to_all(copies, axis, split_axis=0, concat_axis=0, tiled=True)]
    all_to_all x1 -> x3, waiting for transfers between devices: 13.7 us -> 31.2 us  [from_everyone(): return lax.all_to_all(copies, axis, split_axis=0, concat_axis=0, tiled=True)]
    ppermute x0 -> x4, starting transfers between devices: none -> 15.8 us  [ring_shift(): lax.ppermute(array, axis, [(i, (i + by) % devices) for i in range(devices)])]
    pallas_call x0 -> x5, Pallas kernels: none -> 13.6 us  [run(): pl.pallas_call(kernel, out_shape=[jax.ShapeDtypeStruct(s, d) for s, d in...]
    all_to_all x1, starting transfers between devices: 20.7 us -> 9.22 us  [per_device(): tiles = lax.all_to_all(partial, ('fs', 'tp'), 0, 0, tiled=True)]
  transfers between devices with their start and end apart: 5 -> 10, of which waited for: 3 -> 6; matrix products, arithmetic and copies ran while one was open for 21% -> 5% of each run, Pallas kernels for 0% -> 7%
where the time goes in v1:
time: 163 us; the launch traced here: 162 us
  waiting for transfers between devices  50.8 us (31%)
  starting transfers between devices  44.7 us (27%)
  blocking collectives  21.7 us (13%)
  between operations  14.5 us (9%)
  Pallas kernels  13.6 us (8%)
  local copies, waits for them, and re-layouts  10.9 us (7%)
  other arithmetic  3.54 us (2%)
  matrix products  2.21 us (1%)
    all_to_all x3, waiting for transfers between devices, from_everyone(): return lax.all_to_all(copies, axis, split_axis=0, concat_axis=0, tiled=True)  31.2 us
    all_to_all x1, blocking collectives, from_everyone(): return lax.all_to_all(copies, axis, split_axis=0, concat_axis=0, tiled=True)  21.7 us
    all_to_all x3, starting transfers between devices, from_everyone(): return lax.all_to_all(copies, axis, split_axis=0, concat_axis=0, tiled=True)  17.6 us
    ppermute x4, starting transfers between devices, ring_shift(): lax.ppermute(array, axis, [(i, (i + by) % devices) for i in range(devices)])  15.8 us
    all_to_all x1, waiting for transfers between devices, per_device(): tiles = lax.all_to_all(partial, ('fs', 'tp'), 0, 0, tiled=True)  14.3 us
    pallas_call x5, Pallas kernels, run(): pl.pallas_call(kernel, out_shape=[jax.ShapeDtypeStruct(s, d) for s, d in...  13.6 us
    all_to_all x1, starting transfers between devices, per_device(): tiles = lax.all_to_all(partial, ('fs', 'tp'), 0, 0, tiled=True)  9.22 us
    ppermute x4, waiting for transfers between devices, ring_shift(): lax.ppermute(array, axis, [(i, (i + by) % devices) for i in range(devices)])  5.26 us
  transfers between devices with their start and end apart: 10, of which 6 were waited for; matrix products, arithmetic and copies ran while one was open for 5% of the time, Pallas kernels for 7%

profile of v1, /device:TPU:1, one launch (start us, length us, event | category | flops | bytes accessed | tf_op | source)
XLA Modules:
  0.0 162.0 jit_solution(14190533687340213219)
XLA Ops:
  7.2 0.0 all-gather.2.cloned.1.call-start
  7.2 0.9 concatenate.19
  8.2 21.7 %all_to_all.25 = bf16[8,32,896]{2,1,0:T(8,128)(2,1)S(1)} all-to-all(bf16[8,32,896]{2,1,0:T(8,128)(2,1)S(1)} %broadcast_in_dim.42), channel_id=1, replica_groups=mesh['sp_0'=8,'sp_1'=8,'fs'=4,'tp'=2] {'sp_1'}, dimensions={0} | all-to-all | bytes 917504 | tf_op jit(solution)/shard_map/all_to_all | solution.py:42
  29.9 0.8 slice.53
  30.6 0.0 all-gather.2.cloned.1.call-update
  30.7 1.0 broadcast_in_dim.43
  31.8 10.8 %all-to-all-start.1 = ((bf16[8,256,256]{2,1,0:T(8,128)(2,1)}), bf16[8,256,256]{2,1,0:T(8,128)(2,1)S(1)}, u32[]{:S(2)}, u32[]{:S(2)}) async-start(bf16[8,256,256]{2,1,0:T(8,128)(2,1)} %broadcast_in_dim.43), calls=%async_computation.1 | async-start | bytes 2097152 | tf_op jit(solution)/shard_map/all_to_all | solution.py:42
  42.5 3.1 %collective-permute-start = (bf16[256,256]{1,0:T(8,128)(2,1)S(1)}, bf16[256,256]{1,0:T(8,128)(2,1)S(1)}, u32[]{:S(2)}, u32[]{:S(2)}) collective-permute-start(bf16[256,256]{1,0:T(8,128)(2,1)S(1)} %copy-done.1), channel_id=1, source_target_pairs={{0,2},{2,4},{4,6},{6,0},{1,3},{3,5},{5,7},{7,1},{8,10},{10,12},{12... | collective-permute-start | bytes 393224 | tf_op jit(solution)/shard_map/ppermute | solution.py:31
  45.6 3.4 %collective-permute-start.1 = (bf16[256,256]{1,0:T(8,128)(2,1)S(1)}, bf16[256,256]{1,0:T(8,128)(2,1)S(1)}, u32[]{:S(2)}, u32[]{:S(2)}) collective-permute-start(bf16[256,256]{1,0:T(8,128)(2,1)S(1)} %copy-done.1), channel_id=1, source_target_pairs={{0,6},{2,0},{4,2},{6,4},{1,7},{3,1},{5,3},{7,5},{8,14},{10,8},{12,... | collective-permute-start | bytes 393224 | tf_op jit(solution)/shard_map/ppermute | solution.py:31
  49.0 3.4 %collective-permute-start.2 = (bf16[256,256]{1,0:T(8,128)(2,1)S(1)}, bf16[256,256]{1,0:T(8,128)(2,1)S(1)}, u32[]{:S(2)}, u32[]{:S(2)}) collective-permute-start(bf16[256,256]{1,0:T(8,128)(2,1)S(1)} %copy-done.1), channel_id=1, source_target_pairs={{0,4},{2,6},{4,0},{6,2},{1,5},{3,7},{5,1},{7,3},{8,12},{10,14},{12... | collective-permute-start | bytes 393224 | tf_op jit(solution)/shard_map/ppermute | solution.py:31
  52.5 4.0 %collective-permute-done.2.across = bf16[256,256]{1,0:T(8,128)(2,1)S(1)} collective-permute-done((bf16[256,256]{1,0:T(8,128)(2,1)S(1)}, bf16[256,256]{1,0:T(8,128)(2,1)S(1)}, u32[]{:S(2)}, u32[]{:S(2)}) %collective-permute-start.2) | collective-permute-done | bytes 131104 | tf_op jit(solution)/shard_map/ppermute | solution.py:31
  56.5 0.9 pad_maximum_fusion
  57.4 5.8 %collective-permute-start.3 = (bf16[4,256,256]{2,1,0:T(8,128)(2,1)}, bf16[4,256,256]{2,1,0:T(8,128)(2,1)S(1)}, u32[]{:S(2)}, u32[]{:S(2)}) collective-permute-start(bf16[4,256,256]{2,1,0:T(8,128)(2,1)} %pad_maximum_fusion), channel_id=1, source_target_pairs={{0,1},{1,0},{2,3},{3,2},{4,5},{5,4},{6,7},{7,6},{8,9},{9,8},{10,11... | collective-permute-start | bytes 1572872 | tf_op jit(solution)/shard_map/ppermute | solution.py:31
  63.2 0.3 copy.45.down
  63.5 0.1 copy.46.lr
  63.7 0.1 pad_add_fusion.place
  63.7 1.2 collective-permute-done.3.other
  65.0 1.9 %hidden.1 = (bf16[256,2048]{1,0:T(8,128)(2,1)S(1)}, f32[128,256]{1,0:T(8,128)S(1)}, f32[128,256]{1,0:T(8,128)S(1)}, f32[128,256]{1,0:T(8,128)S(1)}) custom-call(s32[2]{0:T(128)S(1)} %pad_add_fusion.place, bf16[256,256]{1,0:T(8,128)(2,1)S(1)} %copy-done.1, bf16[256,256]{1,0:T(8,128)(2,1)S(1)} %collective-permute-done.next_, ...), custom_call_target="tpu_custom_call" | custom-call | flops 134217728 | bytes 2097152 | tf_op jit(solution)/shard_map/hidden/pallas_call | solution.py:51
  66.9 0.9 copy-done.4
  67.8 12.8 %all-to-all-done.1 = bf16[8,256,256]{2,1,0:T(8,128)(2,1)S(1)} async-done(((bf16[8,256,256]{2,1,0:T(8,128)(2,1)}), bf16[8,256,256]{2,1,0:T(8,128)(2,1)S(1)}, u32[]{:S(2)}, u32[]{:S(2)}) %all-to-all-start.1) | async-done | bytes 1048608 | tf_op jit(solution)/shard_map/all_to_all | solution.py:42
  80.6 1.2 copy-done.5
  81.8 5.5 %state.1 = (bf16[2,128,64]{2,1,0:T(8,128)(2,1)S(1)}, f32[128,256]{1,0:T(8,128)S(1)}, f32[128,256]{1,0:T(8,128)S(1)}, bf16[2,128,256]{2,1,0:T(8,128)(2,1)S(1)}, bf16[2,128,512]{2,1,0:T(8,128)(2,1)S(1)}) custom-call(bf16[256,2048]{1,0:T(8,128)(2,1)S(1)} %copy-done.5, bf16[2048,256]{1,0:T(8,128)(2,1)S(1)} %bitcast.79, f32[128,1]{1,0:T(8,128)S(1)} %copy.46.lr, ...), custom_call_target="tpu_custom_call" | custom-call | flops 2147483648 | bytes 2097152 | tf_op jit(solution)/shard_map/state/pallas_call | solution.py:51
  87.3 0.1 copy.47
  87.4 0.8 broadcast_in_dim.44
  88.2 3.4 %all-to-all-start.2 = ((bf16[8,2,128,64]{2,3,1,0:T(8,128)(2,1)}), bf16[8,2,128,64]{2,3,1,0:T(8,128)(2,1)S(1)}, u32[]{:S(2)}, u32[]{:S(2)}) async-start(bf16[8,2,128,64]{2,3,1,0:T(8,128)(2,1)} %broadcast_in_dim.44), calls=%async_computation.2 | async-start | bytes 524288 | tf_op jit(solution)/shard_map/all_to_all | solution.py:42
  91.6 0.1 add_compare_fusion
  91.7 9.4 %all-to-all-done.2 = bf16[8,2,128,64]{2,3,1,0:T(8,128)(2,1)S(1)} async-done(((bf16[8,2,128,64]{2,3,1,0:T(8,128)(2,1)}), bf16[8,2,128,64]{2,3,1,0:T(8,128)(2,1)S(1)}, u32[]{:S(2)}, u32[]{:S(2)}) %all-to-all-start.2) | async-done | bytes 262176 | tf_op jit(solution)/shard_map/all_to_all | solution.py:42
  101.1 0.3 copy.48.pieces
  101.4 0.9 rowchain.1
  102.3 0.1 copy.49
  102.4 0.8 broadcast_in_dim.45
  103.2 3.4 %all-to-all-start.3 = ((bf16[8,2,128,64]{2,3,1,0:T(8,128)(2,1)}), bf16[8,2,128,64]{2,3,1,0:T(8,128)(2,1)S(1)}, u32[]{:S(2)}, u32[]{:S(2)}) async-start(bf16[8,2,128,64]{2,3,1,0:T(8,128)(2,1)} %broadcast_in_dim.45), calls=%async_computation.3 | async-start | bytes 524288 | tf_op jit(solution)/shard_map/all_to_all | solution.py:42
  106.6 0.1 copy.61.gain
  106.8 0.1 broadcast_and_fusion
  106.9 9.0 %all-to-all-done.3 = bf16[8,2,128,64]{2,3,1,0:T(8,128)(2,1)S(1)} async-done(((bf16[8,2,128,64]{2,3,1,0:T(8,128)(2,1)}), bf16[8,2,128,64]{2,3,1,0:T(8,128)(2,1)S(1)}, u32[]{:S(2)}, u32[]{:S(2)}) %all-to-all-start.3) | async-done | bytes 262176 | tf_op jit(solution)/shard_map/all_to_all | solution.py:42
  115.9 0.3 copy.60.pieces
  116.2 0.0 all-gather.2.cloned.1.call-done
  116.2 1.7 %convolution_convert_fusion = bf16[256,256]{1,0:T(8,128)(2,1)S(1)} fusion(bf16[256,2048]{1,0:T(8,128)(2,1)S(1)} %copy-done.6, bf16[2048,640]{1,0:T(8,128)(2,1)} %all-gather.2.cloned.1.call-done), kind=kOutput, calls=%fused_computation.3 | convolution fusion | flops 268500992 | bytes 2228224 | tf_op jit(solution)/shard_map/dot_general | solution.py:427
  118.0 0.1 slice.57
  118.0 0.1 fusion.6
  118.2 0.1 copy.54
  118.3 0.1 reshape.200
  118.3 0.1 copy.55
  118.5 0.1 fusion.8
  118.6 0.1 fusion.13
  118.7 2.1 %collective-permute-start.4 = (bf16[128,128]{1,0:T(8,128)(2,1)S(1)}, bf16[128,128]{1,0:T(8,128)(2,1)S(1)}, u32[]{:S(2)}, u32[]{:S(2)}) collective-permute-start(bf16[128,128]{1,0:T(8,128)(2,1)S(1)} %get-tuple-element.24), channel_id=1, source_target_pairs={{0,8},{8,16},{16,24},{24,32},{32,40},{40,48},{48,56},{56,64},{64,7... | collective-permute-start | bytes 98312 | tf_op jit(solution)/shard_map/ppermute | solution.py:37
  120.8 0.1 multiply_convert_fusion
  121.0 1.1 slice.54.w
  122.1 2.8 %reads.1.local = f32[2,128,256]{2,1,0:T(8,128)S(1)} custom-call(bf16[256,2048]{1,0:T(8,128)(2,1)S(1)} %copy-done.6, bf16[2048,128]{1,0:T(8,128)(2,1)S(1)} %slice.54.w, f32[128,1]{1,0:T(8,128)S(1)} %copy.46.lr, f32[128,256]{1,0:T(8,128)S(1)} %get-tuple-element.15.cum, f32[128,256]{1,0:T(8,128)S(1)} %get-tuple-element.20.unit, ...), custom_call_target="tpu_custom_call" | custom-call | flops 2147483648 | bytes 2097152 | tf_op jit(solution)/shard_map/reads/pallas_call | solution.py:51
  124.9 1.3 slice.63.w
  126.2 0.1 maximum_maximum_fusion
  126.3 0.1 copy.51
  126.4 0.3 fusion.20
  126.7 0.1 broadcast_maximum_fusion
  126.8 0.1 fusion.4
  126.9 0.1 exponential_add_fusion
  127.0 0.3 fusion.2
  127.3 0.1 copy.67
  127.4 0.1 reshape.205.att
  127.5 2.6 %final.1 = bf16[8,32,2048]{2,1,0:T(8,128)(2,1)} custom-call(s32[1]{0:T(128)} %bitcast.place, bf16[8,2,128,64]{3,2,1,0:T(8,128)(2,1)S(1)} %copy.60.pieces, bf16[2,128,64]{2,1,0:T(8,128)(2,1)S(1)} %get-tuple-element.19.inside, f32[2,128,256]{2,1,0:T(8,128)S(1)} %reads.1.local, f32[128,1]{1,0:T(8,128)S(1)} %copy.61.gain, bf16[256,128]{1,0:T(8,128)(2,1)S(1)} %reshape.205.att, ...), custom_call_target="tpu_custom_call" | custom-call | flops 1073741824 | bytes 2097152 | tf_op jit(solution)/shard_map/final/pallas_call | solution.py:51
  130.1 9.2 %all-to-all-start.4 = ((bf16[8,32,2048]{2,1,0:T(8,128)(2,1)}), bf16[8,32,2048]{2,1,0:T(8,128)(2,1)S(1)}, u32[]{:S(2)}, u32[]{:S(2)}) async-start(bf16[8,32,2048]{2,1,0:T(8,128)(2,1)} %final.1), calls=%async_computation.4 | async-start | bytes 2097152 | tf_op jit(solution)/shard_map/all_to_all | solution.py:441
  139.3 0.7 fusion.18
  140.0 14.3 %all-to-all-done.4 = bf16[8,32,2048]{2,1,0:T(8,128)(2,1)S(1)} async-done(((bf16[8,32,2048]{2,1,0:T(8,128)(2,1)}), bf16[8,32,2048]{2,1,0:T(8,128)(2,1)S(1)}, u32[]{:S(2)}, u32[]{:S(2)}) %all-to-all-start.4) | async-done | bytes 1048608 | tf_op jit(solution)/shard_map/all_to_all | solution.py:441
  154.3 0.8 reduce_sum.44
  (39 shorter events, 0.2 us)
Async XLA Ops:
  7.2 56.6 %copy-start = (bf16[64,1024]{1,0:T(8,128)(2,1)S(1)}, bf16[64,1024]{1,0:T(8,128)(2,1)}, u32[]{:S(2)}) copy-start(bf16[64,1024]{1,0:T(8,128)(2,1)} %param.27) | copy-start | bytes 393220
  7.2 109.0 %all-gather.2.cloned.1.call-start = ((), (), s32[]{:S(2)}) async-start(), calls=%async_computation.5 | async-start | bytes 2949120 | tf_op jit(solution)/shard_map/all_gather | solution.py:373
  8.2 34.3 %copy-start.1 = (bf16[256,256]{1,0:T(8,128)(2,1)S(1)}, bf16[256,256]{1,0:T(8,128)(2,1)}, u32[]{:S(2)}) copy-start(bf16[256,256]{1,0:T(8,128)(2,1)} %own.1) | copy-start | bytes 393220
  30.6 32.6 %copy-start.7 = (bf16[2048,64]{0,1:T(8,128)(2,1)S(1)}, bf16[2048,64]{0,1:T(8,128)(2,1)}, u32[]{:S(2)}) copy-start(bf16[2048,64]{0,1:T(8,128)(2,1)} %param.26) | copy-start | bytes 786436
  30.7 32.9 %copy-start.9 = (f32[128]{0:T(128)S(1)}, f32[128]{0:T(128)}, u32[]{:S(2)}) copy-start(f32[128]{0:T(128)} %param.29) | copy-start | bytes 1540
  30.7 34.3 %copy-start.2 = (f32[2048]{0:T(1024)S(1)}, f32[2048]{0:T(1024)}, u32[]{:S(2)}) copy-start(f32[2048]{0:T(1024)} %param.19) | copy-start | bytes 24580
  30.7 34.3 %copy-start.3 = (f32[2,256]{1,0:T(2,128)S(1)}, f32[2,256]{1,0:T(2,128)}, u32[]{:S(2)}) copy-start(f32[2,256]{1,0:T(2,128)} %base.1) | copy-start | bytes 6148
  31.8 48.9 %all-to-all-start.1 = ((bf16[8,256,256]{2,1,0:T(8,128)(2,1)}), bf16[8,256,256]{2,1,0:T(8,128)(2,1)S(1)}, u32[]{:S(2)}, u32[]{:S(2)}) async-start(bf16[8,256,256]{2,1,0:T(8,128)(2,1)} %broadcast_in_dim.43), calls=%async_computation.1 | async-start | bytes 2097152 | tf_op jit(solution)/shard_map/all_to_all | solution.py:42
  42.5 10.0 %collective-permute-start = (bf16[256,256]{1,0:T(8,128)(2,1)S(1)}, bf16[256,256]{1,0:T(8,128)(2,1)S(1)}, u32[]{:S(2)}, u32[]{:S(2)}) collective-permute-start(bf16[256,256]{1,0:T(8,128)(2,1)S(1)} %copy-done.1), channel_id=1, source_target_pairs={{0,2},{2,4},{4,6},{6,0},{1,3},{3,5},{5,7},{7,1},{8,10},{10,12},{12... | collective-permute-start | bytes 393224 | tf_op jit(solution)/shard_map/ppermute | solution.py:31
  45.6 6.8 %collective-permute-start.1 = (bf16[256,256]{1,0:T(8,128)(2,1)S(1)}, bf16[256,256]{1,0:T(8,128)(2,1)S(1)}, u32[]{:S(2)}, u32[]{:S(2)}) collective-permute-start(bf16[256,256]{1,0:T(8,128)(2,1)S(1)} %copy-done.1), channel_id=1, source_target_pairs={{0,6},{2,0},{4,2},{6,4},{1,7},{3,1},{5,3},{7,5},{8,14},{10,8},{12,... | collective-permute-start | bytes 393224 | tf_op jit(solution)/shard_map/ppermute | solution.py:31
  49.0 7.5 %collective-permute-start.2 = (bf16[256,256]{1,0:T(8,128)(2,1)S(1)}, bf16[256,256]{1,0:T(8,128)(2,1)S(1)}, u32[]{:S(2)}, u32[]{:S(2)}) collective-permute-start(bf16[256,256]{1,0:T(8,128)(2,1)S(1)} %copy-done.1), channel_id=1, source_target_pairs={{0,4},{2,6},{4,0},{6,2},{1,5},{3,7},{5,1},{7,3},{8,12},{10,14},{12... | collective-permute-start | bytes 393224 | tf_op jit(solution)/shard_map/ppermute | solution.py:31
  57.4 7.6 %collective-permute-start.3 = (bf16[4,256,256]{2,1,0:T(8,128)(2,1)}, bf16[4,256,256]{2,1,0:T(8,128)(2,1)S(1)}, u32[]{:S(2)}, u32[]{:S(2)}) collective-permute-start(bf16[4,256,256]{2,1,0:T(8,128)(2,1)} %pad_maximum_fusion), channel_id=1, source_target_pairs={{0,1},{1,0},{2,3},{3,2},{4,5},{5,4},{6,7},{7,6},{8,9},{9,8},{10,11... | collective-permute-start | bytes 1572872 | tf_op jit(solution)/shard_map/ppermute | solution.py:31
  66.9 1.0 copy-start.4
  80.6 1.2 copy-start.5
  87.3 19.3 %copy-start.10 = (f32[128]{0:T(128)S(1)}, f32[128]{0:T(128)}, u32[]{:S(2)}) copy-start(f32[128]{0:T(128)} %param.33) | copy-start | bytes 1540
  87.3 28.9 %copy-start.6 = (bf16[256,2048]{1,0:T(8,128)(2,1)S(1)}, bf16[256,2048]{1,0:T(8,128)(2,1)}, u32[]{:S(2)}) copy-start(bf16[256,2048]{1,0:T(8,128)(2,1)} %copy-done.4) | copy-start | bytes 3145732
  88.2 12.9 %all-to-all-start.2 = ((bf16[8,2,128,64]{2,3,1,0:T(8,128)(2,1)}), bf16[8,2,128,64]{2,3,1,0:T(8,128)(2,1)S(1)}, u32[]{:S(2)}, u32[]{:S(2)}) async-start(bf16[8,2,128,64]{2,3,1,0:T(8,128)(2,1)} %broadcast_in_dim.44), calls=%async_computation.2 | async-start | bytes 524288 | tf_op jit(solution)/shard_map/all_to_all | solution.py:42
  103.2 12.8 %all-to-all-start.3 = ((bf16[8,2,128,64]{2,3,1,0:T(8,128)(2,1)}), bf16[8,2,128,64]{2,3,1,0:T(8,128)(2,1)S(1)}, u32[]{:S(2)}, u32[]{:S(2)}) async-start(bf16[8,2,128,64]{2,3,1,0:T(8,128)(2,1)} %broadcast_in_dim.45), calls=%async_computation.3 | async-start | bytes 524288 | tf_op jit(solution)/shard_map/all_to_all | solution.py:42
  106.6 11.9 %copy-start.11 = (f32[64]{0:T(128)S(1)}, f32[64]{0:T(128)}, u32[]{:S(2)}) copy-start(f32[64]{0:T(128)} %param.31) | copy-start | bytes 772
  106.9 13.9 %copy-start.12 = (f32[64]{0:T(128)S(1)}, f32[64]{0:T(128)}, u32[]{:S(2)}) copy-start(f32[64]{0:T(128)} %param.30) | copy-start | bytes 772
  118.7 7.5 %collective-permute-start.4 = (bf16[128,128]{1,0:T(8,128)(2,1)S(1)}, bf16[128,128]{1,0:T(8,128)(2,1)S(1)}, u32[]{:S(2)}, u32[]{:S(2)}) collective-permute-start(bf16[128,128]{1,0:T(8,128)(2,1)S(1)} %get-tuple-element.24), channel_id=1, source_target_pairs={{0,8},{8,16},{16,24},{24,32},{32,40},{40,48},{48,56},{56,64},{64,7... | collective-permute-start | bytes 98312 | tf_op jit(solution)/shard_map/ppermute | solution.py:37
  124.9 1.8 %copy-start.8 = (f32[2]{0:T(128)S(1)}, f32[2]{0:T(128)}, u32[]{:S(2)}) copy-start(f32[2]{0:T(128)} %param.32) | copy-start | bytes 28
  130.1 24.2 %all-to-all-start.4 = ((bf16[8,32,2048]{2,1,0:T(8,128)(2,1)}), bf16[8,32,2048]{2,1,0:T(8,128)(2,1)S(1)}, u32[]{:S(2)}, u32[]{:S(2)}) async-start(bf16[8,32,2048]{2,1,0:T(8,128)(2,1)} %final.1), calls=%async_computation.4 | async-start | bytes 2097152 | tf_op jit(solution)/shard_map/all_to_all | solution.py:441
Sparse Core Ops, SparseCore 0:
  30.8 62.8 all-gather.1

commit v2 on v1

v2 whole, which is shorter than its diff:
```python
import math

import jax
import jax.numpy as jnp
from jax import lax
from jax.experimental import pallas as pl
from jax.experimental.pallas import tpu as pltpu
from jax.sharding import Mesh
from jax.sharding import PartitionSpec as P

HEAD = 64
WINDOW = 128
CHUNK = 32
SP = ("sp_0", "sp_1")
SP_FS_TP = ("sp_0", "sp_1", "fs", "tp")
F32 = jnp.float32
BF16 = jnp.bfloat16

NORM_EPS = 1e-06
KEY_EPS = 1e-06
GROUP_EPS = 0.00064
DECAY_FLOOR = -104.0

NT = (((1,), (1,)), ((), ()))
TN = (((0,), (0,)), ((), ()))


def ring_shift(array, axis, by):
    devices = lax.axis_size(axis)
    return lax.ppermute(array, axis, [(i, (i + by) % devices) for i in range(devices)])


def passed_along(array, axis, by):
    devices = lax.axis_size(axis)
    pairs = [(i, i + by) for i in range(devices) if 0 <= i + by < devices]
    return lax.ppermute(array, axis, pairs)


def from_everyone(array, axis):
    copies = jnp.broadcast_to(array, (lax.axis_size(axis), *array.shape))
    return lax.all_to_all(copies, axis, split_axis=0, concat_axis=0, tiled=True)


class Fetched:
    def __init__(self, source, target, sem):
        self.copy = pltpu.make_async_copy(source, target, sem)
        self.copy.start()
        self.target = target

    def get(self):
        self.copy.wait()
        return self.target


class Stored:
    def __init__(self, ref, target, sem):
        self.ref = ref
        self.copy = pltpu.make_async_copy(ref, target, sem)

    def put(self):
        self.copy.start()


def call(kernel, outs, scratch=(), flops=0, smem=0, far=None, far_out=()):
    far = far or {}

    def run(*args):
        n_in, n_out = len(args), len(outs)
        held = []
        for i in sorted(far):
            rows, width = args[i].shape[-2:]
            if far[i] is not None:
                width = far[i][0]
            held.append(pltpu.VMEM((*args[i].shape[:-2], rows, width), args[i].dtype))
        held += [pltpu.VMEM(*outs[i]) for i in far_out]
        ins = [
            pl.BlockSpec(memory_space=pltpu.SMEM)
            if i < smem
            else pl.BlockSpec(memory_space=pltpu.HBM if i in far else pltpu.VMEM)
            for i in range(n_in)
        ]

        def body(*refs):
            refs = list(refs)
            extra = refs[n_in + n_out :]
            sems = extra[len(held)]
            for k, i in enumerate(sorted(far)):
                source = refs[i]
                if far[i] is not None:
                    width, block = far[i]
                    source = source.at[:, pl.ds(width * block, width)]
                refs[i] = Fetched(source, extra[k], sems.at[k])
            stored = []
            for k, i in enumerate(far_out):
                at = len(far) + k
                stored.append(Stored(extra[at], refs[n_in + i], sems.at[at]))
                refs[n_in + i] = stored[-1]
            kernel(*refs[: n_in + n_out], *extra[len(held) + 1 :])
            for one in stored:
                one.copy.wait()

        return pl.pallas_call(
            body,
            out_shape=[jax.ShapeDtypeStruct(s, d) for s, d in outs],
            in_specs=ins,
            out_specs=[
                pl.BlockSpec(memory_space=pltpu.HBM if i in far_out else pltpu.VMEM)
                for i in range(n_out)
            ],
            scratch_shapes=[*held, pltpu.SemaphoreType.DMA((max(1, len(held)),)), *scratch],
            cost_estimate=pl.CostEstimate(flops=flops, bytes_accessed=1 << 21, transcendentals=0),
            compiler_params=pltpu.CompilerParams(vmem_limit_bytes=24 << 20),
        )(*args)

    return run


def dot(a, b, dims=(((1,), (0,)), ((), ()))):
    return lax.dot_general(a.astype(BF16), b.astype(BF16), dims, preferred_element_type=F32)


def hidden_kernel(place, own, next_, before, across, other, gain, down, up, base, hid, decays):
    x = place[0]
    core = place[1]
    rows = own.shape[0]
    blocks = [own, before, across, next_]
    sums = jnp.zeros((rows, 1), F32)
    for k in range(4):
        mine = blocks[k][...].astype(F32)
        theirs = other[k].astype(F32)
        sums += jnp.sum(mine * mine + theirs * theirs, axis=1, keepdims=True)
    width = own.shape[1]
    scale = lax.rsqrt(sums / (8 * width) + NORM_EPS)
    low = jnp.zeros((rows, down.shape[0]), F32)
    for k in range(4):
        chip = lax.rem(x + k, 4)
        for c, block in ((core, blocks[k][...]), (1 - core, other[k])):
            at = pl.multiple_of((chip * 2 + c) * width, width)
            h = (block.astype(F32) * scale * gain[:, pl.ds(at, width)]).astype(BF16)
            hid.ref[:, pl.ds(at, width)] = h
            low += lax.dot_general(h, down[:, pl.ds(at, width)], NT, preferred_element_type=F32)
    hid.put()
    low = jnp.tanh(low).astype(BF16)
    rate = lax.dot_general(up[...], low, (((0,), (1,)), ((), ())), preferred_element_type=F32)
    heads = base.shape[0]
    base_rows = jnp.concatenate(
        [jnp.broadcast_to(base[h : h + 1, :], (HEAD, rows)) for h in range(heads)], axis=0
    )
    log_decay = jnp.maximum(-jnp.exp(rate + base_rows), DECAY_FLOOR)
    lane = lax.broadcasted_iota(jnp.int32, log_decay.shape, 1) % CHUNK
    total, after = log_decay, log_decay
    step = 1
    while step < CHUNK:
        total = total + jnp.where(lane >= step, pltpu.roll(total, step, 1), 0.0)
        after = after + jnp.where(lane < CHUNK - step, pltpu.roll(after, rows - step, 1), 0.0)
        step *= 2
    decays.ref[0] = total
    decays.ref[1] = total - log_decay
    decays.ref[2] = after - log_decay
    decays.put()


def as_column(row):
    return jnp.broadcast_to(row, (8, row.shape[1])).T[:, :1]


def head_rows(h):
    return slice(h * HEAD, (h + 1) * HEAD)


def band_tables(left, right, start, end, rate, first, heads):
    rows = left.shape[1]
    dist = (
        lax.broadcasted_iota(jnp.int32, (CHUNK, rows), 1) % CHUNK
        - lax.broadcasted_iota(jnp.int32, (CHUNK, rows), 0)
    )
    plain, rated = [], []
    for h in range(heads):
        sl = head_rows(h)
        l, r, s, e = left[sl, :], right[sl, :], start[sl, :], end[sl, :]
        speed = jnp.broadcast_to(rate[sl, :], l.shape)
        t_plain = jnp.zeros((CHUNK, rows), F32)
        t_rated = jnp.zeros((CHUNK, rows), F32)
        for d in range(first, CHUNK):
            rd = r if d == 0 else pltpu.roll(r, d, 1)
            ed = e if d == 0 else pltpu.roll(e, d, 1)
            x = l * rd * jnp.exp(s - ed)
            here = dist == d
            t_plain = jnp.where(here, jnp.sum(x, axis=0, keepdims=True), t_plain)
            t_rated = jnp.where(here, jnp.sum(x * speed, axis=0, keepdims=True), t_rated)
        plain.append(t_plain)
        rated.append(t_rated)
    return plain, rated


def in_chunks(table):
    rows = table.shape[1]
    tall = jnp.concatenate([table] * (rows // CHUNK), axis=0)
    same = (
        lax.broadcasted_iota(jnp.int32, (rows, rows), 0) // CHUNK
        == lax.broadcasted_iota(jnp.int32, (rows, rows), 1) // CHUNK
    )
    return jnp.where(same, tall, 0.0).astype(BF16)


def by_chunk(array):
    rows = array.shape[1]
    chunk = lax.broadcasted_iota(jnp.int32, array.shape, 1) // CHUNK
    return jnp.concatenate(
        [jnp.where(chunk == c, array, 0.0).astype(BF16) for c in range(rows // CHUNK)], axis=0
    )


def state_kernel(hid, w, lr, decays, ends, units, tables, dec):
    rows = dec.shape[0]
    heads = lr.shape[1] // HEAD
    span = heads * HEAD
    lr = as_column(lr[...])
    hid, decays = hid.get(), decays.get()
    kv = jnp.dot(hid[...], w[...], preferred_element_type=F32).astype(BF16).astype(F32)
    kv_t = kv.T
    for h in range(heads):
        k = kv_t[head_rows(h), :]
        square = jnp.sum(k * k, axis=0, keepdims=True) + KEY_EPS
        inv = lax.rsqrt(square)
        units.ref[0, head_rows(h), :] = k * inv
        units.ref[1, head_rows(h), :] = kv_t[span + h * HEAD : span + (h + 1) * HEAD, :] * (square * inv)
    cum_all = decays[0]
    prev = decays[1]
    dec[...] = jnp.exp(cum_all).T
    u = units.ref[0]
    v = units.ref[1]
    plain, rated = band_tables(u, u, prev, cum_all, lr, 1, heads)
    reach = jnp.exp(prev)
    x, q = [], []
    for h in range(heads):
        sl = head_rows(h)
        x.append(jnp.concatenate([-u[sl, :] * reach[sl, :], -dot(v[sl, :], in_chunks(plain[h]))], axis=0))
        q.append(in_chunks(-rated[h]))
    units.put()
    power = 1
    while power < CHUNK:
        for h in range(heads):
            x[h] = x[h] + dot(x[h], q[h])
        power *= 2
        if power < CHUNK:
            for h in range(heads):
                q[h] = dot(q[h], q[h]).astype(BF16)
    left = jnp.exp(decays[2])
    chunks = rows // CHUNK
    grow = []
    for h in range(heads):
        sl = head_rows(h)
        tables.ref[h, :, :rows] = x[h].astype(BF16)
        out_u = u[sl, :] * left[sl, :]
        out_b = out_u * lr[sl, :]
        g = dot(x[h], by_chunk(out_b), NT)
        g_low = g[HEAD:, :] + dot(v[sl, :], by_chunk(out_u), NT)
        grow.append((g[:HEAD, :].astype(BF16), g_low))
    eye = (
        lax.broadcasted_iota(jnp.int32, (2 * HEAD, HEAD), 0)
        == lax.broadcasted_iota(jnp.int32, (2 * HEAD, HEAD), 1)
    ).astype(F32)
    state = [eye] * heads
    zero = jnp.zeros((HEAD, HEAD), F32)
    for c in range(chunks):
        at = slice(c * HEAD, (c + 1) * HEAD)
        last = c * CHUNK + CHUNK - 1
        for h in range(heads):
            low = state[h].astype(BF16)
            tables.ref[h, :, rows + c * HEAD : rows + (c + 1) * HEAD] = low
            kept = state[h] * dec[last : last + 1, head_rows(h)]
            added = jnp.concatenate([zero, grow[h][1][:, at]], axis=0)
            state[h] = kept + added + jnp.dot(low, grow[h][0][:, at], preferred_element_type=F32)
    packed = jnp.concatenate(state, axis=1).astype(BF16)
    for k in range(ends.shape[0]):
        ends[k] = packed
    tables.put()


def read_kernel(hid, w, lr, decays, units, tables, out):
    heads = lr.shape[1] // HEAD
    lr = as_column(lr[...])
    hid, w, decays, units = hid.get(), w.get(), decays.get(), units.get()
    rows = hid.shape[0]
    reads = jnp.dot(hid[...], w[...], preferred_element_type=F32).astype(BF16).astype(F32)
    r = reads.T
    cum_all = decays[0]
    plain, rated = band_tables(r, units[0], cum_all, cum_all, lr, 0, heads)
    reach = r * jnp.exp(cum_all)
    tables = tables.get()
    for h in range(heads):
        sl = head_rows(h)
        mixed = dot(tables[h, :, :rows], in_chunks(rated[h]))
        query = mixed[:HEAD, :] + reach[sl, :]
        local = mixed[HEAD:, :] + dot(units[1, sl, :], in_chunks(plain[h]))
        both = dot(tables[h, :, rows:], by_chunk(query))
        out.ref[h, :HEAD, :] = both[:HEAD, :]
        out.ref[h, HEAD:, :] = both[HEAD:, :] + local
    out.put()


def chain(earlier, later):
    moved = jnp.dot(earlier.astype(BF16), later[:HEAD, :], preferred_element_type=F32)
    return moved + jnp.concatenate([jnp.zeros((HEAD, HEAD), F32), later[HEAD:, :].astype(F32)], axis=0)


def row_kernel(place, pieces, total_out, inside_out):
    devices, heads = pieces.shape[0], pieces.shape[2] // HEAD
    eye = (
        lax.broadcasted_iota(jnp.int32, (2 * HEAD, HEAD), 0)
        == lax.broadcasted_iota(jnp.int32, (2 * HEAD, HEAD), 1)
    ).astype(F32)
    total = [eye] * heads
    inside = [eye] * heads
    for k in range(devices):
        passed = k < place[0]
        for h in range(heads):
            later = pieces[k, :, head_rows(h)]
            total[h] = later.astype(F32) if k == 0 else chain(total[h], later)
            inside[h] = jnp.where(passed, total[h], inside[h])
    packed = jnp.concatenate(total, axis=1).astype(BF16)
    for k in range(total_out.shape[0]):
        total_out[k] = packed
    inside_out[...] = jnp.concatenate(inside, axis=1).astype(BF16)


def final_kernel(place, pieces, inside, local, gain, att, w, out):
    devices, heads = pieces.shape[0], pieces.shape[2] // HEAD
    state = [jnp.zeros((HEAD, HEAD), F32)] * heads
    for k in range(devices - 1):
        passed = k < place[0]
        for h in range(heads):
            later = pieces[k, :, head_rows(h)]
            new = jnp.dot(state[h].astype(BF16), later[:HEAD, :], preferred_element_type=F32)
            state[h] = jnp.where(passed, new + later[HEAD:, :].astype(F32), state[h])
    rows = []
    gain = as_column(gain[...])
    inside, local = inside.get(), local.get()
    for h in range(heads):
        near = inside[:, head_rows(h)]
        start = jnp.dot(state[h].astype(BF16), near[:HEAD, :], preferred_element_type=F32)
        start = start + near[HEAD:, :].astype(F32)
        y = dot(start, local[h, :HEAD, :]) + local[h, HEAD:, :]
        centered = y - jnp.mean(y, axis=0, keepdims=True)
        variance = jnp.mean(centered * centered, axis=0, keepdims=True)
        rows.append(centered * lax.rsqrt(variance + GROUP_EPS) * gain[head_rows(h), :])
    rec = jnp.concatenate(rows, axis=0).T.astype(BF16)
    mix = jnp.concatenate([att.get()[...], rec], axis=1)
    w = w.get()
    groups, width = out.shape[0], 512
    size = out.shape[1]
    for n in range(w.shape[0] // width):
        at = slice(n * width, (n + 1) * width)
        part = lax.dot_general(mix, w[at, :], NT, preferred_element_type=F32).astype(BF16)
        for g in range(groups):
            out[g, :, at] = part[g * size : (g + 1) * size, :]


def head_rms(values, gain):
    heads = []
    for h in range(values.shape[1] // HEAD):
        x = values[:, head_rows(h)]
        mean_sq = jnp.mean(x * x, axis=1, keepdims=True)
        heads.append((x * lax.rsqrt(mean_sq + NORM_EPS) * gain).astype(BF16))
    return heads


def attention_in_kernel(hid, w, query_gain, key_gain, queries, keys_values):
    q_w, kv_w = queries.shape[1], keys_values.shape[1] // 2
    hid, w = hid.get(), w.get()
    rows = jnp.dot(hid[...], w[...], preferred_element_type=F32).astype(BF16)
    normed = head_rms(rows[:, :q_w].astype(F32), query_gain[...])
    queries[...] = jnp.concatenate(normed, axis=1)
    normed = head_rms(rows[:, q_w : q_w + kv_w].astype(F32), key_gain[...])
    keys_values[...] = jnp.concatenate(normed + [rows[:, q_w + kv_w :]], axis=1)


def attention_kernel(place, sink, queries, keys_values, before, out, lse):
    rows = queries.shape[0]
    heads = queries.shape[1] // HEAD
    shape = (2 * WINDOW, WINDOW)
    key_at = lax.broadcasted_iota(jnp.int32, shape, 0)
    lag = lax.broadcasted_iota(jnp.int32, shape, 1) + WINDOW - key_at
    near = (lag >= 0) & (lag < WINDOW)
    for n in range(rows // WINDOW):
        at = slice(n * WINDOW, (n + 1) * WINDOW)
        if n == 0:
            band = jnp.concatenate([before[...], keys_values[at, :]], axis=0)
            allowed = near & ((key_at >= WINDOW) | (place[0] > 0))
        else:
            band = keys_values[(n - 1) * WINDOW : (n + 1) * WINDOW, :]
            allowed = near
        tiles = []
        for h in range(heads):
            score = lax.dot_general(
                band[:, :HEAD], queries[at, head_rows(h)], NT, preferred_element_type=F32
            ) * (1.0 / math.sqrt(HEAD))
            score = jnp.where(allowed, score, -jnp.inf)
            top = jnp.maximum(jnp.max(score, axis=0, keepdims=True), sink[h])
            weight = jnp.exp(score - top)
            total = jnp.sum(weight, axis=0, keepdims=True) + jnp.exp(sink[h] - top)
            lse[h : h + 1, at] = top + jnp.log(total)
            probs = (weight / total).astype(BF16)
            mixed = lax.dot_general(probs, band[:, HEAD:], TN, preferred_element_type=F32)
            tiles.append(mixed.astype(BF16))
        out[at, :] = jnp.concatenate(tiles, axis=1)


def per_device(
    tokens,
    norm_gain,
    query_w,
    key_w,
    value_w,
    recept_w,
    rec_key_w,
    rec_value_w,
    decay_down,
    decay_up,
    decay_base,
    learn_rate,
    query_gain,
    key_gain,
    sink_logit,
    group_gain,
    out_att_w,
    out_rec_w,
):
    rows = tokens.shape[0]
    span = recept_w.shape[1]
    heads = span // HEAD
    features = norm_gain.shape[0]
    groups = lax.axis_size(("fs", "tp"))
    place_zy = [lax.axis_index(a).astype(jnp.int32).reshape(1) for a in SP]

    own = jnp.concatenate(
        [rec_key_w, rec_value_w, query_w, key_w, value_w, out_att_w.T, out_rec_w.T, recept_w], axis=1
    )
    column = from_everyone(own, "sp_1").reshape(-1, own.shape[1])
    state_w = from_everyone(column[:, : 2 * span], "sp_0").reshape(features, 2 * span)
    before = ring_shift(tokens, "fs", -1)
    across = ring_shift(tokens, "fs", 2)
    next_ = ring_shift(tokens, "fs", 1)
    other = ring_shift(jnp.stack([tokens, before, across, next_]), "tp", 1)


    place_xc = jnp.stack([lax.axis_index("fs"), lax.axis_index("tp")]).astype(jnp.int32)
    decay_cols = lax.dynamic_slice_in_dim(
        decay_up, lax.axis_index(("fs", "tp")) * span, span, 1
    )
    flat = (span, rows)
    hid, decays = call(
        hidden_kernel,
        [((rows, features), BF16), ((3, *flat), F32)],
        smem=1,
        flops=1 << 27,
        far_out=(0, 1),
    )(
        place_xc, tokens, next_, before, across, other, norm_gain.reshape(1, -1), decay_down.T, decay_cols, decay_base
    )

    held, hid = lax.optimization_barrier((column[:, 2 * span :], hid))
    other_w = lax.all_gather(held, "sp_0", axis=0, tiled=True)

    lr = learn_rate.reshape(1, span)
    chunks = rows // CHUNK
    pair = (2 * HEAD, span)
    ends, units, tables = call(
        state_kernel,
        [
            ((lax.axis_size("sp_1"), *pair), BF16),
            ((2, *flat), F32),
            ((heads, 2 * HEAD, rows + chunks * HEAD), BF16),
        ],
        scratch=[pltpu.VMEM((rows, span), F32)],
        flops=1 << 31,
        far={0: None, 3: None},
        far_out=(1, 2),
    )(hid, state_w, lr, decays)

    row_pieces = lax.all_to_all(ends, "sp_1", 0, 0, tiled=True)
    row_total, inside = call(
        row_kernel, [((lax.axis_size("sp_0"), *pair), BF16), (pair, BF16)], smem=1, flops=1 << 27
    )(place_zy[1], row_pieces)
    all_pieces = lax.all_to_all(row_total, "sp_0", 0, 0, tiled=True)

    q_w, kv_w = query_w.shape[1], key_w.shape[1]
    whole = q_w + 2 * kv_w
    (local,) = call(
        read_kernel, [((heads, 2 * HEAD, rows), F32)], flops=1 << 31,
        far={0: None, 1: (span, 2 * whole // span), 3: None, 4: None, 5: None}, far_out=(0,),
    )(hid, other_w, lr, decays, units, tables)
    queries, keys_values = call(
        attention_in_kernel,
        [((rows, q_w), BF16), ((rows, 2 * kv_w), BF16)],
        flops=1 << 28,
        far={0: None, 1: (whole, 0)},
    )(hid, other_w, query_gain.reshape(1, HEAD), key_gain.reshape(1, HEAD))
    before_keys = passed_along(keys_values[rows - WINDOW :], SP, 1)
    place_sp = lax.axis_index(SP).astype(jnp.int32).reshape(1)
    att_mix, row_lse = call(
        attention_kernel, [((rows, q_w), BF16), ((q_w // HEAD, rows), F32)], smem=2, flops=1 << 28
    )(place_sp, sink_logit, queries, keys_values, before_keys)

    (partial,) = call(
        final_kernel,
        [((groups, rows // groups, features), BF16)],
        smem=1,
        flops=1 << 30,
        far={2: None, 3: None, 5: None, 6: (whole, 1)},
    )(place_zy[0], all_pieces, inside, local, group_gain.reshape(1, span), att_mix, other_w)
    tiles = lax.all_to_all(partial, ("fs", "tp"), 0, 0, tiled=True)
    mixed = jnp.sum(tiles.astype(F32), axis=0).astype(BF16)
    return (mixed, row_lse)


def solution(mesh):
    split = Mesh(
        mesh.devices.reshape(8, 8, mesh.shape["fs"], mesh.shape["tp"]), ("sp_0", "sp_1", "fs", "tp")
    )
    in_specs = (
        P(SP, ("fs", "tp")),
        P(),
        P(SP, ("fs", "tp")),
        P(SP, ("fs", "tp")),
        P(SP, ("fs", "tp")),
        P(SP, ("fs", "tp")),
        P(SP, ("fs", "tp")),
        P(SP, ("fs", "tp")),
        P(),
        P(),
        P(("fs", "tp"), SP),
        P(("fs", "tp")),
        P(),
        P(),
        P(("fs", "tp")),
        P(("fs", "tp")),
        P(("fs", "tp"), SP),
        P(("fs", "tp"), SP),
    )
    out_specs = (P(SP_FS_TP, None), P(("fs", "tp"), SP))

    return jax.shard_map(
        per_device, mesh=split, in_specs=in_specs, out_specs=out_specs, check_vma=False
    )
```

time: 163 us -> 162 us (level)
  blocking collectives: 21.7 us -> 64.9 us
  waiting for transfers between devices: 50.8 us -> 14.8 us
  starting transfers between devices: 44.7 us -> 37.4 us
  Pallas kernels: 13.6 us -> 19.2 us
  local copies, waits for them, and re-layouts: 10.9 us -> 7.77 us
  matrix products: 2.21 us -> 0 us
  other arithmetic: 3.54 us -> 1.86 us
    all_to_all x3 -> x1, waiting for transfers between devices: 31.2 us -> 0.01 us  [from_everyone(): return lax.all_to_all(copies, axis, split_axis=0, concat_axis=0, tiled=True)]
    all_to_all x1, blocking collectives: 21.7 us -> 43.5 us  [from_everyone(): return lax.all_to_all(copies, axis, split_axis=0, concat_axis=0, tiled=True)]
    all_to_all x0 -> x1, blocking collectives: none -> 21.4 us  [per_device(): tiles = lax.all_to_all(partial, ('fs', 'tp'), 0, 0, tiled=True)]
    all_to_all x3 -> x1, starting transfers between devices: 17.6 us -> 7.64 us  [from_everyone(): return lax.all_to_all(copies, axis, split_axis=0, concat_axis=0, tiled=True)]
    pallas_call x5 -> x7, Pallas kernels: 13.6 us -> 19.2 us  [run(): pl.pallas_call(body, out_shape=[jax.ShapeDtypeStruct(s, d) for s, d in ou...]
    all_to_all x1 -> x2, waiting for transfers between devices: 14.3 us -> 9.4 us  [the longest x1 9.4 us: per_device(): row_pieces = lax.all_to_all(ends, 'sp_1', 0, 0, tiled=True)]
    dot_general x3 -> x0, matrix products: 2.21 us -> none  [the longest x1 1.66 us: per_device(): jnp.dot(hid, att_w, preferred_element_type=F32).astype(BF16)]
    broadcast_in_dim x4 -> x2, local copies, waits for them, and re-layouts: 2.61 us -> 0.89 us  [from_everyone(): copies = jnp.broadcast_to(array, (lax.axis_size(axis), *array.shape))]
  transfers between devices with their start and end apart: 10 -> 9, of which waited for: 6 -> 3; matrix products, arithmetic and copies ran while one was open for 5% -> 1% of each run, Pallas kernels for 7% -> 11%
where the time goes in v2:
time: 162 us; the launch traced here: 160 us
  blocking collectives  64.9 us (40%)
  starting transfers between devices  37.4 us (23%)
  Pallas kernels  19.2 us (12%)
  waiting for transfers between devices  14.8 us (9%)
  between operations  14.4 us (9%)
  local copies, waits for them, and re-layouts  7.77 us (5%)
  other arithmetic  1.86 us (1%)
    all_to_all x1, blocking collectives, from_everyone(): return lax.all_to_all(copies, axis, split_axis=0, concat_axis=0, tiled=True)  43.5 us
    all_to_all x1, blocking collectives, per_device(): tiles = lax.all_to_all(partial, ('fs', 'tp'), 0, 0, tiled=True)  21.4 us
    pallas_call x7, Pallas kernels, run(): pl.pallas_call(body, out_shape=[jax.ShapeDtypeStruct(s, d) for s, d in ou...  19.2 us
    ppermute x4, starting transfers between devices, ring_shift(): lax.ppermute(array, axis, [(i, (i + by) % devices) for i in range(devices)])  16.9 us
    all_to_all x1, waiting for transfers between devices, per_device(): row_pieces = lax.all_to_all(ends, 'sp_1', 0, 0, tiled=True)  9.4 us
    all_to_all x1, starting transfers between devices, from_everyone(): return lax.all_to_all(copies, axis, split_axis=0, concat_axis=0, tiled=True)  7.64 us
    all_to_all x1, starting transfers between devices, per_device(): row_pieces = lax.all_to_all(ends, 'sp_1', 0, 0, tiled=True)  7.06 us
    ppermute x4, waiting for transfers between devices, ring_shift(): lax.ppermute(array, axis, [(i, (i + by) % devices) for i in range(devices)])  5.38 us
  transfers between devices with their start and end apart: 9, of which 3 were waited for; matrix products, arithmetic and copies ran while one was open for 1% of the time, Pallas kernels for 11%

profile of v2, /device:TPU:1, one launch (start us, length us, event | category | flops | bytes accessed | tf_op | source)
XLA Modules:
  0.0 160.3 jit_solution(18397572835448739711)
XLA Ops:
  7.2 0.0 copy-start
  7.2 0.0 copy-start.5
  7.2 0.0 copy-start.7
  7.2 0.0 copy-start.6
  7.2 0.0 copy-start.8
  7.2 0.9 concatenate.3
  8.2 0.8 broadcast_in_dim.6
  9.0 7.6 %all-to-all-start = ((bf16[8,32,896]{2,1,0:T(8,128)(2,1)}), bf16[8,32,896]{2,1,0:T(8,128)(2,1)}, u32[]{:S(2)}, u32[]{:S(2)}) async-start(bf16[8,32,896]{2,1,0:T(8,128)(2,1)} %broadcast_in_dim.6), calls=%async_computation | async-start | bytes 917504 | tf_op jit(solution)/shard_map/all_to_all | solution.py:41
  16.6 0.0 all-gather.2.cloned.1.call-start
  16.7 3.1 %collective-permute-start = (bf16[256,256]{1,0:T(8,128)(2,1)}, bf16[256,256]{1,0:T(8,128)(2,1)S(1)}, u32[]{:S(2)}, u32[]{:S(2)}) collective-permute-start(bf16[256,256]{1,0:T(8,128)(2,1)} %refs_1_.2), channel_id=1, source_target_pairs={{0,2},{2,4},{4,6},{6,0},{1,3},{3,5},{5,7},{7,1},{8,10},{10,12},{12... | collective-permute-start | bytes 393224 | tf_op jit(solution)/shard_map/ppermute | solution.py:30
  19.8 3.4 %collective-permute-start.1 = (bf16[256,256]{1,0:T(8,128)(2,1)}, bf16[256,256]{1,0:T(8,128)(2,1)S(1)}, u32[]{:S(2)}, u32[]{:S(2)}) collective-permute-start(bf16[256,256]{1,0:T(8,128)(2,1)} %refs_1_.2), channel_id=1, source_target_pairs={{0,6},{2,0},{4,2},{6,4},{1,7},{3,1},{5,3},{7,5},{8,14},{10,8},{12,... | collective-permute-start | bytes 393224 | tf_op jit(solution)/shard_map/ppermute | solution.py:30
  23.2 3.4 %collective-permute-start.2 = (bf16[256,256]{1,0:T(8,128)(2,1)}, bf16[256,256]{1,0:T(8,128)(2,1)S(1)}, u32[]{:S(2)}, u32[]{:S(2)}) collective-permute-start(bf16[256,256]{1,0:T(8,128)(2,1)} %refs_1_.2), channel_id=1, source_target_pairs={{0,4},{2,6},{4,0},{6,2},{1,5},{3,7},{5,1},{7,3},{8,12},{10,14},{12... | collective-permute-start | bytes 393224 | tf_op jit(solution)/shard_map/ppermute | solution.py:30
  26.6 0.0 collective-permute-done.refs_2_
  26.6 0.0 collective-permute-done.1.refs_3_
  26.7 4.0 %collective-permute-done.2.refs_4_ = bf16[256,256]{1,0:T(8,128)(2,1)S(1)} collective-permute-done((bf16[256,256]{1,0:T(8,128)(2,1)}, bf16[256,256]{1,0:T(8,128)(2,1)S(1)}, u32[]{:S(2)}, u32[]{:S(2)}) %collective-permute-start.2) | collective-permute-done | bytes 131104 | tf_op jit(solution)/shard_map/ppermute | solution.py:30
  30.6 1.0 pad_maximum_fusion
  31.6 6.9 %collective-permute-start.3 = (bf16[4,256,256]{2,1,0:T(8,128)(2,1)S(1)}, bf16[4,256,256]{2,1,0:T(8,128)(2,1)S(1)}, u32[]{:S(2)}, u32[]{:S(2)}) collective-permute-start(bf16[4,256,256]{2,1,0:T(8,128)(2,1)S(1)} %pad_maximum_fusion), channel_id=1, source_target_pairs={{0,1},{1,0},{2,3},{3,2},{4,5},{5,4},{6,7},{7,6},{8,9},{9,8},{10,11... | collective-permute-start | bytes 1572872 | tf_op jit(solution)/shard_map/ppermute | solution.py:30
  38.5 0.1 pad_add_fusion.refs_0_
  38.6 0.0 copy-done
  38.6 1.4 collective-permute-done.3.refs_5_
  40.1 0.0 copy-done.5
  40.1 0.0 copy-done.7
  40.1 0.0 copy-done.6
  40.1 0.0 copy-done.8
  40.1 0.0 copy-start.14
  40.1 2.3 %shard_map.185 = (bf16[256,2048]{1,0:T(8,128)(2,1)S(1)}, f32[3,128,256]{2,1,0:T(8,128)S(1)}) custom-call(s32[2]{0:T(128)S(1)} %pad_add_fusion.refs_0_, bf16[256,256]{1,0:T(8,128)(2,1)S(1)} %copy-done.5, bf16[256,256]{1,0:T(8,128)(2,1)S(1)} %collective-permute-done.refs_2_, bf16[256,256]{1,0:T(8,128)(2,1)S(1)} %collective-permute-done.1.refs_3_, ...), custom_call_target="tpu_custom_call" | custom-call | flops 134217728 | bytes 2097152 | tf_op jit(solution)/shard_map/pallas_call | solution.py:102
  42.4 0.0 copy-start.3
  42.4 0.0 copy-start.12
  42.4 0.0 all-to-all-done
  42.4 2.0 %slice.12 = bf16[256,640]{1,0:T(8,128)(2,1)} slice(bf16[256,896]{1,0:T(8,128)(2,1)} %bitcast.4), slice={[0:256], [256:896]} | slice | bytes 655360 | tf_op jit(solution)/shard_map/slice | solution.py:463
  44.4 0.0 all-gather.2.cloned.1.call-update
  44.4 0.9 slice.13
  45.3 0.1 broadcast_in_dim.7
  45.4 43.5 %all_to_all.25 = bf16[8,256,256]{2,1,0:T(8,128)(2,1)S(1)} all-to-all(bf16[8,256,256]{2,1,0:T(8,128)(2,1)S(1)} %broadcast_in_dim.7), channel_id=1, replica_groups=mesh['sp_0'=8,'sp_1'=8,'fs'=4,'tp'=2] {'sp_0'}, dimensions={0} | all-to-all | bytes 2097152 | tf_op jit(solution)/shard_map/all_to_all | solution.py:41
  88.8 0.0 copy-done.14
  88.8 6.7 %shard_map.186 = (bf16[8,128,128]{2,1,0:T(8,128)(2,1)}, f32[2,128,256]{2,1,0:T(8,128)S(1)}, bf16[2,128,768]{2,1,0:T(8,128)(2,1)S(1)}) custom-call(bf16[256,2048]{1,0:T(8,128)(2,1)S(1)} %get-tuple-element.16.refs_0_, bf16[2048,256]{1,0:T(8,128)(2,1)S(1)} %bitcast.19, f32[1,128]{1,0:T(1,128)S(1)} %bitcast.29, f32[3,128,256]{2,1,0:T(8,128)S(1)} %get-tuple-element.17.refs_3_), custom_call_target="tpu_custom_call" | custom-call | flops 2147483648 | bytes 2097152 | tf_op jit(solution)/shard_map/pallas_call | solution.py:102
  95.6 7.1 %all-to-all-start.2 = ((bf16[8,128,128]{2,1,0:T(8,128)(2,1)}), bf16[8,128,128]{2,1,0:T(8,128)(2,1)S(1)}, u32[]{:S(2)}, u32[]{:S(2)}) async-start(bf16[8,128,128]{2,1,0:T(8,128)(2,1)} %get-tuple-element.18), calls=%async_computation.2 | async-start | bytes 524288 | tf_op jit(solution)/shard_map/all_to_all | solution.py:482
  102.6 9.4 %all-to-all-done.2.refs_1_ = bf16[8,128,128]{2,1,0:T(8,128)(2,1)S(1)} async-done(((bf16[8,128,128]{2,1,0:T(8,128)(2,1)}), bf16[8,128,128]{2,1,0:T(8,128)(2,1)S(1)}, u32[]{:S(2)}, u32[]{:S(2)}) %all-to-all-start.2) | async-done | bytes 262176 | tf_op jit(solution)/shard_map/all_to_all | solution.py:482
  112.0 1.7 %shard_map.187 = (bf16[8,128,128]{2,1,0:T(8,128)(2,1)}, bf16[128,128]{1,0:T(8,128)(2,1)S(1)}) custom-call(s32[1]{0:T(128)} %bitcast.1.refs_0_, bf16[8,128,128]{2,1,0:T(8,128)(2,1)S(1)} %all-to-all-done.2.refs_1_), custom_call_target="tpu_custom_call" | custom-call | flops 134217728 | bytes 2097152 | tf_op jit(solution)/shard_map/pallas_call | solution.py:102
  113.8 3.4 %all-to-all-start.3 = ((bf16[8,128,128]{2,1,0:T(8,128)(2,1)}), bf16[8,128,128]{2,1,0:T(8,128)(2,1)S(1)}, u32[]{:S(2)}, u32[]{:S(2)}) async-start(bf16[8,128,128]{2,1,0:T(8,128)(2,1)} %get-tuple-element.19), calls=%async_computation.3 | async-start | bytes 524288 | tf_op jit(solution)/shard_map/all_to_all | solution.py:486
  117.2 0.0 all-gather.2.cloned.1.call-done.refs_1_.refs_6_
  117.2 0.0 copy-done.16
  117.2 0.0 copy-done.18
  117.2 0.0 copy-done.9
  117.2 0.0 copy-done.10
  117.3 0.0 copy-start.1
  117.3 1.7 %copy-done.1 = bf16[2048,640]{1,0:T(8,128)(2,1)S(1)} copy-done((bf16[2048,640]{1,0:T(8,128)(2,1)S(1)}, bf16[2048,640]{1,0:T(8,128)(2,1)}, u32[]{:S(2)}) %copy-start.1) | copy-done | bytes 2621464
  119.0 1.2 copy-done.4
  120.2 1.2 shard_map.189
  121.4 2.3 %collective-permute-start.4 = (bf16[128,128]{1,0:T(8,128)(2,1)S(1)}, bf16[128,128]{1,0:T(8,128)(2,1)S(1)}, u32[]{:S(2)}, u32[]{:S(2)}) collective-permute-start(bf16[128,128]{1,0:T(8,128)(2,1)S(1)} %slice.11), channel_id=1, source_target_pairs={{0,8},{8,16},{16,24},{24,32},{32,40},{40,48},{48,56},{56,64},{64,7... | collective-permute-start | bytes 98312 | tf_op jit(solution)/shard_map/ppermute | solution.py:36
  123.7 0.0 copy-done.2
  123.7 0.0 copy-done.13
  123.7 0.0 copy-done.17
  123.8 0.0 copy-done.19
  123.8 0.0 copy-start.15
  123.8 0.0 copy-start.11
  123.8 3.5 %shard_map.188.refs_3_ = f32[2,128,256]{2,1,0:T(8,128)S(1)} custom-call(bf16[256,2048]{1,0:T(8,128)(2,1)S(1)} %copy-done.4, bf16[2048,640]{1,0:T(8,128)(2,1)S(1)} %copy-done.2, f32[1,128]{1,0:T(1,128)S(1)} %bitcast.30, f32[3,128,256]{2,1,0:T(8,128)S(1)} %copy-done.13, f32[2,128,256]{2,1,0:T(8,128)S(1)} %copy-done.19, bf16[2,128,768]{2,1,0:T(8,128)(2,1)S(1)} %copy-done.17), custom_call_target="tpu_custom_call" | custom-call | flops 2147483648 | bytes 2097152 | tf_op jit(solution)/shard_map/pallas_call | solution.py:102
  127.3 0.0 collective-permute-done.4.refs_4_
  127.3 0.0 copy-done.15
  127.3 1.8 %shard_map.190 = (bf16[256,128]{1,0:T(8,128)(2,1)S(1)}, f32[2,256]{1,0:T(2,128)}) custom-call(s32[1]{0:T(128)} %bitcast.16.refs_0_, f32[2]{0:T(128)S(1)} %copy-done.15, bf16[256,128]{1,0:T(8,128)(2,1)S(1)} %get-tuple-element.24.refs_2_, bf16[256,128]{1,0:T(8,128)(2,1)S(1)} %get-tuple-element.25.refs_3_, bf16[128,128]{1,0:T(8,128)(2,1)S(1)} %collective-permute-done.4.refs_4_), custom_call_target="tpu_custom_call" | custom-call | flops 268435456 | bytes 2097152 | tf_op jit(solution)/shard_map/pallas_call | solution.py:102
  129.1 0.0 all-to-all-done.3.refs_1_
  129.1 2.1 %shard_map.191 = bf16[8,32,2048]{2,1,0:T(8,128)(2,1)S(1)} custom-call(s32[1]{0:T(128)} %bitcast.refs_0_, bf16[8,128,128]{2,1,0:T(8,128)(2,1)S(1)} %all-to-all-done.3.refs_1_, bf16[128,128]{1,0:T(8,128)(2,1)S(1)} %get-tuple-element.20.refs_2_, f32[2,128,256]{2,1,0:T(8,128)S(1)} %shard_map.188.refs_3_, f32[1,128]{1,0:T(1,128)S(1)} %bitcast.28, ...), custom_call_target="tpu_custom_call" | custom-call | flops 1073741824 | bytes 2097152 | tf_op jit(solution)/shard_map/pallas_call | solution.py:102
  131.2 21.4 %all_to_all.26 = bf16[8,32,2048]{2,1,0:T(8,128)(2,1)S(1)} all-to-all(bf16[8,32,2048]{2,1,0:T(8,128)(2,1)S(1)} %shard_map.191), channel_id=1, replica_groups=mesh['sp_0'=8,'sp_1'=8,'fs'=4,'tp'=2] {'fs','tp'}, dimensions={0} | all-to-all | bytes 2097152 | tf_op jit(solution)/shard_map/all_to_all | solution.py:513
  152.6 0.8 reduce_sum.12
  (14 shorter events, 0.0 us)
Async XLA Ops:
  7.2 31.5 %copy-start = (bf16[64,1024]{1,0:T(8,128)(2,1)S(1)}, bf16[64,1024]{1,0:T(8,128)(2,1)}, u32[]{:S(2)}) copy-start(bf16[64,1024]{1,0:T(8,128)(2,1)} %param.27) | copy-start | bytes 393220
  7.2 32.9 %copy-start.5 = (bf16[256,256]{1,0:T(8,128)(2,1)S(1)}, bf16[256,256]{1,0:T(8,128)(2,1)}, u32[]{:S(2)}) copy-start(bf16[256,256]{1,0:T(8,128)(2,1)} %refs_1_.2) | copy-start | bytes 393220
  7.2 32.9 %copy-start.7 = (f32[2048]{0:T(1024)S(1)}, f32[2048]{0:T(1024)}, u32[]{:S(2)}) copy-start(f32[2048]{0:T(1024)} %param.19) | copy-start | bytes 24580
  7.2 32.9 %copy-start.6 = (bf16[2048,64]{0,1:T(8,128)(2,1)S(1)}, bf16[2048,64]{0,1:T(8,128)(2,1)}, u32[]{:S(2)}) copy-start(bf16[2048,64]{0,1:T(8,128)(2,1)} %param.26) | copy-start | bytes 786436
  7.2 32.8 %copy-start.8 = (f32[2,256]{1,0:T(2,128)S(1)}, f32[2,256]{1,0:T(2,128)}, u32[]{:S(2)}) copy-start(f32[2,256]{1,0:T(2,128)} %refs_9_.1) | copy-start | bytes 6148
  9.0 33.4 %all-to-all-start = ((bf16[8,32,896]{2,1,0:T(8,128)(2,1)}), bf16[8,32,896]{2,1,0:T(8,128)(2,1)}, u32[]{:S(2)}, u32[]{:S(2)}) async-start(bf16[8,32,896]{2,1,0:T(8,128)(2,1)} %broadcast_in_dim.6), calls=%async_computation | async-start | bytes 917504 | tf_op jit(solution)/shard_map/all_to_all | solution.py:41
  16.6 100.6 %all-gather.2.cloned.1.call-start = ((), (), s32[]{:S(2)}) async-start(), calls=%async_computation.5 | async-start | bytes 2949120 | tf_op jit(solution)/shard_map/all_gather | solution.py:464
  16.7 10.0 %collective-permute-start = (bf16[256,256]{1,0:T(8,128)(2,1)}, bf16[256,256]{1,0:T(8,128)(2,1)S(1)}, u32[]{:S(2)}, u32[]{:S(2)}) collective-permute-start(bf16[256,256]{1,0:T(8,128)(2,1)} %refs_1_.2), channel_id=1, source_target_pairs={{0,2},{2,4},{4,6},{6,0},{1,3},{3,5},{5,7},{7,1},{8,10},{10,12},{12... | collective-permute-start | bytes 393224 | tf_op jit(solution)/shard_map/ppermute | solution.py:30
  19.8 6.8 %collective-permute-start.1 = (bf16[256,256]{1,0:T(8,128)(2,1)}, bf16[256,256]{1,0:T(8,128)(2,1)S(1)}, u32[]{:S(2)}, u32[]{:S(2)}) collective-permute-start(bf16[256,256]{1,0:T(8,128)(2,1)} %refs_1_.2), channel_id=1, source_target_pairs={{0,6},{2,0},{4,2},{6,4},{1,7},{3,1},{5,3},{7,5},{8,14},{10,8},{12,... | collective-permute-start | bytes 393224 | tf_op jit(solution)/shard_map/ppermute | solution.py:30
  23.2 7.4 %collective-permute-start.2 = (bf16[256,256]{1,0:T(8,128)(2,1)}, bf16[256,256]{1,0:T(8,128)(2,1)S(1)}, u32[]{:S(2)}, u32[]{:S(2)}) collective-permute-start(bf16[256,256]{1,0:T(8,128)(2,1)} %refs_1_.2), channel_id=1, source_target_pairs={{0,4},{2,6},{4,0},{6,2},{1,5},{3,7},{5,1},{7,3},{8,12},{10,14},{12... | collective-permute-start | bytes 393224 | tf_op jit(solution)/shard_map/ppermute | solution.py:30
  31.6 8.5 %collective-permute-start.3 = (bf16[4,256,256]{2,1,0:T(8,128)(2,1)S(1)}, bf16[4,256,256]{2,1,0:T(8,128)(2,1)S(1)}, u32[]{:S(2)}, u32[]{:S(2)}) collective-permute-start(bf16[4,256,256]{2,1,0:T(8,128)(2,1)S(1)} %pad_maximum_fusion), channel_id=1, source_target_pairs={{0,1},{1,0},{2,3},{3,2},{4,5},{5,4},{6,7},{7,6},{8,9},{9,8},{10,11... | collective-permute-start | bytes 1572872 | tf_op jit(solution)/shard_map/ppermute | solution.py:30
  40.1 48.8 %copy-start.14 = (f32[128]{0:T(128)S(1)}, f32[128]{0:T(128)}, u32[]{:S(2)}) copy-start(f32[128]{0:T(128)} %param.29) | copy-start | bytes 1540
  42.4 53.2 %copy-start.3 = (bf16[256,2048]{1,0:T(8,128)(2,1)}, bf16[256,2048]{1,0:T(8,128)(2,1)S(1)}, u32[]{:S(2)}) copy-start(bf16[256,2048]{1,0:T(8,128)(2,1)S(1)} %get-tuple-element.16.refs_0_) | copy-start | bytes 3145732
  42.4 53.2 %copy-start.12 = (f32[3,128,256]{2,1,0:T(8,128)}, f32[3,128,256]{2,1,0:T(8,128)S(1)}, u32[]{:S(2)}) copy-start(f32[3,128,256]{2,1,0:T(8,128)S(1)} %get-tuple-element.17.refs_3_) | copy-start | bytes 1179652
  88.8 28.4 %copy-start.9 = (f32[64]{0:T(128)S(1)}, f32[64]{0:T(128)}, u32[]{:S(2)}) copy-start(f32[64]{0:T(128)} %param.30) | copy-start | bytes 772
  88.8 28.4 %copy-start.10 = (f32[64]{0:T(128)S(1)}, f32[64]{0:T(128)}, u32[]{:S(2)}) copy-start(f32[64]{0:T(128)} %param.31) | copy-start | bytes 772
  95.5 21.7 %copy-start.16 = (bf16[2,128,768]{2,1,0:T(8,128)(2,1)}, bf16[2,128,768]{2,1,0:T(8,128)(2,1)S(1)}, u32[]{:S(2)}) copy-start(bf16[2,128,768]{2,1,0:T(8,128)(2,1)S(1)} %get-tuple-element.23.refs_5_) | copy-start | bytes 1179652
  95.6 21.7 %copy-start.18 = (f32[2,128,256]{2,1,0:T(8,128)}, f32[2,128,256]{2,1,0:T(8,128)S(1)}, u32[]{:S(2)}) copy-start(f32[2,128,256]{2,1,0:T(8,128)S(1)} %get-tuple-element.22.refs_4_) | copy-start | bytes 786436
  95.6 16.5 %all-to-all-start.2 = ((bf16[8,128,128]{2,1,0:T(8,128)(2,1)}), bf16[8,128,128]{2,1,0:T(8,128)(2,1)S(1)}, u32[]{:S(2)}, u32[]{:S(2)}) async-start(bf16[8,128,128]{2,1,0:T(8,128)(2,1)} %get-tuple-element.18), calls=%async_computation.2 | async-start | bytes 524288 | tf_op jit(solution)/shard_map/all_to_all | solution.py:482
  113.8 15.4 %all-to-all-start.3 = ((bf16[8,128,128]{2,1,0:T(8,128)(2,1)}), bf16[8,128,128]{2,1,0:T(8,128)(2,1)S(1)}, u32[]{:S(2)}, u32[]{:S(2)}) async-start(bf16[8,128,128]{2,1,0:T(8,128)(2,1)} %get-tuple-element.19), calls=%async_computation.3 | async-start | bytes 524288 | tf_op jit(solution)/shard_map/all_to_all | solution.py:486
  117.3 1.7 %copy-start.1 = (bf16[2048,640]{1,0:T(8,128)(2,1)S(1)}, bf16[2048,640]{1,0:T(8,128)(2,1)}, u32[]{:S(2)}) copy-start(bf16[2048,640]{1,0:T(8,128)(2,1)} %all-gather.2.cloned.1.call-done.refs_1_.refs_6_) | copy-start | bytes 7864324
  119.0 1.2 copy-start.4
  120.2 3.5 %copy-start.2 = (bf16[2048,640]{1,0:T(8,128)(2,1)S(1)}, bf16[2048,640]{1,0:T(8,128)(2,1)}, u32[]{:S(2)}) copy-start(bf16[2048,640]{1,0:T(8,128)(2,1)} %all-gather.2.cloned.1.call-done.refs_1_.refs_6_) | copy-start | bytes 7864324
  120.2 3.5 %copy-start.13 = (f32[3,128,256]{2,1,0:T(8,128)S(1)}, f32[3,128,256]{2,1,0:T(8,128)}, u32[]{:S(2)}) copy-start(f32[3,128,256]{2,1,0:T(8,128)} %copy-done.12) | copy-start | bytes 1179652
  120.2 3.5 %copy-start.17 = (bf16[2,128,768]{2,1,0:T(8,128)(2,1)S(1)}, bf16[2,128,768]{2,1,0:T(8,128)(2,1)}, u32[]{:S(2)}) copy-start(bf16[2,128,768]{2,1,0:T(8,128)(2,1)} %copy-done.16) | copy-start | bytes 1179652
  120.2 3.5 %copy-start.19 = (f32[2,128,256]{2,1,0:T(8,128)S(1)}, f32[2,128,256]{2,1,0:T(8,128)}, u32[]{:S(2)}) copy-start(f32[2,128,256]{2,1,0:T(8,128)} %copy-done.18) | copy-start | bytes 786436
  121.4 5.9 %collective-permute-start.4 = (bf16[128,128]{1,0:T(8,128)(2,1)S(1)}, bf16[128,128]{1,0:T(8,128)(2,1)S(1)}, u32[]{:S(2)}, u32[]{:S(2)}) collective-permute-start(bf16[128,128]{1,0:T(8,128)(2,1)S(1)} %slice.11), channel_id=1, source_target_pairs={{0,8},{8,16},{16,24},{24,32},{32,40},{40,48},{48,56},{56,64},{64,7... | collective-permute-start | bytes 98312 | tf_op jit(solution)/shard_map/ppermute | solution.py:36
  123.8 3.6 %copy-start.15 = (f32[2]{0:T(128)S(1)}, f32[2]{0:T(128)}, u32[]{:S(2)}) copy-start(f32[2]{0:T(128)} %refs_1_.3) | copy-start | bytes 28
  123.8 5.3 %copy-start.11 = (f32[128]{0:T(128)S(1)}, f32[128]{0:T(128)}, u32[]{:S(2)}) copy-start(f32[128]{0:T(128)} %param.33) | copy-start | bytes 1540
Sparse Core Ops, SparseCore 0:
  44.5 59.7 all-gather.1

commit v3 on v2

--- a/solution.py
+++ b/solution.py
@@ -11,6 +11,7 @@
 HEAD = 64
 WINDOW = 128
 CHUNK = 32
+HALF = 16
 SP = ("sp_0", "sp_1")
 SP_FS_TP = ("sp_0", "sp_1", "fs", "tp")
 F32 = jnp.float32
@@ -70,7 +71,7 @@
         for i in sorted(far):
             rows, width = args[i].shape[-2:]
             if far[i] is not None:
-                width = far[i][0]
+                _, rows, _, width = far[i]
             held.append(pltpu.VMEM((*args[i].shape[:-2], rows, width), args[i].dtype))
         held += [pltpu.VMEM(*outs[i]) for i in far_out]
         ins = [
@@ -87,8 +88,7 @@
             for k, i in enumerate(sorted(far)):
                 source = refs[i]
                 if far[i] is not None:
-                    width, block = far[i]
-                    source = source.at[:, pl.ds(width * block, width)]
+                    source = source.at[pl.ds(*far[i][:2]), pl.ds(*far[i][2:])]
                 refs[i] = Fetched(source, extra[k], sems.at[k])
             stored = []
             for k, i in enumerate(far_out):
@@ -99,9 +99,16 @@
             for one in stored:
                 one.copy.wait()
 
+        args = [
+            pltpu.with_memory_space_constraint(a, pltpu.HBM) if i in far else a
+            for i, a in enumerate(args)
+        ]
         return pl.pallas_call(
             body,
-            out_shape=[jax.ShapeDtypeStruct(s, d) for s, d in outs],
+            out_shape=[
+                pltpu.HBM(*o) if i in far_out else jax.ShapeDtypeStruct(*o)
+                for i, o in enumerate(outs)
+            ],
             in_specs=ins,
             out_specs=[
                 pl.BlockSpec(memory_space=pltpu.HBM if i in far_out else pltpu.VMEM)
@@ -117,6 +124,18 @@
 
 def dot(a, b, dims=(((1,), (0,)), ((), ()))):
     return lax.dot_general(a.astype(BF16), b.astype(BF16), dims, preferred_element_type=F32)
+
+
+def running_sums(x, size):
+    rows = x.shape[1]
+    lane = lax.broadcasted_iota(jnp.int32, x.shape, 1) % size
+    total, after = x, x
+    step = 1
+    while step < size:
+        total = total + jnp.where(lane >= step, pltpu.roll(total, step, 1), 0.0)
+        after = after + jnp.where(lane < size - step, pltpu.roll(after, rows - step, 1), 0.0)
+        step *= 2
+    return total, after
 
 
 def hidden_kernel(place, own, next_, before, across, other, gain, down, up, base, hid, decays):
@@ -140,23 +159,18 @@
             hid.ref[:, pl.ds(at, width)] = h
             low += lax.dot_general(h, down[:, pl.ds(at, width)], NT, preferred_element_type=F32)
     hid.put()
-    low = jnp.tanh(low).astype(BF16)
+    low = jnp.tanh(low[WINDOW:, :]).astype(BF16)
     rate = lax.dot_general(up[...], low, (((0,), (1,)), ((), ())), preferred_element_type=F32)
     heads = base.shape[0]
     base_rows = jnp.concatenate(
-        [jnp.broadcast_to(base[h : h + 1, :], (HEAD, rows)) for h in range(heads)], axis=0
+        [jnp.broadcast_to(base[h : h + 1, :], (HEAD, base.shape[1])) for h in range(heads)], axis=0
     )
     log_decay = jnp.maximum(-jnp.exp(rate + base_rows), DECAY_FLOOR)
-    lane = lax.broadcasted_iota(jnp.int32, log_decay.shape, 1) % CHUNK
-    total, after = log_decay, log_decay
-    step = 1
-    while step < CHUNK:
-        total = total + jnp.where(lane >= step, pltpu.roll(total, step, 1), 0.0)
-        after = after + jnp.where(lane < CHUNK - step, pltpu.roll(after, rows - step, 1), 0.0)
-        step *= 2
-    decays.ref[0] = total
-    decays.ref[1] = total - log_decay
-    decays.ref[2] = after - log_decay
+    for k, size in enumerate((CHUNK, HALF)):
+        total, after = running_sums(log_decay, size)
+        decays.ref[3 * k] = total
+        decays.ref[3 * k + 1] = total - log_decay
+        decays.ref[3 * k + 2] = after - log_decay
     decays.put()
 
 
@@ -168,12 +182,15 @@
     return slice(h * HEAD, (h + 1) * HEAD)
 
 
-def band_tables(left, right, start, end, rate, first, heads):
+def pair_tables(left, right, start, end, near_start, near_end, rate, first, heads):
     rows = left.shape[1]
-    dist = (
-        lax.broadcasted_iota(jnp.int32, (CHUNK, rows), 1) % CHUNK
-        - lax.broadcasted_iota(jnp.int32, (CHUNK, rows), 0)
-    )
+    at_j = lax.broadcasted_iota(jnp.int32, (CHUNK, rows), 0)
+    at_i = lax.broadcasted_iota(jnp.int32, (CHUNK, rows), 1) % CHUNK
+    dist = jnp.where(at_i // HALF == at_j // HALF, at_i - at_j, -1)
+    all_j = lax.broadcasted_iota(jnp.int32, (rows, rows), 0)
+    all_i = lax.broadcasted_iota(jnp.int32, (rows, rows), 1)
+    same = all_i // CHUNK == all_j // CHUNK
+    across = same & (all_i // HALF > all_j // HALF)
     plain, rated = [], []
     for h in range(heads):
         sl = head_rows(h)
@@ -181,26 +198,20 @@
         speed = jnp.broadcast_to(rate[sl, :], l.shape)
         t_plain = jnp.zeros((CHUNK, rows), F32)
         t_rated = jnp.zeros((CHUNK, rows), F32)
-        for d in range(first, CHUNK):
+        for d in range(first, HALF):
             rd = r if d == 0 else pltpu.roll(r, d, 1)
             ed = e if d == 0 else pltpu.roll(e, d, 1)
             x = l * rd * jnp.exp(s - ed)
             here = dist == d
             t_plain = jnp.where(here, jnp.sum(x, axis=0, keepdims=True), t_plain)
             t_rated = jnp.where(here, jnp.sum(x * speed, axis=0, keepdims=True), t_rated)
-        plain.append(t_plain)
-        rated.append(t_rated)
+        later = l * jnp.exp(near_start[sl, :])
+        earlier = r * jnp.exp(near_end[sl, :])
+        for table, weight, out in ((t_plain, earlier, plain), (t_rated, earlier * speed, rated)):
+            far = dot(weight, later, TN)
+            tall = jnp.concatenate([table] * (rows // CHUNK), axis=0)
+            out.append(jnp.where(across, far, jnp.where(same, tall, 0.0)).astype(BF16))
     return plain, rated
-
-
-def in_chunks(table):
-    rows = table.shape[1]
-    tall = jnp.concatenate([table] * (rows // CHUNK), axis=0)
-    same = (
-        lax.broadcasted_iota(jnp.int32, (rows, rows), 0) // CHUNK
-        == lax.broadcasted_iota(jnp.int32, (rows, rows), 1) // CHUNK
-    )
-    return jnp.where(same, tall, 0.0).astype(BF16)
 
 
 def by_chunk(array):
@@ -211,11 +222,30 @@
     )
 
 
-def state_kernel(hid, w, lr, decays, ends, units, tables, dec):
+def spread(row):
+    eye = (
+        lax.broadcasted_iota(jnp.int32, (HEAD, HEAD), 0)
+        == lax.broadcasted_iota(jnp.int32, (HEAD, HEAD), 1)
+    )
+    return jnp.where(eye, row, 0.0)
+
+
+def followed(state, kept, change, added):
+    low = state.astype(BF16)
+    new = state * kept + jnp.dot(low, change.astype(BF16), preferred_element_type=F32)
+    return new + jnp.concatenate([jnp.zeros((HEAD, HEAD), F32), added], axis=0)
+
+
+def kept_by(decays, c, h):
+    last = c * CHUNK + CHUNK - 1
+    return decays[last : last + 1, head_rows(h)]
+
+
+def state_kernel(hid, w, lr, decays, ends, units, tables, changes, adds, dec):
     rows = dec.shape[0]
-    heads = lr.shape[1] // HEAD
-    span = heads * HEAD
-    lr = as_column(lr[...])
+    lr = as_column(lr.get()[...])
+    span = lr.shape[0]
+    heads = span // HEAD
     hid, decays = hid.get(), decays.get()
     kv = jnp.dot(hid[...], w[...], preferred_element_type=F32).astype(BF16).astype(F32)
     kv_t = kv.T
@@ -225,18 +255,17 @@
         inv = lax.rsqrt(square)
         units.ref[0, head_rows(h), :] = k * inv
         units.ref[1, head_rows(h), :] = kv_t[span + h * HEAD : span + (h + 1) * HEAD, :] * (square * inv)
-    cum_all = decays[0]
-    prev = decays[1]
-    dec[...] = jnp.exp(cum_all).T
+    cum, prev = decays[0], decays[1]
+    dec[...] = jnp.exp(cum).T
     u = units.ref[0]
     v = units.ref[1]
-    plain, rated = band_tables(u, u, prev, cum_all, lr, 1, heads)
+    plain, rated = pair_tables(u, u, prev, cum, decays[4], decays[5], lr, 1, heads)
     reach = jnp.exp(prev)
     x, q = [], []
     for h in range(heads):
         sl = head_rows(h)
-        x.append(jnp.concatenate([-u[sl, :] * reach[sl, :], -dot(v[sl, :], in_chunks(plain[h]))], axis=0))
-        q.append(in_chunks(-rated[h]))
+        x.append(jnp.concatenate([-u[sl, :] * reach[sl, :], -dot(v[sl, :], plain[h])], axis=0))
+        q.append(-rated[h])
     units.put()
     power = 1
     while power < CHUNK:
@@ -248,53 +277,63 @@
                 q[h] = dot(q[h], q[h]).astype(BF16)
     left = jnp.exp(decays[2])
     chunks = rows // CHUNK
-    grow = []
     for h in range(heads):
         sl = head_rows(h)
-        tables.ref[h, :, :rows] = x[h].astype(BF16)
+        tables.ref[h] = x[h].astype(BF16)
         out_u = u[sl, :] * left[sl, :]
         out_b = out_u * lr[sl, :]
         g = dot(x[h], by_chunk(out_b), NT)
-        g_low = g[HEAD:, :] + dot(v[sl, :], by_chunk(out_u), NT)
-        grow.append((g[:HEAD, :].astype(BF16), g_low))
-    eye = (
-        lax.broadcasted_iota(jnp.int32, (2 * HEAD, HEAD), 0)
-        == lax.broadcasted_iota(jnp.int32, (2 * HEAD, HEAD), 1)
-    ).astype(F32)
-    state = [eye] * heads
-    zero = jnp.zeros((HEAD, HEAD), F32)
-    for c in range(chunks):
-        at = slice(c * HEAD, (c + 1) * HEAD)
-        last = c * CHUNK + CHUNK - 1
-        for h in range(heads):
-            low = state[h].astype(BF16)
-            tables.ref[h, :, rows + c * HEAD : rows + (c + 1) * HEAD] = low
-            kept = state[h] * dec[last : last + 1, head_rows(h)]
-            added = jnp.concatenate([zero, grow[h][1][:, at]], axis=0)
-            state[h] = kept + added + jnp.dot(low, grow[h][0][:, at], preferred_element_type=F32)
-    packed = jnp.concatenate(state, axis=1).astype(BF16)
+        changes.ref[h] = g[:HEAD, :].astype(BF16)
+        adds.ref[h] = g[HEAD:, :] + dot(v[sl, :], by_chunk(out_u), NT)
+    parts = []
+    for h in range(heads):
+        for c in range(chunks):
+            at = slice(c * HEAD, (c + 1) * HEAD)
+            parts.append((h, kept_by(dec, c, h), changes.ref[h, :, at].astype(F32), adds.ref[h, :, at]))
+    tables.put()
+    changes.put()
+    adds.put()
+    while len(parts) > heads:
+        joined = []
+        for (h, kept, change, added), (_, kept2, change2, added2) in zip(parts[::2], parts[1::2]):
+            both = jnp.concatenate([change + spread(kept), added], axis=0)
+            both = followed(both, kept2, change2, added2)
+            kept = kept * kept2
+            joined.append((h, kept, both[:HEAD, :] - spread(kept), both[HEAD:, :]))
+        parts = joined
+    packed = jnp.concatenate(
+        [jnp.concatenate([change + spread(kept), added], axis=0) for _, kept, change, added in parts],
+        axis=1,
+    ).astype(BF16)
     for k in range(ends.shape[0]):
         ends[k] = packed
-    tables.put()
-
-
-def read_kernel(hid, w, lr, decays, units, tables, out):
-    heads = lr.shape[1] // HEAD
-    lr = as_column(lr[...])
-    hid, w, decays, units = hid.get(), w.get(), decays.get(), units.get()
-    rows = hid.shape[0]
-    reads = jnp.dot(hid[...], w[...], preferred_element_type=F32).astype(BF16).astype(F32)
+
+
+def read_part(reads, lr, decays, units, tables, changes, adds, out):
+    rows = reads.shape[0]
+    heads = lr.shape[0] // HEAD
     r = reads.T
-    cum_all = decays[0]
-    plain, rated = band_tables(r, units[0], cum_all, cum_all, lr, 0, heads)
-    reach = r * jnp.exp(cum_all)
-    tables = tables.get()
+    cum = decays[0]
+    reach = jnp.exp(cum)
+    dec = reach.T
+    eye = jnp.concatenate([spread(jnp.ones((1, HEAD), F32)), jnp.zeros((HEAD, HEAD), F32)], axis=0)
+    starts = [[eye] for _ in range(heads)]
+    for c in range(rows // CHUNK - 1):
+        at = slice(c * HEAD, (c + 1) * HEAD)
+        for h in range(heads):
+            starts[h].append(
+                followed(starts[h][-1], kept_by(dec, c, h), changes[h, :, at], adds[h, :, at])
+            )
+    near = decays[3]
+    plain, rated = pair_tables(r, units[0], cum, cum, near, decays[5], lr, 0, heads)
+    reach = r * reach
     for h in range(heads):
         sl = head_rows(h)
-        mixed = dot(tables[h, :, :rows], in_chunks(rated[h]))
+        mixed = dot(tables[h], rated[h])
         query = mixed[:HEAD, :] + reach[sl, :]
-        local = mixed[HEAD:, :] + dot(units[1, sl, :], in_chunks(plain[h]))
-        both = dot(tables[h, :, rows:], by_chunk(query))
+        local = mixed[HEAD:, :] + dot(units[1, sl, :], plain[h])
+        start = jnp.concatenate([x.astype(BF16) for x in starts[h]], axis=1)
+        both = dot(start, by_chunk(query))
         out.ref[h, :HEAD, :] = both[:HEAD, :]
         out.ref[h, HEAD:, :] = both[HEAD:, :] + local
     out.put()
@@ -335,7 +374,7 @@
             new = jnp.dot(state[h].astype(BF16), later[:HEAD, :], preferred_element_type=F32)
             state[h] = jnp.where(passed, new + later[HEAD:, :].astype(F32), state[h])
     rows = []
-    gain = as_column(gain[...])
+    gain = as_column(gain.get()[...])
     inside, local = inside.get(), local.get()
     for h in range(heads):
         near = inside[:, head_rows(h)]
@@ -354,7 +393,7 @@
         at = slice(n * width, (n + 1) * width)
         part = lax.dot_general(mix, w[at, :], NT, preferred_element_type=F32).astype(BF16)
         for g in range(groups):
-            out[g, :, at] = part[g * size : (g + 1) * size, :]
+            out[g % 2 * (groups // 2) + g // 2, :, at] = part[g * size : (g + 1) * size, :]
 
 
 def head_rms(values, gain):
@@ -366,35 +405,19 @@
     return heads
 
 
-def attention_in_kernel(hid, w, query_gain, key_gain, queries, keys_values):
-    q_w, kv_w = queries.shape[1], keys_values.shape[1] // 2
-    hid, w = hid.get(), w.get()
-    rows = jnp.dot(hid[...], w[...], preferred_element_type=F32).astype(BF16)
-    normed = head_rms(rows[:, :q_w].astype(F32), query_gain[...])
-    queries[...] = jnp.concatenate(normed, axis=1)
-    normed = head_rms(rows[:, q_w : q_w + kv_w].astype(F32), key_gain[...])
-    keys_values[...] = jnp.concatenate(normed + [rows[:, q_w + kv_w :]], axis=1)
-
-
-def attention_kernel(place, sink, queries, keys_values, before, out, lse):
-    rows = queries.shape[0]
-    heads = queries.shape[1] // HEAD
+def attention_part(at_start, sink, queries, keys, values, out, lse):
     shape = (2 * WINDOW, WINDOW)
     key_at = lax.broadcasted_iota(jnp.int32, shape, 0)
     lag = lax.broadcasted_iota(jnp.int32, shape, 1) + WINDOW - key_at
     near = (lag >= 0) & (lag < WINDOW)
-    for n in range(rows // WINDOW):
+    for n in range(queries[0].shape[0] // WINDOW):
         at = slice(n * WINDOW, (n + 1) * WINDOW)
-        if n == 0:
-            band = jnp.concatenate([before[...], keys_values[at, :]], axis=0)
-            allowed = near & ((key_at >= WINDOW) | (place[0] > 0))
-        else:
-            band = keys_values[(n - 1) * WINDOW : (n + 1) * WINDOW, :]
-            allowed = near
+        band = slice(n * WINDOW, (n + 2) * WINDOW)
+        allowed = near & ((key_at >= WINDOW) | jnp.logical_not(at_start)) if n == 0 else near
         tiles = []
-        for h in range(heads):
+        for h, query in enumerate(queries):
             score = lax.dot_general(
-                band[:, :HEAD], queries[at, head_rows(h)], NT, preferred_element_type=F32
+                keys[band, :], query[at, :], NT, preferred_element_type=F32
             ) * (1.0 / math.sqrt(HEAD))
             score = jnp.where(allowed, score, -jnp.inf)
             top = jnp.maximum(jnp.max(score, axis=0, keepdims=True), sink[h])
@@ -402,9 +425,24 @@
             total = jnp.sum(weight, axis=0, keepdims=True) + jnp.exp(sink[h] - top)
             lse[h : h + 1, at] = top + jnp.log(total)
             probs = (weight / total).astype(BF16)
-            mixed = lax.dot_general(probs, band[:, HEAD:], TN, preferred_element_type=F32)
+            mixed = lax.dot_general(probs, values[band, :], TN, preferred_element_type=F32)
             tiles.append(mixed.astype(BF16))
-        out[at, :] = jnp.concatenate(tiles, axis=1)
+        out.ref[at, :] = jnp.concatenate(tiles, axis=1)
+    out.put()
+
+
+def late_kernel(place, sink, hid, w, query_gain, key_gain, lr, decays, units, tables, changes, adds, local, mix, lse):
+    q_w = mix.ref.shape[1]
+    lr = as_column(lr.get()[...])
+    hid, w = hid.get(), w.get()
+    both = jnp.dot(hid[...], w[...], preferred_element_type=F32).astype(BF16)
+    own = both[WINDOW:, :]
+    whole = own.shape[1] - lr.shape[0]
+    made = [ref.get() for ref in (decays, units, tables, changes, adds)]
+    read_part(own[:, whole:].astype(F32), lr, *made, local)
+    queries = head_rms(own[:, :q_w].astype(F32), query_gain[...])
+    (keys,) = head_rms(both[:, q_w : q_w + HEAD].astype(F32), key_gain[...])
+    attention_part(place[0] == 0, sink, queries, keys, both[:, q_w + HEAD : whole], mix, lse)
 
 
 def per_device(
@@ -435,13 +473,17 @@
     place_zy = [lax.axis_index(a).astype(jnp.int32).reshape(1) for a in SP]
 
     own = jnp.concatenate(
-        [rec_key_w, rec_value_w, query_w, key_w, value_w, out_att_w.T, out_rec_w.T, recept_w], axis=1
+        [rec_key_w, rec_value_w, query_w, key_w, value_w, recept_w, out_att_w.T, out_rec_w.T], axis=1
     )
     column = from_everyone(own, "sp_1").reshape(-1, own.shape[1])
     state_w = from_everyone(column[:, : 2 * span], "sp_0").reshape(features, 2 * span)
+    ahead = passed_along(tokens[rows - WINDOW :], SP, 1)
+    tokens = jnp.concatenate([ahead, tokens], axis=0)
     before = ring_shift(tokens, "fs", -1)
     across = ring_shift(tokens, "fs", 2)
     next_ = ring_shift(tokens, "fs", 1)
+    held, before = lax.optimization_barrier((column[:, 2 * span :], before))
+    other_w = lax.all_gather(held, "sp_0", axis=0, tiled=True)
     other = ring_shift(jnp.stack([tokens, before, across, next_]), "tp", 1)
 
 
@@ -451,32 +493,28 @@
     )
     flat = (span, rows)
     hid, decays = call(
-        hidden_kernel,
-        [((rows, features), BF16), ((3, *flat), F32)],
-        smem=1,
-        flops=1 << 27,
-        far_out=(0, 1),
+        hidden_kernel, [((WINDOW + rows, features), BF16), ((6, *flat), F32)], smem=1, flops=1 << 27, far_out=(0, 1)
     )(
         place_xc, tokens, next_, before, across, other, norm_gain.reshape(1, -1), decay_down.T, decay_cols, decay_base
     )
 
-    held, hid = lax.optimization_barrier((column[:, 2 * span :], hid))
-    other_w = lax.all_gather(held, "sp_0", axis=0, tiled=True)
 
     lr = learn_rate.reshape(1, span)
     chunks = rows // CHUNK
     pair = (2 * HEAD, span)
-    ends, units, tables = call(
+    ends, *made = call(
         state_kernel,
         [
             ((lax.axis_size("sp_1"), *pair), BF16),
             ((2, *flat), F32),
-            ((heads, 2 * HEAD, rows + chunks * HEAD), BF16),
+            ((heads, 2 * HEAD, rows), BF16),
+            ((heads, HEAD, chunks * HEAD), BF16),
+            ((heads, HEAD, chunks * HEAD), F32),
         ],
         scratch=[pltpu.VMEM((rows, span), F32)],
         flops=1 << 31,
-        far={0: None, 3: None},
-        far_out=(1, 2),
+        far={0: (WINDOW, rows, 0, features), 2: None, 3: None},
+        far_out=(1, 2, 3, 4),
     )(hid, state_w, lr, decays)
 
     row_pieces = lax.all_to_all(ends, "sp_1", 0, 0, tiled=True)
@@ -486,31 +524,30 @@
     all_pieces = lax.all_to_all(row_total, "sp_0", 0, 0, tiled=True)
 
     q_w, kv_w = query_w.shape[1], key_w.shape[1]
-    whole = q_w + 2 * kv_w
-    (local,) = call(
-        read_kernel, [((heads, 2 * HEAD, rows), F32)], flops=1 << 31,
-        far={0: None, 1: (span, 2 * whole // span), 3: None, 4: None, 5: None}, far_out=(0,),
-    )(hid, other_w, lr, decays, units, tables)
-    queries, keys_values = call(
-        attention_in_kernel,
-        [((rows, q_w), BF16), ((rows, 2 * kv_w), BF16)],
-        flops=1 << 28,
-        far={0: None, 1: (whole, 0)},
-    )(hid, other_w, query_gain.reshape(1, HEAD), key_gain.reshape(1, HEAD))
-    before_keys = passed_along(keys_values[rows - WINDOW :], SP, 1)
+    early = q_w + 2 * kv_w + span
     place_sp = lax.axis_index(SP).astype(jnp.int32).reshape(1)
-    att_mix, row_lse = call(
-        attention_kernel, [((rows, q_w), BF16), ((q_w // HEAD, rows), F32)], smem=2, flops=1 << 28
-    )(place_sp, sink_logit, queries, keys_values, before_keys)
+    local, att_mix, row_lse = call(
+        late_kernel,
+        [((heads, 2 * HEAD, rows), F32), ((rows, q_w), BF16), ((q_w // HEAD, rows), F32)],
+        smem=2,
+        flops=1 << 31,
+        far={2: None, 3: (0, features, 0, early), **{i: None for i in range(6, 12)}},
+        far_out=(0, 1),
+    )(
+        place_sp, sink_logit, hid, other_w, query_gain.reshape(1, HEAD), key_gain.reshape(1, HEAD),
+        lr, decays, *made,
+    )
 
     (partial,) = call(
         final_kernel,
         [((groups, rows // groups, features), BF16)],
         smem=1,
         flops=1 << 30,
-        far={2: None, 3: None, 5: None, 6: (whole, 1)},
+        far={2: None, 3: None, 4: None, 5: None, 6: (0, features, early, q_w + span)},
     )(place_zy[0], all_pieces, inside, local, group_gain.reshape(1, span), att_mix, other_w)
-    tiles = lax.all_to_all(partial, ("fs", "tp"), 0, 0, tiled=True)
+    tiles = lax.all_to_all(partial, "tp", 0, 0, tiled=True).reshape(2, groups // 2, -1, features)
+    tiles = jnp.sum(tiles.astype(F32), axis=0).astype(BF16)
+    tiles = lax.all_to_all(tiles, "fs", 0, 0, tiled=True)
     mixed = jnp.sum(tiles.astype(F32), axis=0).astype(BF16)
     return (mixed, row_lse)
 
@@ -541,6 +578,4 @@
     )
     out_specs = (P(SP_FS_TP, None), P(("fs", "tp"), SP))
 
-    return jax.shard_map(
-        per_device, mesh=split, in_specs=in_specs, out_specs=out_specs, check_vma=False
-    )
+    return jax.shard_map(per_device, mesh=split, in_specs=in_specs, out_specs=out_specs, check_vma=False)

time: 162 us -> 158 us (0.975)
  blocking collectives: 64.9 us -> 21.5 us
  starting transfers between devices: 37.4 us -> 60.5 us
  waiting for transfers between devices: 14.8 us -> 30.8 us
  Pallas kernels: 19.2 us -> 21.7 us
  local copies, waits for them, and re-layouts: 7.77 us -> 5.99 us
    all_to_all x2, blocking collectives: 64.9 us -> 21.5 us  [the longest x1 13.8 us: per_device(): tiles = lax.all_to_all(tiles, 'fs', 0, 0, tiled=True)]
    all_to_all x1 -> x2, starting transfers between devices: 7.64 us -> 20.9 us  [from_everyone(): return lax.all_to_all(copies, axis, split_axis=0, concat_axis=0, tiled=True)]
    all_to_all x1 -> x2, waiting for transfers between devices: 0.01 us -> 8.84 us  [from_everyone(): return lax.all_to_all(copies, axis, split_axis=0, concat_axis=0, tiled=True)]
    all_to_all x1, starting transfers between devices: 7.06 us -> 11.9 us  [per_device(): row_pieces = lax.all_to_all(ends, 'sp_1', 0, 0, tiled=True)]
    ppermute x4, starting transfers between devices: 16.9 us -> 21.1 us  [ring_shift(): lax.ppermute(array, axis, [(i, (i + by) % devices) for i in range(devices)])]
    pallas_call x7 -> x5, Pallas kernels: 19.2 us -> 21.7 us  [run(): pl.pallas_call(body, out_shape=[pltpu.HBM(*o) if i in far_out else jax.Sh...]
    ppermute x4, waiting for transfers between devices: 5.38 us -> 7.89 us  [ring_shift(): lax.ppermute(array, axis, [(i, (i + by) % devices) for i in range(devices)])]
    unnamed x40 -> x17, local copies, waits for them, and re-layouts: 3.04 us -> 0.65 us
  transfers between devices with their start and end apart: 9 -> 10, of which waited for: 3 -> 7; matrix products, arithmetic and copies ran while one was open for 1% -> 3% of each run, Pallas kernels for 11% -> 12%
where the time goes in v3:
time: 158 us; the launch traced here: 157 us
  starting transfers between devices  60.5 us (38%)
  waiting for transfers between devices  30.8 us (19%)
  Pallas kernels  21.7 us (14%)
  blocking collectives  21.5 us (14%)
  between operations  14.3 us (9%)
  local copies, waits for them, and re-layouts  5.99 us (4%)
  other arithmetic  2.11 us (1%)
    pallas_call x5, Pallas kernels, run(): pl.pallas_call(body, out_shape=[pltpu.HBM(*o) if i in far_out else jax.Sh...  21.7 us
    ppermute x4, starting transfers between devices, ring_shift(): lax.ppermute(array, axis, [(i, (i + by) % devices) for i in range(devices)])  21.1 us
    all_to_all x2, starting transfers between devices, from_everyone(): return lax.all_to_all(copies, axis, split_axis=0, concat_axis=0, tiled=True)  20.9 us
    all_to_all x1, blocking collectives, per_device(): tiles = lax.all_to_all(tiles, 'fs', 0, 0, tiled=True)  13.8 us
    all_to_all x1, starting transfers between devices, per_device(): row_pieces = lax.all_to_all(ends, 'sp_1', 0, 0, tiled=True)  11.9 us
    all_to_all x1, waiting for transfers between devices, per_device(): row_pieces = lax.all_to_all(ends, 'sp_1', 0, 0, tiled=True)  10.4 us
    all_to_all x2, waiting for transfers between devices, from_everyone(): return lax.all_to_all(copies, axis, split_axis=0, concat_axis=0, tiled=True)  8.84 us
    ppermute x4, waiting for transfers between devices, ring_shift(): lax.ppermute(array, axis, [(i, (i + by) % devices) for i in range(devices)])  7.89 us
  transfers between devices with their start and end apart: 10, of which 7 were waited for; matrix products, arithmetic and copies ran while one was open for 3% of the time, Pallas kernels for 12%

profile of v3, /device:TPU:1, one launch (start us, length us, event | category | flops | bytes accessed | tf_op | source)
XLA Modules:
  0.0 157.0 jit_solution(7833538161036104864)
XLA Ops:
  7.2 0.0 copy-start
  7.2 0.9 concatenate.7
  8.1 0.8 broadcast_in_dim.6
  8.9 7.6 %all-to-all-start = ((bf16[8,32,896]{2,1,0:T(8,128)(2,1)}), bf16[8,32,896]{2,1,0:T(8,128)(2,1)S(1)}, u32[]{:S(2)}, u32[]{:S(2)}) async-start(bf16[8,32,896]{2,1,0:T(8,128)(2,1)} %broadcast_in_dim.6), calls=%async_computation | async-start | bytes 917504 | tf_op jit(solution)/shard_map/all_to_all | solution.py:42
  16.6 0.0 all-gather.2.cloned.1.call-start
  16.6 0.8 slice.9
  17.5 3.3 %collective-permute-start = (bf16[128,256]{1,0:T(8,128)(2,1)S(1)}, bf16[128,256]{1,0:T(8,128)(2,1)S(1)}, u32[]{:S(2)}, u32[]{:S(2)}) collective-permute-start(bf16[128,256]{1,0:T(8,128)(2,1)S(1)} %slice.9), channel_id=1, source_target_pairs={{0,8},{8,16},{16,24},{24,32},{32,40},{40,48},{48,56},{56,64},{64,7... | collective-permute-start | bytes 196616 | tf_op jit(solution)/shard_map/ppermute | solution.py:37
  20.8 2.2 %collective-permute-done = bf16[128,256]{1,0:T(8,128)(2,1)S(1)} collective-permute-done((bf16[128,256]{1,0:T(8,128)(2,1)S(1)}, bf16[128,256]{1,0:T(8,128)(2,1)S(1)}, u32[]{:S(2)}, u32[]{:S(2)}) %collective-permute-start) | collective-permute-done | bytes 65568 | tf_op jit(solution)/shard_map/ppermute | solution.py:37
  23.0 0.9 constant_dynamic-update-slice_fusion.refs_1_
  23.9 7.0 %collective-permute-start.2 = (bf16[384,256]{1,0:T(8,128)(2,1)S(1)}, bf16[384,256]{1,0:T(8,128)(2,1)S(1)}, u32[]{:S(2)}, u32[]{:S(2)}) collective-permute-start(bf16[384,256]{1,0:T(8,128)(2,1)S(1)} %constant_dynamic-update-slice_fusion.refs_1_), channel_id=1, source_target_pairs={{0,6},{2,0},{4,2},{6,4},{1,7},{3,1},{5,3},{7,5},{8,14},{10,8},{12,... | collective-permute-start | bytes 589832 | tf_op jit(solution)/shard_map/ppermute | solution.py:31
  30.9 0.0 all-to-all-done
  30.9 0.8 slice.12
  31.7 1.8 %collective-permute-done.2.refs_3_ = bf16[384,256]{1,0:T(8,128)(2,1)S(1)} collective-permute-done((bf16[384,256]{1,0:T(8,128)(2,1)S(1)}, bf16[384,256]{1,0:T(8,128)(2,1)S(1)}, u32[]{:S(2)}, u32[]{:S(2)}) %collective-permute-start.2) | collective-permute-done | bytes 196640 | tf_op jit(solution)/shard_map/ppermute | solution.py:31
  33.5 0.0 all-gather.2.cloned.1.call-update
  33.5 0.0 copy-start.1
  33.5 0.0 copy-start.3
  33.5 0.0 copy-start.4
  33.6 1.0 broadcast_in_dim.7
  34.6 13.2 %all-to-all-start.1 = ((bf16[8,256,256]{2,1,0:T(8,128)(2,1)}), bf16[8,256,256]{2,1,0:T(8,128)(2,1)S(1)}, u32[]{:S(2)}, u32[]{:S(2)}) async-start(bf16[8,256,256]{2,1,0:T(8,128)(2,1)} %broadcast_in_dim.7), calls=%async_computation.1 | async-start | bytes 2097152 | tf_op jit(solution)/shard_map/all_to_all | solution.py:42
  47.9 2.5 %collective-permute-start.1 = (bf16[384,256]{1,0:T(8,128)(2,1)S(1)}, bf16[384,256]{1,0:T(8,128)(2,1)S(1)}, u32[]{:S(2)}, u32[]{:S(2)}) collective-permute-start(bf16[384,256]{1,0:T(8,128)(2,1)S(1)} %constant_dynamic-update-slice_fusion.refs_1_), channel_id=1, source_target_pairs={{0,2},{2,4},{4,6},{6,0},{1,3},{3,5},{5,7},{7,1},{8,10},{10,12},{12... | collective-permute-start | bytes 589832 | tf_op jit(solution)/shard_map/ppermute | solution.py:31
  50.4 5.6 %collective-permute-start.3 = (bf16[384,256]{1,0:T(8,128)(2,1)S(1)}, bf16[384,256]{1,0:T(8,128)(2,1)S(1)}, u32[]{:S(2)}, u32[]{:S(2)}) collective-permute-start(bf16[384,256]{1,0:T(8,128)(2,1)S(1)} %constant_dynamic-update-slice_fusion.refs_1_), channel_id=1, source_target_pairs={{0,4},{2,6},{4,0},{6,2},{1,5},{3,7},{5,1},{7,3},{8,12},{10,14},{12... | collective-permute-start | bytes 589832 | tf_op jit(solution)/shard_map/ppermute | solution.py:31
  56.0 0.0 collective-permute-done.1.refs_2_
  56.0 4.1 %collective-permute-done.3.refs_4_ = bf16[384,256]{1,0:T(8,128)(2,1)S(1)} collective-permute-done((bf16[384,256]{1,0:T(8,128)(2,1)S(1)}, bf16[384,256]{1,0:T(8,128)(2,1)S(1)}, u32[]{:S(2)}, u32[]{:S(2)}) %collective-permute-start.3) | collective-permute-done | bytes 196640 | tf_op jit(solution)/shard_map/ppermute | solution.py:31
  60.0 1.0 pad_maximum_fusion
  61.0 6.0 %collective-permute-start.4 = (bf16[4,384,256]{2,1,0:T(8,128)(2,1)}, bf16[4,384,256]{2,1,0:T(8,128)(2,1)S(1)}, u32[]{:S(2)}, u32[]{:S(2)}) collective-permute-start(bf16[4,384,256]{2,1,0:T(8,128)(2,1)} %pad_maximum_fusion), channel_id=1, source_target_pairs={{0,1},{1,0},{2,3},{3,2},{4,5},{5,4},{6,7},{7,6},{8,9},{9,8},{10,11... | collective-permute-start | bytes 2359304 | tf_op jit(solution)/shard_map/ppermute | solution.py:31
  67.0 0.1 pad_add_fusion.refs_0_
  67.1 0.0 copy-done
  67.1 2.0 %collective-permute-done.4.refs_5_ = bf16[4,384,256]{2,1,0:T(8,128)(2,1)S(1)} collective-permute-done((bf16[4,384,256]{2,1,0:T(8,128)(2,1)}, bf16[4,384,256]{2,1,0:T(8,128)(2,1)S(1)}, u32[]{:S(2)}, u32[]{:S(2)}) %collective-permute-start.4) | collective-permute-done | bytes 786464 | tf_op jit(solution)/shard_map/ppermute | solution.py:31
  69.1 0.0 copy-done.1
  69.1 0.0 copy-done.3
  69.1 0.0 copy-done.4
  69.1 3.4 %shard_map.185 = (bf16[384,2048]{1,0:T(8,128)(2,1)}, f32[6,128,256]{2,1,0:T(8,128)}) custom-call(s32[2]{0:T(128)S(1)} %pad_add_fusion.refs_0_, bf16[384,256]{1,0:T(8,128)(2,1)S(1)} %constant_dynamic-update-slice_fusion.refs_1_, bf16[384,256]{1,0:T(8,128)(2,1)S(1)} %collective-permute-done.1.refs_2_, bf16[384,256]{1,0:T(8,128)(2,1)S(1)} %collective-permute-done.2.refs_3_, ...), custom_call_target="tpu_custom_call" | custom-call | flops 134217728 | bytes 2097152 | tf_op jit(solution)/shard_map/pallas_call | solution.py:106
  72.5 8.8 %all-to-all-done.1 = bf16[8,256,256]{2,1,0:T(8,128)(2,1)S(1)} async-done(((bf16[8,256,256]{2,1,0:T(8,128)(2,1)}), bf16[8,256,256]{2,1,0:T(8,128)(2,1)S(1)}, u32[]{:S(2)}, u32[]{:S(2)}) %all-to-all-start.1) | async-done | bytes 1048608 | tf_op jit(solution)/shard_map/all_to_all | solution.py:42
  81.4 0.0 copy-start.5
  81.4 0.0 copy-start.6
  81.4 0.0 copy-start.7
  81.4 6.4 %shard_map.186 = (bf16[8,128,128]{2,1,0:T(8,128)(2,1)}, f32[2,128,256]{2,1,0:T(8,128)}, bf16[2,128,256]{2,1,0:T(8,128)(2,1)}, bf16[2,64,512]{2,1,0:T(8,128)(2,1)}, f32[2,64,512]{2,1,0:T(8,128)}) custom-call(bf16[384,2048]{1,0:T(8,128)(2,1)} %get-tuple-element.17.refs_0_.refs_2_, bf16[2048,256]{1,0:T(8,128)(2,1)S(1)} %bitcast.21, f32[1,128]{1,0:T(1,128)} %bitcast.35, ...), custom_call_target="tpu_custom_call" | custom-call | flops 2147483648 | bytes 2097152 | tf_op jit(solution)/shard_map/pallas_call | solution.py:106
  87.7 11.9 %all-to-all-start.2 = ((bf16[8,128,128]{2,1,0:T(8,128)(2,1)}), bf16[8,128,128]{2,1,0:T(8,128)(2,1)S(1)}, u32[]{:S(2)}, u32[]{:S(2)}) async-start(bf16[8,128,128]{2,1,0:T(8,128)(2,1)} %get-tuple-element.19), calls=%async_computation.2 | async-start | bytes 524288 | tf_op jit(solution)/shard_map/all_to_all | solution.py:520
  99.6 10.4 %all-to-all-done.2.refs_1_ = bf16[8,128,128]{2,1,0:T(8,128)(2,1)S(1)} async-done(((bf16[8,128,128]{2,1,0:T(8,128)(2,1)}), bf16[8,128,128]{2,1,0:T(8,128)(2,1)S(1)}, u32[]{:S(2)}, u32[]{:S(2)}) %all-to-all-start.2) | async-done | bytes 262176 | tf_op jit(solution)/shard_map/all_to_all | solution.py:520
  110.0 1.7 %shard_map.187 = (bf16[8,128,128]{2,1,0:T(8,128)(2,1)}, bf16[128,128]{1,0:T(8,128)(2,1)S(1)}) custom-call(s32[1]{0:T(128)} %bitcast.1.refs_0_, bf16[8,128,128]{2,1,0:T(8,128)(2,1)S(1)} %all-to-all-done.2.refs_1_), custom_call_target="tpu_custom_call" | custom-call | flops 134217728 | bytes 2097152 | tf_op jit(solution)/shard_map/pallas_call | solution.py:106
  111.7 0.0 copy-start.2
  111.7 0.6 copy-done.2
  112.3 3.4 %all-to-all-start.3 = ((bf16[8,128,128]{2,1,0:T(8,128)(2,1)}), bf16[8,128,128]{2,1,0:T(8,128)(2,1)S(1)}, u32[]{:S(2)}, u32[]{:S(2)}) async-start(bf16[8,128,128]{2,1,0:T(8,128)(2,1)} %get-tuple-element.20), calls=%async_computation.3 | async-start | bytes 524288 | tf_op jit(solution)/shard_map/all_to_all | solution.py:524
  115.7 0.0 all-gather.2.cloned.1.call-done.refs_3_.refs_6_
  115.8 0.0 copy-done.5
  115.8 0.0 copy-done.6
  115.8 0.0 copy-done.7
  115.8 7.8 %shard_map.188 = (f32[2,128,256]{2,1,0:T(8,128)}, bf16[256,128]{1,0:T(8,128)(2,1)}, f32[2,256]{1,0:T(2,128)}) custom-call(s32[1]{0:T(128)} %bitcast.15.refs_0_, f32[2]{0:T(128)S(1)} %copy-done.5, bf16[384,2048]{1,0:T(8,128)(2,1)} %get-tuple-element.17.refs_0_.refs_2_, bf16[2048,640]{1,0:T(8,128)(2,1)} %all-gather.2.cloned.1.call-done.refs_3_.refs_6_, ...), custom_call_target="tpu_custom_call" | custom-call | flops 2147483648 | bytes 2097152 | tf_op jit(solution)/shard_map/pallas_call | solution.py:106
  123.6 1.5 all-to-all-done.3.refs_1_
  125.1 2.5 %shard_map.189 = bf16[8,32,2048]{2,1,0:T(8,128)(2,1)S(1)} custom-call(s32[1]{0:T(128)} %bitcast.refs_0_, bf16[8,128,128]{2,1,0:T(8,128)(2,1)S(1)} %all-to-all-done.3.refs_1_, bf16[128,128]{1,0:T(8,128)(2,1)} %copy-done.2, f32[2,128,256]{2,1,0:T(8,128)} %get-tuple-element.27.refs_3_, f32[1,128]{1,0:T(1,128)} %bitcast.34, ...), custom_call_target="tpu_custom_call" | custom-call | flops 1073741824 | bytes 2097152 | tf_op jit(solution)/shard_map/pallas_call | solution.py:106
  127.6 7.7 %all_to_all.30 = bf16[8,32,2048]{2,1,0:T(8,128)(2,1)S(1)} all-to-all(bf16[8,32,2048]{2,1,0:T(8,128)(2,1)S(1)} %shard_map.189), channel_id=1, replica_groups=mesh['sp_0'=8,'sp_1'=8,'fs'=4,'tp'=2] {'tp'}, dimensions={0} | all-to-all | bytes 2097152 | tf_op jit(solution)/shard_map/all_to_all | solution.py:548
  135.3 0.3 reduce_sum.24
  135.6 13.8 %all_to_all.31 = bf16[4,32,2048]{2,1,0:T(8,128)(2,1)S(1)} all-to-all(bf16[4,32,2048]{2,1,0:T(8,128)(2,1)S(1)} %reduce_sum.24), channel_id=1, replica_groups=mesh['sp_0'=8,'sp_1'=8,'fs'=4,'tp'=2] {'fs'}, dimensions={0} | all-to-all | bytes 1048576 | tf_op jit(solution)/shard_map/all_to_all | solution.py:550
  149.4 0.7 reduce_sum.25
  (3 shorter events, 0.0 us)
Async XLA Ops:
  7.2 59.9 %copy-start = (bf16[64,1024]{1,0:T(8,128)(2,1)S(1)}, bf16[64,1024]{1,0:T(8,128)(2,1)}, u32[]{:S(2)}) copy-start(bf16[64,1024]{1,0:T(8,128)(2,1)} %param.27) | copy-start | bytes 393220
  8.9 22.0 %all-to-all-start = ((bf16[8,32,896]{2,1,0:T(8,128)(2,1)}), bf16[8,32,896]{2,1,0:T(8,128)(2,1)S(1)}, u32[]{:S(2)}, u32[]{:S(2)}) async-start(bf16[8,32,896]{2,1,0:T(8,128)(2,1)} %broadcast_in_dim.6), calls=%async_computation | async-start | bytes 917504 | tf_op jit(solution)/shard_map/all_to_all | solution.py:42
  16.6 99.2 %all-gather.2.cloned.1.call-start = ((), (), s32[]{:S(2)}) async-start(), calls=%async_computation.6 | async-start | bytes 2949120 | tf_op jit(solution)/shard_map/all_gather | solution.py:486
  17.5 5.5 %collective-permute-start = (bf16[128,256]{1,0:T(8,128)(2,1)S(1)}, bf16[128,256]{1,0:T(8,128)(2,1)S(1)}, u32[]{:S(2)}, u32[]{:S(2)}) collective-permute-start(bf16[128,256]{1,0:T(8,128)(2,1)S(1)} %slice.9), channel_id=1, source_target_pairs={{0,8},{8,16},{16,24},{24,32},{32,40},{40,48},{48,56},{56,64},{64,7... | collective-permute-start | bytes 196616 | tf_op jit(solution)/shard_map/ppermute | solution.py:37
  23.9 9.6 %collective-permute-start.2 = (bf16[384,256]{1,0:T(8,128)(2,1)S(1)}, bf16[384,256]{1,0:T(8,128)(2,1)S(1)}, u32[]{:S(2)}, u32[]{:S(2)}) collective-permute-start(bf16[384,256]{1,0:T(8,128)(2,1)S(1)} %constant_dynamic-update-slice_fusion.refs_1_), channel_id=1, source_target_pairs={{0,6},{2,0},{4,2},{6,4},{1,7},{3,1},{5,3},{7,5},{8,14},{10,8},{12,... | collective-permute-start | bytes 589832 | tf_op jit(solution)/shard_map/ppermute | solution.py:31
  33.5 35.6 %copy-start.1 = (bf16[2048,64]{0,1:T(8,128)(2,1)S(1)}, bf16[2048,64]{0,1:T(8,128)(2,1)}, u32[]{:S(2)}) copy-start(bf16[2048,64]{0,1:T(8,128)(2,1)} %param.26) | copy-start | bytes 786436
  33.5 35.6 %copy-start.3 = (f32[2048]{0:T(1024)S(1)}, f32[2048]{0:T(1024)}, u32[]{:S(2)}) copy-start(f32[2048]{0:T(1024)} %param.19) | copy-start | bytes 24580
  33.5 35.6 %copy-start.4 = (f32[2,256]{1,0:T(2,128)S(1)}, f32[2,256]{1,0:T(2,128)}, u32[]{:S(2)}) copy-start(f32[2,256]{1,0:T(2,128)} %refs_9_.1) | copy-start | bytes 6148
  34.6 46.7 %all-to-all-start.1 = ((bf16[8,256,256]{2,1,0:T(8,128)(2,1)}), bf16[8,256,256]{2,1,0:T(8,128)(2,1)S(1)}, u32[]{:S(2)}, u32[]{:S(2)}) async-start(bf16[8,256,256]{2,1,0:T(8,128)(2,1)} %broadcast_in_dim.7), calls=%async_computation.1 | async-start | bytes 2097152 | tf_op jit(solution)/shard_map/all_to_all | solution.py:42
  47.9 8.1 %collective-permute-start.1 = (bf16[384,256]{1,0:T(8,128)(2,1)S(1)}, bf16[384,256]{1,0:T(8,128)(2,1)S(1)}, u32[]{:S(2)}, u32[]{:S(2)}) collective-permute-start(bf16[384,256]{1,0:T(8,128)(2,1)S(1)} %constant_dynamic-update-slice_fusion.refs_1_), channel_id=1, source_target_pairs={{0,2},{2,4},{4,6},{6,0},{1,3},{3,5},{5,7},{7,1},{8,10},{10,12},{12... | collective-permute-start | bytes 589832 | tf_op jit(solution)/shard_map/ppermute | solution.py:31
  50.4 9.6 %collective-permute-start.3 = (bf16[384,256]{1,0:T(8,128)(2,1)S(1)}, bf16[384,256]{1,0:T(8,128)(2,1)S(1)}, u32[]{:S(2)}, u32[]{:S(2)}) collective-permute-start(bf16[384,256]{1,0:T(8,128)(2,1)S(1)} %constant_dynamic-update-slice_fusion.refs_1_), channel_id=1, source_target_pairs={{0,4},{2,6},{4,0},{6,2},{1,5},{3,7},{5,1},{7,3},{8,12},{10,14},{12... | collective-permute-start | bytes 589832 | tf_op jit(solution)/shard_map/ppermute | solution.py:31
  61.0 8.1 %collective-permute-start.4 = (bf16[4,384,256]{2,1,0:T(8,128)(2,1)}, bf16[4,384,256]{2,1,0:T(8,128)(2,1)S(1)}, u32[]{:S(2)}, u32[]{:S(2)}) collective-permute-start(bf16[4,384,256]{2,1,0:T(8,128)(2,1)} %pad_maximum_fusion), channel_id=1, source_target_pairs={{0,1},{1,0},{2,3},{3,2},{4,5},{5,4},{6,7},{7,6},{8,9},{9,8},{10,11... | collective-permute-start | bytes 2359304 | tf_op jit(solution)/shard_map/ppermute | solution.py:31
  81.4 34.4 %copy-start.5 = (f32[2]{0:T(128)S(1)}, f32[2]{0:T(128)}, u32[]{:S(2)}) copy-start(f32[2]{0:T(128)} %refs_1_.1) | copy-start | bytes 28
  81.4 34.4 %copy-start.6 = (f32[64]{0:T(128)S(1)}, f32[64]{0:T(128)}, u32[]{:S(2)}) copy-start(f32[64]{0:T(128)} %param.30) | copy-start | bytes 772
  81.4 34.4 %copy-start.7 = (f32[64]{0:T(128)S(1)}, f32[64]{0:T(128)}, u32[]{:S(2)}) copy-start(f32[64]{0:T(128)} %param.31) | copy-start | bytes 772
  87.7 22.2 %all-to-all-start.2 = ((bf16[8,128,128]{2,1,0:T(8,128)(2,1)}), bf16[8,128,128]{2,1,0:T(8,128)(2,1)S(1)}, u32[]{:S(2)}, u32[]{:S(2)}) async-start(bf16[8,128,128]{2,1,0:T(8,128)(2,1)} %get-tuple-element.19), calls=%async_computation.2 | async-start | bytes 524288 | tf_op jit(solution)/shard_map/all_to_all | solution.py:520
  111.7 0.6 copy-start.2
  112.3 12.8 %all-to-all-start.3 = ((bf16[8,128,128]{2,1,0:T(8,128)(2,1)}), bf16[8,128,128]{2,1,0:T(8,128)(2,1)S(1)}, u32[]{:S(2)}, u32[]{:S(2)}) async-start(bf16[8,128,128]{2,1,0:T(8,128)(2,1)} %get-tuple-element.20), calls=%async_computation.3 | async-start | bytes 524288 | tf_op jit(solution)/shard_map/all_to_all | solution.py:524
Sparse Core Ops, SparseCore 0:
  33.6 65.5 all-gather.1

commit v4 on v3

--- a/solution.py
+++ b/solution.py
@@ -138,28 +138,37 @@
     return total, after
 
 
-def hidden_kernel(place, own, next_, before, across, other, gain, down, up, base, hid, decays):
-    x = place[0]
-    core = place[1]
-    rows = own.shape[0]
-    blocks = [own, before, across, next_]
+def hidden_parts(place, blocks, other, gain):
+    x, core = place[0], place[1]
+    rows, width = blocks[0].shape
     sums = jnp.zeros((rows, 1), F32)
     for k in range(4):
         mine = blocks[k][...].astype(F32)
         theirs = other[k].astype(F32)
         sums += jnp.sum(mine * mine + theirs * theirs, axis=1, keepdims=True)
-    width = own.shape[1]
     scale = lax.rsqrt(sums / (8 * width) + NORM_EPS)
-    low = jnp.zeros((rows, down.shape[0]), F32)
     for k in range(4):
         chip = lax.rem(x + k, 4)
         for c, block in ((core, blocks[k][...]), (1 - core, other[k])):
             at = pl.multiple_of((chip * 2 + c) * width, width)
-            h = (block.astype(F32) * scale * gain[:, pl.ds(at, width)]).astype(BF16)
-            hid.ref[:, pl.ds(at, width)] = h
-            low += lax.dot_general(h, down[:, pl.ds(at, width)], NT, preferred_element_type=F32)
+            yield at, (block.astype(F32) * scale * gain[:, pl.ds(at, width)]).astype(BF16)
+
+
+def halo_kernel(place, own, next_, before, across, other, gain, hid):
+    width = own.shape[1]
+    for at, h in hidden_parts(place, [own, before, across, next_], other, gain):
+        hid.ref[:, pl.ds(at, width)] = h
     hid.put()
-    low = jnp.tanh(low[WINDOW:, :]).astype(BF16)
+
+
+def hidden_kernel(place, own, next_, before, across, other, gain, down, up, base, hid, decays):
+    rows, width = own.shape
+    low = jnp.zeros((rows, down.shape[0]), F32)
+    for at, h in hidden_parts(place, [own, before, across, next_], other, gain):
+        hid.ref[:, pl.ds(at, width)] = h
+        low += lax.dot_general(h, down[:, pl.ds(at, width)], NT, preferred_element_type=F32)
+    hid.put()
+    low = jnp.tanh(low).astype(BF16)
     rate = lax.dot_general(up[...], low, (((0,), (1,)), ((), ())), preferred_element_type=F32)
     heads = base.shape[0]
     base_rows = jnp.concatenate(
@@ -339,40 +348,44 @@
     out.put()
 
 
-def chain(earlier, later):
-    moved = jnp.dot(earlier.astype(BF16), later[:HEAD, :], preferred_element_type=F32)
-    return moved + jnp.concatenate([jnp.zeros((HEAD, HEAD), F32), later[HEAD:, :].astype(F32)], axis=0)
-
-
-def row_kernel(place, pieces, total_out, inside_out):
+def chain(parts):
+    while len(parts) > 1:
+        parts = [
+            jnp.dot(a.astype(BF16), b[:HEAD, :].astype(BF16), preferred_element_type=F32)
+            + jnp.concatenate([jnp.zeros((HEAD, HEAD), F32), b[HEAD:, :]], axis=0)
+            for a, b in zip(parts[::2], parts[1::2])
+        ]
+    return parts[0]
+
+
+def piece(pieces, k, h):
+    return pieces[k, :, head_rows(h)].astype(F32)
+
+
+def chain_before(place, pieces, h):
+    eye = jnp.concatenate([spread(jnp.ones((1, HEAD), F32)), jnp.zeros((HEAD, HEAD), F32)], axis=0)
+    devices = pieces.shape[0]
+    return chain([jnp.where(k < place, piece(pieces, k, h), eye) for k in range(devices)])
+
+
+def row_kernel(pieces, total):
     devices, heads = pieces.shape[0], pieces.shape[2] // HEAD
-    eye = (
-        lax.broadcasted_iota(jnp.int32, (2 * HEAD, HEAD), 0)
-        == lax.broadcasted_iota(jnp.int32, (2 * HEAD, HEAD), 1)
-    ).astype(F32)
-    total = [eye] * heads
-    inside = [eye] * heads
-    for k in range(devices):
-        passed = k < place[0]
-        for h in range(heads):
-            later = pieces[k, :, head_rows(h)]
-            total[h] = later.astype(F32) if k == 0 else chain(total[h], later)
-            inside[h] = jnp.where(passed, total[h], inside[h])
-    packed = jnp.concatenate(total, axis=1).astype(BF16)
-    for k in range(total_out.shape[0]):
-        total_out[k] = packed
-    inside_out[...] = jnp.concatenate(inside, axis=1).astype(BF16)
+    parts = [chain([piece(pieces, k, h) for k in range(devices)]) for h in range(heads)]
+    packed = jnp.concatenate(parts, axis=1).astype(BF16)
+    for k in range(total.shape[0]):
+        total[k] = packed
+
+
+def inside_kernel(place, pieces, inside):
+    pieces = pieces.get()
+    heads = pieces.shape[2] // HEAD
+    parts = [chain_before(place[0], pieces, h) for h in range(heads)]
+    inside[...] = jnp.concatenate(parts, axis=1).astype(BF16)
 
 
 def final_kernel(place, pieces, inside, local, gain, att, w, out):
-    devices, heads = pieces.shape[0], pieces.shape[2] // HEAD
-    state = [jnp.zeros((HEAD, HEAD), F32)] * heads
-    for k in range(devices - 1):
-        passed = k < place[0]
-        for h in range(heads):
-            later = pieces[k, :, head_rows(h)]
-            new = jnp.dot(state[h].astype(BF16), later[:HEAD, :], preferred_element_type=F32)
-            state[h] = jnp.where(passed, new + later[HEAD:, :].astype(F32), state[h])
+    heads = pieces.shape[2] // HEAD
+    state = [chain_before(place[0], pieces, h)[HEAD:, :] for h in range(heads)]
     rows = []
     gain = as_column(gain.get()[...])
     inside, local = inside.get(), local.get()
@@ -431,18 +444,19 @@
     out.put()
 
 
-def late_kernel(place, sink, hid, w, query_gain, key_gain, lr, decays, units, tables, changes, adds, local, mix, lse):
+def late_kernel(place, sink, hid, halo, w, query_gain, key_gain, lr, decays, units, tables, changes, adds, local, mix, lse):
     q_w = mix.ref.shape[1]
     lr = as_column(lr.get()[...])
-    hid, w = hid.get(), w.get()
-    both = jnp.dot(hid[...], w[...], preferred_element_type=F32).astype(BF16)
-    own = both[WINDOW:, :]
+    hid, w, halo = hid.get(), w.get(), halo.get()
+    own = jnp.dot(hid[...], w[...], preferred_element_type=F32).astype(BF16)
     whole = own.shape[1] - lr.shape[0]
+    ahead = jnp.dot(halo[...], w[:, q_w:whole], preferred_element_type=F32).astype(BF16)
     made = [ref.get() for ref in (decays, units, tables, changes, adds)]
     read_part(own[:, whole:].astype(F32), lr, *made, local)
     queries = head_rms(own[:, :q_w].astype(F32), query_gain[...])
-    (keys,) = head_rms(both[:, q_w : q_w + HEAD].astype(F32), key_gain[...])
-    attention_part(place[0] == 0, sink, queries, keys, both[:, q_w + HEAD : whole], mix, lse)
+    both = jnp.concatenate([ahead, own[:, q_w:whole]], axis=0)
+    (keys,) = head_rms(both[:, :HEAD].astype(F32), key_gain[...])
+    attention_part(place[0] == 0, sink, queries, keys, both[:, HEAD:], mix, lse)
 
 
 def per_device(
@@ -477,13 +491,10 @@
     )
     column = from_everyone(own, "sp_1").reshape(-1, own.shape[1])
     state_w = from_everyone(column[:, : 2 * span], "sp_0").reshape(features, 2 * span)
-    ahead = passed_along(tokens[rows - WINDOW :], SP, 1)
-    tokens = jnp.concatenate([ahead, tokens], axis=0)
     before = ring_shift(tokens, "fs", -1)
     across = ring_shift(tokens, "fs", 2)
     next_ = ring_shift(tokens, "fs", 1)
-    held, before = lax.optimization_barrier((column[:, 2 * span :], before))
-    other_w = lax.all_gather(held, "sp_0", axis=0, tiled=True)
+    ahead = passed_along(tokens[rows - WINDOW :], SP, 1)
     other = ring_shift(jnp.stack([tokens, before, across, next_]), "tp", 1)
 
 
@@ -493,11 +504,23 @@
     )
     flat = (span, rows)
     hid, decays = call(
-        hidden_kernel, [((WINDOW + rows, features), BF16), ((6, *flat), F32)], smem=1, flops=1 << 27, far_out=(0, 1)
+        hidden_kernel, [((rows, features), BF16), ((6, *flat), F32)], smem=1, flops=1 << 27, far_out=(0, 1)
     )(
         place_xc, tokens, next_, before, across, other, norm_gain.reshape(1, -1), decay_down.T, decay_cols, decay_base
     )
 
+
+    held, hid = lax.optimization_barrier((column[:, 2 * span :], hid))
+    other_w = lax.all_gather(held, "sp_0", axis=0, tiled=True)
+
+    ahead, hid = lax.optimization_barrier((ahead, hid))
+    halo_before = ring_shift(ahead, "fs", -1)
+    halo_across = ring_shift(ahead, "fs", 2)
+    halo_next = ring_shift(ahead, "fs", 1)
+    halo_other = ring_shift(jnp.stack([ahead, halo_before, halo_across, halo_next]), "tp", 1)
+    (halo,) = call(
+        halo_kernel, [((WINDOW, features), BF16)], smem=1, flops=1 << 26, far_out=(0,)
+    )(place_xc, ahead, halo_next, halo_before, halo_across, halo_other, norm_gain.reshape(1, -1))
 
     lr = learn_rate.reshape(1, span)
     chunks = rows // CHUNK
@@ -513,28 +536,28 @@
         ],
         scratch=[pltpu.VMEM((rows, span), F32)],
         flops=1 << 31,
-        far={0: (WINDOW, rows, 0, features), 2: None, 3: None},
+        far={0: None, 2: None, 3: None},
         far_out=(1, 2, 3, 4),
     )(hid, state_w, lr, decays)
 
     row_pieces = lax.all_to_all(ends, "sp_1", 0, 0, tiled=True)
-    row_total, inside = call(
-        row_kernel, [((lax.axis_size("sp_0"), *pair), BF16), (pair, BF16)], smem=1, flops=1 << 27
-    )(place_zy[1], row_pieces)
+    (row_total,) = call(row_kernel, [((lax.axis_size("sp_0"), *pair), BF16)], flops=1 << 27)(row_pieces)
+    (inside,) = call(inside_kernel, [(pair, BF16)], smem=1, flops=1 << 27, far={1: None})(place_zy[1], row_pieces)
     all_pieces = lax.all_to_all(row_total, "sp_0", 0, 0, tiled=True)
 
     q_w, kv_w = query_w.shape[1], key_w.shape[1]
-    early = q_w + 2 * kv_w + span
+    whole = q_w + 2 * kv_w
+    early = whole + span
     place_sp = lax.axis_index(SP).astype(jnp.int32).reshape(1)
     local, att_mix, row_lse = call(
         late_kernel,
         [((heads, 2 * HEAD, rows), F32), ((rows, q_w), BF16), ((q_w // HEAD, rows), F32)],
         smem=2,
         flops=1 << 31,
-        far={2: None, 3: (0, features, 0, early), **{i: None for i in range(6, 12)}},
+        far={2: None, 3: None, 4: (0, features, 0, early), **{i: None for i in range(7, 13)}},
         far_out=(0, 1),
     )(
-        place_sp, sink_logit, hid, other_w, query_gain.reshape(1, HEAD), key_gain.reshape(1, HEAD),
+        place_sp, sink_logit, hid, halo, other_w, query_gain.reshape(1, HEAD), key_gain.reshape(1, HEAD),
         lr, decays, *made,
     )
 

time: 158 us -> 166 us (1.051)
  waiting for transfers between devices: 30.8 us -> 49.7 us
  starting transfers between devices: 60.5 us -> 54.1 us
  blocking collectives: 21.5 us -> 16.1 us
  Pallas kernels: 21.7 us -> 23.7 us
  local copies, waits for them, and re-layouts: 5.99 us -> 4.2 us
    all_to_all x2, waiting for transfers between devices: 8.84 us -> 35.7 us  [from_everyone(): return lax.all_to_all(copies, axis, split_axis=0, concat_axis=0, tiled=True)]
    all_to_all x1, waiting for transfers between devices: 10.4 us -> 0.01 us  [per_device(): row_pieces = lax.all_to_all(ends, 'sp_1', 0, 0, tiled=True)]
    all_to_all x1, starting transfers between devices: 11.9 us -> 5.43 us  [per_device(): row_pieces = lax.all_to_all(ends, 'sp_1', 0, 0, tiled=True)]
    ppermute x4 -> x8, waiting for transfers between devices: 7.89 us -> 12.1 us  [ring_shift(): lax.ppermute(array, axis, [(i, (i + by) % devices) for i in range(devices)])]
    all_to_all x2, starting transfers between devices: 20.9 us -> 17.7 us  [from_everyone(): return lax.all_to_all(copies, axis, split_axis=0, concat_axis=0, tiled=True)]
    all_to_all x1, blocking collectives: 7.72 us -> 4.64 us  [per_device(): lax.all_to_all(partial, 'tp', 0, 0, tiled=True)]
    ppermute x4 -> x8, starting transfers between devices: 21.1 us -> 23.8 us  [ring_shift(): lax.ppermute(array, axis, [(i, (i + by) % devices) for i in range(devices)])]
    all_to_all x1, blocking collectives: 13.8 us -> 11.4 us  [per_device(): tiles = lax.all_to_all(tiles, 'fs', 0, 0, tiled=True)]
  transfers between devices with their start and end apart: 10 -> 14, of which waited for: 7 -> 8; matrix products, arithmetic and copies ran while one was open for 3% -> 1% of each run, Pallas kernels for 12% -> 13%
where the time goes in v4:
time: 166 us; the launch traced here: 164 us
  starting transfers between devices  54.1 us (33%)
  waiting for transfers between devices  49.7 us (30%)
  Pallas kernels  23.7 us (14%)
  blocking collectives  16.1 us (10%)
  between operations  14.4 us (9%)
  local copies, waits for them, and re-layouts  4.2 us (3%)
  other arithmetic  2.13 us (1%)
    all_to_all x2, waiting for transfers between devices, from_everyone(): return lax.all_to_all(copies, axis, split_axis=0, concat_axis=0, tiled=True)  35.7 us
    ppermute x8, starting transfers between devices, ring_shift(): lax.ppermute(array, axis, [(i, (i + by) % devices) for i in range(devices)])  23.8 us
    pallas_call x7, Pallas kernels, run(): pl.pallas_call(body, out_shape=[pltpu.HBM(*o) if i in far_out else jax.Sh...  23.7 us
    all_to_all x2, starting transfers between devices, from_everyone(): return lax.all_to_all(copies, axis, split_axis=0, concat_axis=0, tiled=True)  17.7 us
    ppermute x8, waiting for transfers between devices, ring_shift(): lax.ppermute(array, axis, [(i, (i + by) % devices) for i in range(devices)])  12.1 us
    all_to_all x1, blocking collectives, per_device(): tiles = lax.all_to_all(tiles, 'fs', 0, 0, tiled=True)  11.4 us
    all_to_all x1, starting transfers between devices, per_device(): row_pieces = lax.all_to_all(ends, 'sp_1', 0, 0, tiled=True)  5.43 us
    all_to_all x1, blocking collectives, per_device(): lax.all_to_all(partial, 'tp', 0, 0, tiled=True)  4.64 us
  transfers between devices with their start and end apart: 14, of which 8 were waited for; matrix products, arithmetic and copies ran while one was open for 1% of the time, Pallas kernels for 13%

profile of v4, /device:TPU:1, one launch (start us, length us, event | category | flops | bytes accessed | tf_op | source)
XLA Modules:
  0.0 164.3 jit_solution(10511677593837997751)
XLA Ops:
  7.2 0.0 copy-start
  7.2 0.0 copy-start.2
  7.2 0.0 copy-start.5
  7.2 0.0 copy-start.3
  7.2 0.0 copy-start.6
  7.2 0.9 concatenate.3
  8.2 0.8 broadcast_in_dim.6
  9.0 7.6 %all-to-all-start = ((bf16[8,32,896]{2,1,0:T(8,128)(2,1)}), bf16[8,32,896]{2,1,0:T(8,128)(2,1)S(1)}, u32[]{:S(2)}, u32[]{:S(2)}) async-start(bf16[8,32,896]{2,1,0:T(8,128)(2,1)} %broadcast_in_dim.6), calls=%async_computation | async-start | bytes 917504 | tf_op jit(solution)/shard_map/all_to_all | solution.py:42
  16.6 0.0 all-gather.2.cloned.1.call-start
  16.7 4.4 %collective-permute-start.2 = (bf16[256,256]{1,0:T(8,128)(2,1)}, bf16[256,256]{1,0:T(8,128)(2,1)S(1)}, u32[]{:S(2)}, u32[]{:S(2)}) collective-permute-start(bf16[256,256]{1,0:T(8,128)(2,1)} %refs_1_.2), channel_id=1, source_target_pairs={{0,6},{2,0},{4,2},{6,4},{1,7},{3,1},{5,3},{7,5},{8,14},{10,8},{12,... | collective-permute-start | bytes 393224 | tf_op jit(solution)/shard_map/ppermute | solution.py:31
  21.1 2.4 %collective-permute-start.3 = (bf16[256,256]{1,0:T(8,128)(2,1)}, bf16[256,256]{1,0:T(8,128)(2,1)S(1)}, u32[]{:S(2)}, u32[]{:S(2)}) collective-permute-start(bf16[256,256]{1,0:T(8,128)(2,1)} %refs_1_.2), channel_id=1, source_target_pairs={{0,4},{2,6},{4,0},{6,2},{1,5},{3,7},{5,1},{7,3},{8,12},{10,14},{12... | collective-permute-start | bytes 393224 | tf_op jit(solution)/shard_map/ppermute | solution.py:31
  23.5 2.5 %collective-permute-start.1 = (bf16[256,256]{1,0:T(8,128)(2,1)}, bf16[256,256]{1,0:T(8,128)(2,1)S(1)}, u32[]{:S(2)}, u32[]{:S(2)}) collective-permute-start(bf16[256,256]{1,0:T(8,128)(2,1)} %refs_1_.2), channel_id=1, source_target_pairs={{0,2},{2,4},{4,6},{6,0},{1,3},{3,5},{5,7},{7,1},{8,10},{10,12},{12... | collective-permute-start | bytes 393224 | tf_op jit(solution)/shard_map/ppermute | solution.py:31
  26.0 0.0 collective-permute-done.2.refs_3_
  26.0 2.8 %collective-permute-done.3.refs_4_ = bf16[256,256]{1,0:T(8,128)(2,1)S(1)} collective-permute-done((bf16[256,256]{1,0:T(8,128)(2,1)}, bf16[256,256]{1,0:T(8,128)(2,1)S(1)}, u32[]{:S(2)}, u32[]{:S(2)}) %collective-permute-start.3) | collective-permute-done | bytes 131104 | tf_op jit(solution)/shard_map/ppermute | solution.py:31
  28.8 3.6 %collective-permute-done.1.refs_2_ = bf16[256,256]{1,0:T(8,128)(2,1)S(1)} collective-permute-done((bf16[256,256]{1,0:T(8,128)(2,1)}, bf16[256,256]{1,0:T(8,128)(2,1)S(1)}, u32[]{:S(2)}, u32[]{:S(2)}) %collective-permute-start.1) | collective-permute-done | bytes 131104 | tf_op jit(solution)/shard_map/ppermute | solution.py:31
  32.4 1.0 pad_maximum_fusion
  33.4 3.3 %collective-permute-start.4 = (bf16[4,256,256]{2,1,0:T(8,128)(2,1)S(1)}, bf16[4,256,256]{2,1,0:T(8,128)(2,1)S(1)}, u32[]{:S(2)}, u32[]{:S(2)}) collective-permute-start(bf16[4,256,256]{2,1,0:T(8,128)(2,1)S(1)} %pad_maximum_fusion), channel_id=1, source_target_pairs={{0,1},{1,0},{2,3},{3,2},{4,5},{5,4},{6,7},{7,6},{8,9},{9,8},{10,11... | collective-permute-start | bytes 1572872 | tf_op jit(solution)/shard_map/ppermute | solution.py:31
  36.7 0.1 pad_add_fusion.refs_0_
  36.8 0.0 copy-done
  36.8 1.4 collective-permute-done.4.refs_5_
  38.2 0.0 copy-done.2
  38.2 0.0 copy-done.5
  38.2 0.0 copy-done.3
  38.2 0.0 copy-done.6
  38.2 3.0 %shard_map.185 = (bf16[256,2048]{1,0:T(8,128)(2,1)}, f32[6,128,256]{2,1,0:T(8,128)}) custom-call(s32[2]{0:T(128)S(1)} %pad_add_fusion.refs_0_, bf16[256,256]{1,0:T(8,128)(2,1)S(1)} %copy-done.2, bf16[256,256]{1,0:T(8,128)(2,1)S(1)} %collective-permute-done.1.refs_2_, bf16[256,256]{1,0:T(8,128)(2,1)S(1)} %collective-permute-done.2.refs_3_, ...), custom_call_target="tpu_custom_call" | custom-call | flops 134217728 | bytes 2097152 | tf_op jit(solution)/shard_map/pallas_call | solution.py:106
  41.2 0.0 all-to-all-done
  41.3 0.8 slice.12
  42.0 0.0 all-gather.2.cloned.1.call-update
  42.1 1.0 broadcast_in_dim.7
  43.1 10.0 %all-to-all-start.1 = ((bf16[8,256,256]{2,1,0:T(8,128)(2,1)}), bf16[8,256,256]{2,1,0:T(8,128)(2,1)S(1)}, u32[]{:S(2)}, u32[]{:S(2)}) async-start(bf16[8,256,256]{2,1,0:T(8,128)(2,1)} %broadcast_in_dim.7), calls=%async_computation.1 | async-start | bytes 2097152 | tf_op jit(solution)/shard_map/all_to_all | solution.py:42
  53.1 3.6 %collective-permute-start = (bf16[128,256]{1,0:T(8,128)(2,1)S(1)}, bf16[128,256]{1,0:T(8,128)(2,1)S(1)}, u32[]{:S(2)}, u32[]{:S(2)}) collective-permute-start(bf16[128,256]{1,0:T(8,128)(2,1)S(1)} %slice.9), channel_id=1, source_target_pairs={{0,8},{8,16},{16,24},{24,32},{32,40},{40,48},{48,56},{56,64},{64,7... | collective-permute-start | bytes 196616 | tf_op jit(solution)/shard_map/ppermute | solution.py:37
  56.7 1.3 collective-permute-done.refs_1_
  58.0 35.7 %all-to-all-done.1 = bf16[8,256,256]{2,1,0:T(8,128)(2,1)S(1)} async-done(((bf16[8,256,256]{2,1,0:T(8,128)(2,1)}), bf16[8,256,256]{2,1,0:T(8,128)(2,1)S(1)}, u32[]{:S(2)}, u32[]{:S(2)}) %all-to-all-start.1) | async-done | bytes 1048608 | tf_op jit(solution)/shard_map/all_to_all | solution.py:42
  93.8 6.3 %shard_map.186 = (bf16[8,128,128]{2,1,0:T(8,128)(2,1)}, f32[2,128,256]{2,1,0:T(8,128)}, bf16[2,128,256]{2,1,0:T(8,128)(2,1)}, bf16[2,64,512]{2,1,0:T(8,128)(2,1)}, f32[2,64,512]{2,1,0:T(8,128)}) custom-call(bf16[256,2048]{1,0:T(8,128)(2,1)} %get-tuple-element.18.refs_0_.refs_2_, bf16[2048,256]{1,0:T(8,128)(2,1)S(1)} %bitcast.24, f32[1,128]{1,0:T(1,128)} %bitcast.44, ...), custom_call_target="tpu_custom_call" | custom-call | flops 2147483648 | bytes 2097152 | tf_op jit(solution)/shard_map/pallas_call | solution.py:106
  100.1 0.0 copy-start.7
  100.1 0.0 copy-start.8
  100.1 0.0 copy-start.9
  100.1 5.4 %all-to-all-start.2 = ((bf16[8,128,128]{2,1,0:T(8,128)(2,1)}), bf16[8,128,128]{2,1,0:T(8,128)(2,1)S(1)}, u32[]{:S(2)}, u32[]{:S(2)}) async-start(bf16[8,128,128]{2,1,0:T(8,128)(2,1)} %get-tuple-element.20), calls=%async_computation.2 | async-start | bytes 524288 | tf_op jit(solution)/shard_map/all_to_all | solution.py:543
  105.6 1.9 %collective-permute-start.6 = (bf16[128,256]{1,0:T(8,128)(2,1)S(1)}, bf16[128,256]{1,0:T(8,128)(2,1)S(1)}, u32[]{:S(2)}, u32[]{:S(2)}) collective-permute-start(bf16[128,256]{1,0:T(8,128)(2,1)S(1)} %collective-permute-done.refs_1_), channel_id=1, source_target_pairs={{0,6},{2,0},{4,2},{6,4},{1,7},{3,1},{5,3},{7,5},{8,14},{10,8},{12,... | collective-permute-start | bytes 196616 | tf_op jit(solution)/shard_map/ppermute | solution.py:31
  107.5 1.9 %collective-permute-start.7 = (bf16[128,256]{1,0:T(8,128)(2,1)S(1)}, bf16[128,256]{1,0:T(8,128)(2,1)S(1)}, u32[]{:S(2)}, u32[]{:S(2)}) collective-permute-start(bf16[128,256]{1,0:T(8,128)(2,1)S(1)} %collective-permute-done.refs_1_), channel_id=1, source_target_pairs={{0,4},{2,6},{4,0},{6,2},{1,5},{3,7},{5,1},{7,3},{8,12},{10,14},{12... | collective-permute-start | bytes 196616 | tf_op jit(solution)/shard_map/ppermute | solution.py:31
  109.4 3.4 %collective-permute-start.5 = (bf16[128,256]{1,0:T(8,128)(2,1)S(1)}, bf16[128,256]{1,0:T(8,128)(2,1)S(1)}, u32[]{:S(2)}, u32[]{:S(2)}) collective-permute-start(bf16[128,256]{1,0:T(8,128)(2,1)S(1)} %collective-permute-done.refs_1_), channel_id=1, source_target_pairs={{0,2},{2,4},{4,6},{6,0},{1,3},{3,5},{5,7},{7,1},{8,10},{10,12},{12... | collective-permute-start | bytes 196616 | tf_op jit(solution)/shard_map/ppermute | solution.py:31
  112.8 0.0 collective-permute-done.6.refs_3_
  112.8 1.4 collective-permute-done.7.refs_4_
  114.2 2.9 %collective-permute-done.5.refs_2_ = bf16[128,256]{1,0:T(8,128)(2,1)S(1)} collective-permute-done((bf16[128,256]{1,0:T(8,128)(2,1)S(1)}, bf16[128,256]{1,0:T(8,128)(2,1)S(1)}, u32[]{:S(2)}, u32[]{:S(2)}) %collective-permute-start.5) | collective-permute-done | bytes 65568 | tf_op jit(solution)/shard_map/ppermute | solution.py:31
  117.1 4.0 %collective-permute-start.8 = (bf16[4,128,256]{2,1,0:T(8,128)(2,1)S(1)}, bf16[4,128,256]{2,1,0:T(8,128)(2,1)S(1)}, u32[]{:S(2)}, u32[]{:S(2)}) collective-permute-start(bf16[4,128,256]{2,1,0:T(8,128)(2,1)S(1)} %pad_maximum_fusion.1), channel_id=1, source_target_pairs={{0,1},{1,0},{2,3},{3,2},{4,5},{5,4},{6,7},{7,6},{8,9},{9,8},{10,11... | collective-permute-start | bytes 786440 | tf_op jit(solution)/shard_map/ppermute | solution.py:31
  121.1 0.0 all-to-all-done.2.refs_0_.refs_1_
  121.1 0.0 copy-start.1
  121.2 1.3 shard_map.187
  122.5 3.6 %all-to-all-start.3 = ((bf16[8,128,128]{2,1,0:T(8,128)(2,1)}), bf16[8,128,128]{2,1,0:T(8,128)(2,1)S(1)}, u32[]{:S(2)}, u32[]{:S(2)}) async-start(bf16[8,128,128]{2,1,0:T(8,128)(2,1)} %shard_map.187), calls=%async_computation.3 | async-start | bytes 524288 | tf_op jit(solution)/shard_map/all_to_all | solution.py:546
  126.1 0.0 collective-permute-done.8.refs_5_
  126.1 1.7 %shard_map.189.refs_3_ = bf16[128,2048]{1,0:T(8,128)(2,1)} custom-call(s32[2]{0:T(128)S(1)} %pad_add_fusion.refs_0_, bf16[128,256]{1,0:T(8,128)(2,1)S(1)} %collective-permute-done.refs_1_, bf16[128,256]{1,0:T(8,128)(2,1)S(1)} %collective-permute-done.5.refs_2_, bf16[128,256]{1,0:T(8,128)(2,1)S(1)} %collective-permute-done.6.refs_3_, ...), custom_call_target="tpu_custom_call" | custom-call | flops 67108864 | bytes 2097152 | tf_op jit(solution)/shard_map/pallas_call | solution.py:106
  127.8 0.0 copy-done.1
  127.8 1.6 shard_map.188.refs_2_
  129.4 0.0 copy-start.4
  129.4 0.6 copy-done.4
  130.0 0.0 copy-done.7
  130.0 0.0 copy-done.8
  130.0 7.6 %shard_map.190 = (f32[2,128,256]{2,1,0:T(8,128)}, bf16[256,128]{1,0:T(8,128)(2,1)}, f32[2,256]{1,0:T(2,128)}) custom-call(s32[1]{0:T(128)} %bitcast.15.refs_0_, f32[2]{0:T(128)S(1)} %copy-done.7, bf16[256,2048]{1,0:T(8,128)(2,1)} %get-tuple-element.18.refs_0_.refs_2_, bf16[128,2048]{1,0:T(8,128)(2,1)} %shard_map.189.refs_3_, ...), custom_call_target="tpu_custom_call" | custom-call | flops 2147483648 | bytes 2097152 | tf_op jit(solution)/shard_map/pallas_call | solution.py:106
  137.7 0.5 all-to-all-done.3.refs_1_
  138.2 2.1 %shard_map.191 = bf16[8,32,2048]{2,1,0:T(8,128)(2,1)S(1)} custom-call(s32[1]{0:T(128)} %bitcast.refs_0_, bf16[8,128,128]{2,1,0:T(8,128)(2,1)S(1)} %all-to-all-done.3.refs_1_, bf16[128,128]{1,0:T(8,128)(2,1)} %copy-done.4, f32[2,128,256]{2,1,0:T(8,128)} %get-tuple-element.27.refs_3_, f32[1,128]{1,0:T(1,128)} %bitcast.43, ...), custom_call_target="tpu_custom_call" | custom-call | flops 1073741824 | bytes 2097152 | tf_op jit(solution)/shard_map/pallas_call | solution.py:106
  140.4 4.6 %all_to_all.30 = bf16[8,32,2048]{2,1,0:T(8,128)(2,1)S(1)} all-to-all(bf16[8,32,2048]{2,1,0:T(8,128)(2,1)S(1)} %shard_map.191), channel_id=1, replica_groups=mesh['sp_0'=8,'sp_1'=8,'fs'=4,'tp'=2] {'tp'}, dimensions={0} | all-to-all | bytes 2097152 | tf_op jit(solution)/shard_map/all_to_all | solution.py:571
  145.0 0.3 reduce_sum.24
  145.3 11.4 %all_to_all.31 = bf16[4,32,2048]{2,1,0:T(8,128)(2,1)S(1)} all-to-all(bf16[4,32,2048]{2,1,0:T(8,128)(2,1)S(1)} %reduce_sum.24), channel_id=1, replica_groups=mesh['sp_0'=8,'sp_1'=8,'fs'=4,'tp'=2] {'fs'}, dimensions={0} | all-to-all | bytes 1048576 | tf_op jit(solution)/shard_map/all_to_all | solution.py:573
  156.7 0.7 reduce_sum.25
  (6 shorter events, 0.1 us)
Async XLA Ops:
  7.2 29.6 %copy-start = (bf16[64,1024]{1,0:T(8,128)(2,1)S(1)}, bf16[64,1024]{1,0:T(8,128)(2,1)}, u32[]{:S(2)}) copy-start(bf16[64,1024]{1,0:T(8,128)(2,1)} %param.27) | copy-start | bytes 393220
  7.2 31.0 %copy-start.2 = (bf16[256,256]{1,0:T(8,128)(2,1)S(1)}, bf16[256,256]{1,0:T(8,128)(2,1)}, u32[]{:S(2)}) copy-start(bf16[256,256]{1,0:T(8,128)(2,1)} %refs_1_.2) | copy-start | bytes 393220
  7.2 31.0 %copy-start.5 = (f32[2048]{0:T(1024)S(1)}, f32[2048]{0:T(1024)}, u32[]{:S(2)}) copy-start(f32[2048]{0:T(1024)} %param.19) | copy-start | bytes 24580
  7.2 31.0 %copy-start.3 = (bf16[2048,64]{0,1:T(8,128)(2,1)S(1)}, bf16[2048,64]{0,1:T(8,128)(2,1)}, u32[]{:S(2)}) copy-start(bf16[2048,64]{0,1:T(8,128)(2,1)} %param.26) | copy-start | bytes 786436
  7.2 31.0 %copy-start.6 = (f32[2,256]{1,0:T(2,128)S(1)}, f32[2,256]{1,0:T(2,128)}, u32[]{:S(2)}) copy-start(f32[2,256]{1,0:T(2,128)} %refs_9_.1) | copy-start | bytes 6148
  9.0 32.3 %all-to-all-start = ((bf16[8,32,896]{2,1,0:T(8,128)(2,1)}), bf16[8,32,896]{2,1,0:T(8,128)(2,1)S(1)}, u32[]{:S(2)}, u32[]{:S(2)}) async-start(bf16[8,32,896]{2,1,0:T(8,128)(2,1)} %broadcast_in_dim.6), calls=%async_computation | async-start | bytes 917504 | tf_op jit(solution)/shard_map/all_to_all | solution.py:42
  16.6 113.4 %all-gather.2.cloned.1.call-start = ((), (), s32[]{:S(2)}) async-start(), calls=%async_computation.6 | async-start | bytes 2949120 | tf_op jit(solution)/shard_map/all_gather | solution.py:514
  16.7 9.4 %collective-permute-start.2 = (bf16[256,256]{1,0:T(8,128)(2,1)}, bf16[256,256]{1,0:T(8,128)(2,1)S(1)}, u32[]{:S(2)}, u32[]{:S(2)}) collective-permute-start(bf16[256,256]{1,0:T(8,128)(2,1)} %refs_1_.2), channel_id=1, source_target_pairs={{0,6},{2,0},{4,2},{6,4},{1,7},{3,1},{5,3},{7,5},{8,14},{10,8},{12,... | collective-permute-start | bytes 393224 | tf_op jit(solution)/shard_map/ppermute | solution.py:31
  21.1 7.7 %collective-permute-start.3 = (bf16[256,256]{1,0:T(8,128)(2,1)}, bf16[256,256]{1,0:T(8,128)(2,1)S(1)}, u32[]{:S(2)}, u32[]{:S(2)}) collective-permute-start(bf16[256,256]{1,0:T(8,128)(2,1)} %refs_1_.2), channel_id=1, source_target_pairs={{0,4},{2,6},{4,0},{6,2},{1,5},{3,7},{5,1},{7,3},{8,12},{10,14},{12... | collective-permute-start | bytes 393224 | tf_op jit(solution)/shard_map/ppermute | solution.py:31
  23.5 8.9 %collective-permute-start.1 = (bf16[256,256]{1,0:T(8,128)(2,1)}, bf16[256,256]{1,0:T(8,128)(2,1)S(1)}, u32[]{:S(2)}, u32[]{:S(2)}) collective-permute-start(bf16[256,256]{1,0:T(8,128)(2,1)} %refs_1_.2), channel_id=1, source_target_pairs={{0,2},{2,4},{4,6},{6,0},{1,3},{3,5},{5,7},{7,1},{8,10},{10,12},{12... | collective-permute-start | bytes 393224 | tf_op jit(solution)/shard_map/ppermute | solution.py:31
  33.4 4.8 %collective-permute-start.4 = (bf16[4,256,256]{2,1,0:T(8,128)(2,1)S(1)}, bf16[4,256,256]{2,1,0:T(8,128)(2,1)S(1)}, u32[]{:S(2)}, u32[]{:S(2)}) collective-permute-start(bf16[4,256,256]{2,1,0:T(8,128)(2,1)S(1)} %pad_maximum_fusion), channel_id=1, source_target_pairs={{0,1},{1,0},{2,3},{3,2},{4,5},{5,4},{6,7},{7,6},{8,9},{9,8},{10,11... | collective-permute-start | bytes 1572872 | tf_op jit(solution)/shard_map/ppermute | solution.py:31
  43.1 50.7 %all-to-all-start.1 = ((bf16[8,256,256]{2,1,0:T(8,128)(2,1)}), bf16[8,256,256]{2,1,0:T(8,128)(2,1)S(1)}, u32[]{:S(2)}, u32[]{:S(2)}) async-start(bf16[8,256,256]{2,1,0:T(8,128)(2,1)} %broadcast_in_dim.7), calls=%async_computation.1 | async-start | bytes 2097152 | tf_op jit(solution)/shard_map/all_to_all | solution.py:42
  53.1 4.9 %collective-permute-start = (bf16[128,256]{1,0:T(8,128)(2,1)S(1)}, bf16[128,256]{1,0:T(8,128)(2,1)S(1)}, u32[]{:S(2)}, u32[]{:S(2)}) collective-permute-start(bf16[128,256]{1,0:T(8,128)(2,1)S(1)} %slice.9), channel_id=1, source_target_pairs={{0,8},{8,16},{16,24},{24,32},{32,40},{40,48},{48,56},{56,64},{64,7... | collective-permute-start | bytes 196616 | tf_op jit(solution)/shard_map/ppermute | solution.py:37
  100.1 29.9 %copy-start.7 = (f32[2]{0:T(128)S(1)}, f32[2]{0:T(128)}, u32[]{:S(2)}) copy-start(f32[2]{0:T(128)} %refs_1_.3) | copy-start | bytes 28
  100.1 29.9 %copy-start.8 = (f32[64]{0:T(128)S(1)}, f32[64]{0:T(128)}, u32[]{:S(2)}) copy-start(f32[64]{0:T(128)} %param.30) | copy-start | bytes 772
  100.1 29.9 %copy-start.9 = (f32[64]{0:T(128)S(1)}, f32[64]{0:T(128)}, u32[]{:S(2)}) copy-start(f32[64]{0:T(128)} %param.31) | copy-start | bytes 772
  100.1 21.0 %all-to-all-start.2 = ((bf16[8,128,128]{2,1,0:T(8,128)(2,1)}), bf16[8,128,128]{2,1,0:T(8,128)(2,1)S(1)}, u32[]{:S(2)}, u32[]{:S(2)}) async-start(bf16[8,128,128]{2,1,0:T(8,128)(2,1)} %get-tuple-element.20), calls=%async_computation.2 | async-start | bytes 524288 | tf_op jit(solution)/shard_map/all_to_all | solution.py:543
  105.6 7.2 %collective-permute-start.6 = (bf16[128,256]{1,0:T(8,128)(2,1)S(1)}, bf16[128,256]{1,0:T(8,128)(2,1)S(1)}, u32[]{:S(2)}, u32[]{:S(2)}) collective-permute-start(bf16[128,256]{1,0:T(8,128)(2,1)S(1)} %collective-permute-done.refs_1_), channel_id=1, source_target_pairs={{0,6},{2,0},{4,2},{6,4},{1,7},{3,1},{5,3},{7,5},{8,14},{10,8},{12,... | collective-permute-start | bytes 196616 | tf_op jit(solution)/shard_map/ppermute | solution.py:31
  107.5 6.7 %collective-permute-start.7 = (bf16[128,256]{1,0:T(8,128)(2,1)S(1)}, bf16[128,256]{1,0:T(8,128)(2,1)S(1)}, u32[]{:S(2)}, u32[]{:S(2)}) collective-permute-start(bf16[128,256]{1,0:T(8,128)(2,1)S(1)} %collective-permute-done.refs_1_), channel_id=1, source_target_pairs={{0,4},{2,6},{4,0},{6,2},{1,5},{3,7},{5,1},{7,3},{8,12},{10,14},{12... | collective-permute-start | bytes 196616 | tf_op jit(solution)/shard_map/ppermute | solution.py:31
  109.4 7.7 %collective-permute-start.5 = (bf16[128,256]{1,0:T(8,128)(2,1)S(1)}, bf16[128,256]{1,0:T(8,128)(2,1)S(1)}, u32[]{:S(2)}, u32[]{:S(2)}) collective-permute-start(bf16[128,256]{1,0:T(8,128)(2,1)S(1)} %collective-permute-done.refs_1_), channel_id=1, source_target_pairs={{0,2},{2,4},{4,6},{6,0},{1,3},{3,5},{5,7},{7,1},{8,10},{10,12},{12... | collective-permute-start | bytes 196616 | tf_op jit(solution)/shard_map/ppermute | solution.py:31
  117.1 9.0 %collective-permute-start.8 = (bf16[4,128,256]{2,1,0:T(8,128)(2,1)S(1)}, bf16[4,128,256]{2,1,0:T(8,128)(2,1)S(1)}, u32[]{:S(2)}, u32[]{:S(2)}) collective-permute-start(bf16[4,128,256]{2,1,0:T(8,128)(2,1)S(1)} %pad_maximum_fusion.1), channel_id=1, source_target_pairs={{0,1},{1,0},{2,3},{3,2},{4,5},{5,4},{6,7},{7,6},{8,9},{9,8},{10,11... | collective-permute-start | bytes 786440 | tf_op jit(solution)/shard_map/ppermute | solution.py:31
  121.1 6.6 %copy-start.1 = (bf16[8,128,128]{2,1,0:T(8,128)(2,1)}, bf16[8,128,128]{2,1,0:T(8,128)(2,1)S(1)}, u32[]{:S(2)}) copy-start(bf16[8,128,128]{2,1,0:T(8,128)(2,1)S(1)} %all-to-all-done.2.refs_0_.refs_1_) | copy-start | bytes 786436
  122.5 15.7 %all-to-all-start.3 = ((bf16[8,128,128]{2,1,0:T(8,128)(2,1)}), bf16[8,128,128]{2,1,0:T(8,128)(2,1)S(1)}, u32[]{:S(2)}, u32[]{:S(2)}) async-start(bf16[8,128,128]{2,1,0:T(8,128)(2,1)} %shard_map.187), calls=%async_computation.3 | async-start | bytes 524288 | tf_op jit(solution)/shard_map/all_to_all | solution.py:546
  129.4 0.6 copy-start.4
Sparse Core Ops, SparseCore 0:
  42.2 63.6 all-gather.1
